TPU v7x, 32 devices: a whole 2x2x4 slice. The times are simulated.
32 devices in a mesh: sp: 8 (over z, x), tp: 4 (over y, core).
Axes of the slice: x: 2, y: 2, z: 4, core: 2. Of those that a mesh axis runs over, the one named last changes fastest.
Arguments:
- query_proj: bfloat16 [4096, 1024], P('sp', 'tp'), may hold values from -6 to 6
- projected_keys: bfloat16 [4096, 512], P('sp', 'tp'), may hold values from -6 to 6
- projected_values: bfloat16 [4096, 512], P('sp', 'tp'), may hold values from -6 to 6
- residual: bfloat16 [4096, 2048], P(('sp', 'tp')), may hold values from -6 to 6
- out_weight: bfloat16 [1024, 2048], replicated, may hold values from -0.1875 to 0.1875
- mix_gain: float32 [2048], replicated, may hold values from 0.1 to 1.9
- norm_gain: float32 [2048], replicated, may hold values from 0.1 to 1.9
- route_expert: int32 [4096, 2], P(('sp', 'tp')), may hold values from 0 to 31, all different within a row; in each aligned block of 128 rows (0 to 127, 128 to 255, ...) at most 16 rows name the same one
- route_weight: float32 [4096, 2], P(('sp', 'tp')), may hold values from 0.2 to 1
- expert_gate: bfloat16 [32, 2048, 1024], P(('sp', 'tp')), may hold values from -0.125 to 0.125
- expert_up: bfloat16 [32, 2048, 1024], P(('sp', 'tp')), may hold values from -0.125 to 0.125
- expert_down: bfloat16 [32, 1024, 2048], P(('sp', 'tp')), may hold values from -0.1875 to 0.1875
Outputs:
- output: bfloat16 [4096, 2048], P(('sp', 'tp'))
Inputs may be any that keep to these rules, and one draw needn't show every extreme that they name: `route_expert`: each row names 2 different experts. The rows of one device (aligned blocks of 128 rows) name any one expert at most 16 times, and in some blocks some expert is named exactly 16 times.
All inputs are finite; a program needn't handle non-finite values.
Results may differ from a plain program's by a relative error of at most 0.015.
Values may be sent and summed in bfloat16 or wider, within the bound.
No kernel may reach another device: no remote copies, remote signals or barrier semaphores. Data moves between devices by JAX's collectives and lax.ppermute only.
A program may use at most 128 MiB of HBM per device.

v0:
```python
import math

import jax
import jax.numpy as jnp
from jax import lax
from jax.sharding import PartitionSpec as P

D = 2048
HEAD_SIZE = 64
GRID_W = 64


epsilon = 1e-06
base_theta = 10000.0


def unit_length_rows(values):
    values = values.astype(jnp.float32)
    return values * lax.rsqrt(jnp.mean(values * values, axis=-1, keepdims=True) + epsilon)


def rotary_embed(head_vecs, offset):
    row_count = head_vecs.shape[0]
    quarter = head_vecs.shape[-1] // 4
    places = offset + jnp.arange(row_count, dtype=jnp.int32)
    grid_row = (places // GRID_W).astype(jnp.float32)
    grid_col = (places % GRID_W).astype(jnp.float32)
    frequency = base_theta ** (-jnp.arange(quarter, dtype=jnp.float32) / quarter)
    row_angle = grid_row[:, None, None] * frequency
    col_angle = grid_col[:, None, None] * frequency
    row_cos, row_sin = (jnp.cos(row_angle), jnp.sin(row_angle))
    col_cos, col_sin = (jnp.cos(col_angle), jnp.sin(col_angle))
    row_first = head_vecs[..., :quarter]
    row_second = head_vecs[..., quarter : 2 * quarter]
    col_first = head_vecs[..., 2 * quarter : 3 * quarter]
    col_second = head_vecs[..., 3 * quarter :]
    return jnp.concatenate(
        [
            row_first * row_cos - row_second * row_sin,
            row_second * row_cos + row_first * row_sin,
            col_first * col_cos - col_second * col_sin,
            col_second * col_cos + col_first * col_sin,
        ],
        axis=-1,
    )


def local(
    query_proj,
    projected_keys,
    projected_values,
    residual,
    out_weight,
    mix_gain,
    norm_gain,
    route_expert,
    route_weight,
    expert_gate,
    expert_up,
    expert_down,
):
    tok_count = query_proj.shape[0]
    q_heads = query_proj.shape[1] // HEAD_SIZE
    kv_heads = projected_keys.shape[1] // HEAD_SIZE
    query_group = q_heads // kv_heads
    offset = lax.axis_index("sp") * tok_count
    query_prepared = rotary_embed(
        unit_length_rows(query_proj.reshape(tok_count, q_heads, HEAD_SIZE)), offset
    ).astype(jnp.bfloat16)
    query_prepared = query_prepared.reshape(tok_count, kv_heads, query_group, HEAD_SIZE)
    key_prepared = rotary_embed(
        unit_length_rows(projected_keys.reshape(tok_count, kv_heads, HEAD_SIZE)), offset
    ).astype(jnp.bfloat16)
    v_ready = projected_values.reshape(tok_count, kv_heads, HEAD_SIZE)
    scale = HEAD_SIZE ** (-0.5)
    sums_start = jnp.zeros((tok_count, kv_heads, query_group, HEAD_SIZE), jnp.float32)
    totals_start = jnp.zeros((tok_count, kv_heads, query_group), jnp.float32)
    keys_all = lax.all_gather(key_prepared, "sp", axis=0, tiled=True)
    vals_all = lax.all_gather(v_ready, "sp", axis=0, tiled=True)
    key_count = keys_all.shape[0]
    model_width = math.gcd(key_count, 1024)
    key_blocks = keys_all.reshape(key_count // model_width, model_width, kv_heads, HEAD_SIZE)
    val_blocks = vals_all.reshape(key_count // model_width, model_width, kv_heads, HEAD_SIZE)

    def one_block(inner, pair):
        sums, totals = inner
        scores = (
            jnp.einsum(
                "thgd,nhd->thgn", query_prepared, pair[0], preferred_element_type=jnp.float32
            )
            * scale
        )
        weights = jnp.exp(scores)
        totals = totals + jnp.sum(weights, axis=-1)
        sums = sums + jnp.einsum(
            "thgn,nhd->thgd",
            weights.astype(jnp.bfloat16),
            pair[1],
            preferred_element_type=jnp.float32,
        )
        return ((sums, totals), None)

    result, unused = lax.scan(one_block, (sums_start, totals_start), (key_blocks, val_blocks))
    sums, totals = result
    attended = (
        (sums / totals[..., None]).astype(jnp.bfloat16).reshape(tok_count, q_heads * HEAD_SIZE)
    )
    by_token = lax.all_to_all(attended, "tp", split_axis=0, concat_axis=1, tiled=True)
    mixed = jnp.dot(by_token, out_weight, preferred_element_type=jnp.float32)
    stream = (residual.astype(jnp.float32) + unit_length_rows(mixed) * mix_gain).astype(
        jnp.bfloat16
    )
    normed = (unit_length_rows(stream) * norm_gain).astype(jnp.bfloat16)
    row_count = normed.shape[0]
    top_count = route_expert.shape[1]
    experts = lax.axis_size("sp") * lax.axis_size("tp")
    capacity = max(2, 2 * top_count * row_count // experts)
    flat_expert = route_expert.reshape(-1)
    onehot = (flat_expert[:, None] == jnp.arange(experts, dtype=jnp.int32)[None, :]).astype(
        jnp.int32
    )
    earlier = jnp.cumsum(onehot, axis=0) - onehot
    slot_rank = jnp.sum(earlier * onehot, axis=1)
    target = flat_expert * capacity + slot_rank
    placing = jnp.arange(experts * capacity, dtype=jnp.int32)[:, None] == target[None, :]
    placing = jnp.any(placing.reshape(experts * capacity, row_count, top_count), axis=2).astype(
        jnp.bfloat16
    )
    outgoing = jnp.dot(placing, normed, preferred_element_type=jnp.float32).astype(jnp.bfloat16)
    outgoing = outgoing.reshape(experts, capacity, D)
    gate_mat = expert_gate[0]
    up_mat = expert_up[0]
    down_mat = expert_down[0]
    slots = lax.all_to_all(outgoing, ("sp", "tp"), split_axis=0, concat_axis=0, tiled=True)
    flat_rows = slots.reshape(-1, slots.shape[-1])
    gate_pre = jnp.dot(flat_rows, gate_mat, preferred_element_type=jnp.float32)
    up_pre = jnp.dot(flat_rows, up_mat, preferred_element_type=jnp.float32)
    expert_act = (jax.nn.silu(gate_pre) * up_pre).astype(jnp.bfloat16)
    done = jnp.dot(expert_act, down_mat, preferred_element_type=jnp.float32).astype(jnp.bfloat16)
    answered = done.reshape(slots.shape)
    returned = lax.all_to_all(answered, ("sp", "tp"), split_axis=0, concat_axis=0, tiled=True)
    picked = jnp.take(returned.reshape(experts * capacity, D), target, axis=0).reshape(
        row_count, top_count, D
    )
    combined = jnp.sum(picked.astype(jnp.float32) * route_weight[:, :, None], axis=1)
    return (stream.astype(jnp.float32) + combined).astype(jnp.bfloat16)


def solution(mesh):
    return jax.shard_map(
        local,
        mesh=mesh,
        in_specs=(
            P("sp", "tp"),
            P("sp", "tp"),
            P("sp", "tp"),
            P(("sp", "tp"), None),
            P(),
            P(),
            P(),
            P(("sp", "tp"), None),
            P(("sp", "tp"), None),
            P(("sp", "tp"), None, None),
            P(("sp", "tp"), None, None),
            P(("sp", "tp"), None, None),
        ),
        out_specs=P(("sp", "tp"), None),
        check_vma=False,
    )
```

profile of v0, /device:TPU:0, one launch (start us, length us, event | category | flops | bytes accessed | tf_op | source)
XLA Modules:
  0.0 279.2 jit_solution(4073406177149737743)
XLA Ops:
  8.8 1.7 copy.71
  14.1 37.4 %all-gather.5.cloned.1.call-done = bf16[4096,2,64]{0,2,1:T(8,128)(2,1)} async-done(((bf16[512,2,64]{0,2,1:T(8,128)(2,1)}), bf16[4096,2,64]{0,2,1:T(8,128)(2,1)}) %all-gather.5.cloned.1.call-update) | async-done | bytes 1048592 | tf_op jit(solution)/shard_map/all_gather | solution.py:78
  51.5 1.3 copy.93
  52.8 39.2 %all-gather.3.cloned.1.call-done = bf16[4096,2,64]{0,2,1:T(8,128)(2,1)} async-done(((bf16[512,2,64]{0,2,1:T(8,128)(2,1)}), bf16[4096,2,64]{0,2,1:T(8,128)(2,1)}) %all-gather.3.cloned.1.call-update) | async-done | bytes 1048592 | tf_op jit(solution)/shard_map/all_gather | solution.py:79
  93.3 38.0 %while.13 = (s32[]{:T(128)}, f32[512,2,2,64]{0,3,2,1:T(8,128)S(1)}, f32[512,2,2]{0,2,1:T(2,128)S(1)}, bf16[4,1024,2,64]{1,3,2,0:T(8,128)(2,1)S(1)}, bf16[4,1024,...) while((s32[]{:T(128)}, f32[512,2,2,64]{0,3,2,1:T(8,128)S(1)}, ...), condition=%wide.region_4.5_spmd.clone, body=%wide.region_2.4_spmd.clone.sunk | while | flops 545523712 | bytes 18645096 | solution.py:103
  93.4 4.6 %bitcast_reduce_fusion.2 = (f32[512,2,2]{0,2,1:T(2,128)S(1)}, f32[2,1024,512,2]{2,1,3,0:T(8,128)}) fusion(bf16[512,2,2,64]{0,3,2,1:T(8,128)(2,1)S(1)} %get-tuple-element.193, bf16[4,1024,2,64]{1,3,2,0:T(8,128)(2,1)S(1)} %get-tuple-element.192, s32[]{:T(128)} %get-tuple-element.180), kind=kOutput, calls=%fused_computation.1.clone.1 | convolution fusion | flops 272627712 | bytes 8921092 | tf_op jit(solution)/shard_map/while/body/eval_jaxpr/thgd,nhd->thgn/dot_general | solution.py:88
  98.0 4.9 %fusion.58 = f32[512,2,2,64]{0,3,2,1:T(8,128)S(1)} fusion(f32[2,1024,512,2]{2,1,3,0:T(8,128)} %get-tuple-element.170, f32[512,2,2,64]{0,3,2,1:T(8,128)S(1)} %get-tuple-element.181, bf16[4,1024,2,64]{1,3,2,0:T(8,128)(2,1)S(1)} %get-tuple-element.191, s32[]{:T(128)} %get-tuple-element.180, pred[]{:T(512)S(6)} %compare.14), kind=kOutput, calls=%fused_computation.7.clone.1 | convolution fusion | flops 272891904 | bytes 9699333 | tf_op jit(solution)/shard_map/while/body/eval_jaxpr/thgn,nhd->thgd/dot_general | solution.py:95
  102.9 4.6 %bitcast_reduce_fusion.2 = (f32[512,2,2]{0,2,1:T(2,128)S(1)}, f32[2,1024,512,2]{2,1,3,0:T(8,128)}) fusion(bf16[512,2,2,64]{0,3,2,1:T(8,128)(2,1)S(1)} %get-tuple-element.193, bf16[4,1024,2,64]{1,3,2,0:T(8,128)(2,1)S(1)} %get-tuple-element.192, s32[]{:T(128)} %get-tuple-element.180), kind=kOutput, calls=%fused_computation.1.clone.1 | convolution fusion | flops 272627712 | bytes 8921092 | tf_op jit(solution)/shard_map/while/body/eval_jaxpr/thgd,nhd->thgn/dot_general | solution.py:88
  107.5 4.9 %fusion.58 = f32[512,2,2,64]{0,3,2,1:T(8,128)S(1)} fusion(f32[2,1024,512,2]{2,1,3,0:T(8,128)} %get-tuple-element.170, f32[512,2,2,64]{0,3,2,1:T(8,128)S(1)} %get-tuple-element.181, bf16[4,1024,2,64]{1,3,2,0:T(8,128)(2,1)S(1)} %get-tuple-element.191, s32[]{:T(128)} %get-tuple-element.180, pred[]{:T(512)S(6)} %compare.14), kind=kOutput, calls=%fused_computation.7.clone.1 | convolution fusion | flops 272891904 | bytes 9699333 | tf_op jit(solution)/shard_map/while/body/eval_jaxpr/thgn,nhd->thgd/dot_general | solution.py:95
  112.4 4.6 %bitcast_reduce_fusion.2 = (f32[512,2,2]{0,2,1:T(2,128)S(1)}, f32[2,1024,512,2]{2,1,3,0:T(8,128)}) fusion(bf16[512,2,2,64]{0,3,2,1:T(8,128)(2,1)S(1)} %get-tuple-element.193, bf16[4,1024,2,64]{1,3,2,0:T(8,128)(2,1)S(1)} %get-tuple-element.192, s32[]{:T(128)} %get-tuple-element.180), kind=kOutput, calls=%fused_computation.1.clone.1 | convolution fusion | flops 272627712 | bytes 8921092 | tf_op jit(solution)/shard_map/while/body/eval_jaxpr/thgd,nhd->thgn/dot_general | solution.py:88
  117.0 4.9 %fusion.58 = f32[512,2,2,64]{0,3,2,1:T(8,128)S(1)} fusion(f32[2,1024,512,2]{2,1,3,0:T(8,128)} %get-tuple-element.170, f32[512,2,2,64]{0,3,2,1:T(8,128)S(1)} %get-tuple-element.181, bf16[4,1024,2,64]{1,3,2,0:T(8,128)(2,1)S(1)} %get-tuple-element.191, s32[]{:T(128)} %get-tuple-element.180, pred[]{:T(512)S(6)} %compare.14), kind=kOutput, calls=%fused_computation.7.clone.1 | convolution fusion | flops 272891904 | bytes 9699333 | tf_op jit(solution)/shard_map/while/body/eval_jaxpr/thgn,nhd->thgd/dot_general | solution.py:95
  121.9 4.6 %bitcast_reduce_fusion.2 = (f32[512,2,2]{0,2,1:T(2,128)S(1)}, f32[2,1024,512,2]{2,1,3,0:T(8,128)}) fusion(bf16[512,2,2,64]{0,3,2,1:T(8,128)(2,1)S(1)} %get-tuple-element.193, bf16[4,1024,2,64]{1,3,2,0:T(8,128)(2,1)S(1)} %get-tuple-element.192, s32[]{:T(128)} %get-tuple-element.180), kind=kOutput, calls=%fused_computation.1.clone.1 | convolution fusion | flops 272627712 | bytes 8921092 | tf_op jit(solution)/shard_map/while/body/eval_jaxpr/thgd,nhd->thgn/dot_general | solution.py:88
  126.5 4.9 %fusion.58 = f32[512,2,2,64]{0,3,2,1:T(8,128)S(1)} fusion(f32[2,1024,512,2]{2,1,3,0:T(8,128)} %get-tuple-element.170, f32[512,2,2,64]{0,3,2,1:T(8,128)S(1)} %get-tuple-element.181, bf16[4,1024,2,64]{1,3,2,0:T(8,128)(2,1)S(1)} %get-tuple-element.191, s32[]{:T(128)} %get-tuple-element.180, pred[]{:T(512)S(6)} %compare.14), kind=kOutput, calls=%fused_computation.7.clone.1 | convolution fusion | flops 272891904 | bytes 9699333 | tf_op jit(solution)/shard_map/while/body/eval_jaxpr/thgn,nhd->thgd/dot_general | solution.py:95
  132.3 3.5 %all-to-all-start = ((bf16[4,128,256]{1,2,0:T(8,128)(2,1)}), bf16[4,128,256]{1,2,0:T(8,128)(2,1)S(1)}, u32[]{:S(2)}, u32[]{:S(2)}) async-start(bf16[4,128,256]{1,2,0:T(8,128)(2,1)} %copy.76), calls=%async_computation | async-start | bytes 524288 | tf_op jit(solution)/shard_map/all_to_all | solution.py:108
  135.9 5.9 %all-to-all-done = bf16[4,128,256]{1,2,0:T(8,128)(2,1)S(1)} async-done(((bf16[4,128,256]{1,2,0:T(8,128)(2,1)}), bf16[4,128,256]{1,2,0:T(8,128)(2,1)S(1)}, u32[]{:S(2)}, u32[]{:S(2)}) %all-to-all-start) | async-done | bytes 262176 | tf_op jit(solution)/shard_map/all_to_all | solution.py:108
  141.8 3.0 %multiply_reduce_fusion.1 = (f32[128]{0:T(128)S(1)}, f32[128,2048]{1,0:T(8,128)S(1)}) fusion(bf16[128,1024]{0,1:T(8,128)(2,1)S(1)} %bitcast.119, bf16[1024,2048]{1,0:T(8,128)(2,1)} %param.18), kind=kOutput, calls=%fused_computation.38 | convolution fusion | flops 537395072 | bytes 5505536 | tf_op jit(solution)/shard_map/dot_general | solution.py:109
  146.0 51.2 %all_to_all.29 = bf16[32,16,2048]{2,1,0:T(8,128)(2,1)S(1)} all-to-all(bf16[32,16,2048]{2,1,0:T(8,128)(2,1)S(1)} %bitcast.113), channel_id=1, replica_groups=mesh['sp'=8,'tp'=4] {'sp','tp'}, dimensions={0} | all-to-all | bytes 4194304 | tf_op jit(solution)/shard_map/all_to_all | solution.py:134
  197.2 3.7 %fusion.16 = f32[512,1024]{1,0:T(8,128)} fusion(bf16[512,2048]{1,0:T(8,128)(2,1)S(1)} %bitcast.117, bf16[1,2048,1024]{2,1,0:T(8,128)(2,1)S(1)} %copy-done.5), kind=kOutput, calls=%fused_computation.21 | convolution fusion | flops 2147483648 | bytes 8388608 | tf_op jit(solution)/shard_map/dot_general | solution.py:136
  200.9 9.9 %fusion.18 = bf16[512,2048]{1,0:T(8,128)(2,1)} fusion(bf16[1,1024,2048]{2,1,0:T(8,128)(2,1)} %param.25, f32[512,1024]{1,0:T(8,128)} %fusion.16, bf16[512,2048]{1,0:T(8,128)(2,1)S(1)} %bitcast.118, bf16[1,2048,1024]{2,1,0:T(8,128)(2,1)} %param.24), kind=kOutput, calls=%fused_computation.23 | convolution fusion | flops 4299161600 | bytes 14680064 | tf_op jit(solution)/shard_map/dot_general | solution.py:139
  210.8 3.7 %all-to-all-start.2 = ((bf16[32,16,2048]{2,1,0:T(8,128)(2,1)}), bf16[32,16,2048]{2,1,0:T(8,128)(2,1)S(1)}, u32[]{:S(2)}, u32[]{:S(2)}) async-start(bf16[32,16,2048]{2,1,0:T(8,128)(2,1)} %bitcast.116), calls=%async_computation.2 | async-start | bytes 4194304 | tf_op jit(solution)/shard_map/all_to_all | solution.py:141
  215.1 48.2 %all-to-all-done.2 = bf16[32,16,2048]{2,1,0:T(8,128)(2,1)S(1)} async-done(((bf16[32,16,2048]{2,1,0:T(8,128)(2,1)}), bf16[32,16,2048]{2,1,0:T(8,128)(2,1)S(1)}, u32[]{:S(2)}, u32[]{:S(2)}) %all-to-all-start.2) | async-done | bytes 2097184 | tf_op jit(solution)/shard_map/all_to_all | solution.py:141
  263.2 2.3 gather_fusion
  265.6 1.7 gather.7
  267.3 4.1 %multiply_reduce_fusion = f32[128,2048]{1,0:T(8,128)S(1)} fusion(bf16[128,2,2048]{2,1,0:T(2,128)(2,1)S(1)} %gather.7, pred[128,2]{1,0:T(8,128)(4,1)S(1)} %copy.81, f32[128,2]{1,0:T(8,128)S(1)} %copy.83), kind=kLoop, calls=%fused_computation.25 | loop fusion | flops 1835008 | bytes 2098432 | tf_op jit(solution)/shard_map/reduce_sum | solution.py:145
  (66 shorter events, 10.7 us)
Async XLA Ops:
  6.5 45.0 %all-gather.5.cloned.1.call-start = ((), (), s32[]{:S(2)}) async-start(), calls=%async_computation.4 | async-start | bytes 1179648 | tf_op jit(solution)/shard_map/all_gather | solution.py:78
  8.7 83.3 %all-gather.3.cloned.1.call-start = ((), (), s32[]{:S(2)}) async-start(), calls=%async_computation.3 | async-start | bytes 1179648 | tf_op jit(solution)/shard_map/all_gather | solution.py:79
  93.3 42.5 %copy-start.1 = (s32[128,2]{0,1:T(2,128)S(1)}, s32[128,2]{0,1:T(2,128)}, u32[]{:S(2)}) copy-start(s32[128,2]{0,1:T(2,128)} %param.21) | copy-start | bytes 3076
  131.4 13.4 %copy-start = (bf16[128,2048]{1,0:T(8,128)(2,1)S(1)}, bf16[128,2048]{1,0:T(8,128)(2,1)}, u32[]{:S(2)}) copy-start(bf16[128,2048]{1,0:T(8,128)(2,1)} %param.17) | copy-start | bytes 1572868
  131.4 13.4 %copy-start.2 = (f32[2048]{0:T(1024)S(1)}, f32[2048]{0:T(1024)}, u32[]{:S(2)}) copy-start(f32[2048]{0:T(1024)} %param.19) | copy-start | bytes 24580
  132.3 13.0 %copy-start.3 = (f32[2048]{0:T(1024)S(1)}, f32[2048]{0:T(1024)}, u32[]{:S(2)}) copy-start(f32[2048]{0:T(1024)} %param.20) | copy-start | bytes 24580
  132.3 9.5 %all-to-all-start = ((bf16[4,128,256]{1,2,0:T(8,128)(2,1)}), bf16[4,128,256]{1,2,0:T(8,128)(2,1)S(1)}, u32[]{:S(2)}, u32[]{:S(2)}) async-start(bf16[4,128,256]{1,2,0:T(8,128)(2,1)} %copy.76), calls=%async_computation | async-start | bytes 524288 | tf_op jit(solution)/shard_map/all_to_all | solution.py:108
  144.8 52.4 %copy-start.5 = (bf16[1,2048,1024]{2,1,0:T(8,128)(2,1)S(1)}, bf16[1,2048,1024]{2,1,0:T(8,128)(2,1)}, u32[]{:S(2)}) copy-start(bf16[1,2048,1024]{2,1,0:T(8,128)(2,1)} %param.23) | copy-start | bytes 12582916
  210.8 4.1 %copy-start.4 = (f32[128,2]{0,1:T(2,128)S(1)}, f32[128,2]{0,1:T(2,128)}, u32[]{:S(2)}) copy-start(f32[128,2]{0,1:T(2,128)} %param.22) | copy-start | bytes 3076
  210.8 52.4 %all-to-all-start.2 = ((bf16[32,16,2048]{2,1,0:T(8,128)(2,1)}), bf16[32,16,2048]{2,1,0:T(8,128)(2,1)S(1)}, u32[]{:S(2)}, u32[]{:S(2)}) async-start(bf16[32,16,2048]{2,1,0:T(8,128)(2,1)} %bitcast.116), calls=%async_computation.2 | async-start | bytes 4194304 | tf_op jit(solution)/shard_map/all_to_all | solution.py:141
Sparse Core Ops, SparseCore 0:
  9.4 42.1 all-gather.4
  53.6 38.3 all-gather.2
where the time goes:
time: 280 us; the launch traced here: 279 us
  waiting for transfers between devices  131 us (47%)
  matrix products  55.3 us (20%)
  blocking collectives  51.2 us (18%)
  between operations  13.7 us (5%)
  local copies, waits for them, and re-layouts  13.3 us (5%)
  other arithmetic  7.73 us (3%)
  starting transfers between devices  7.26 us (3%)
    all_to_all x1, blocking collectives, local(): lax.all_to_all(outgoing, ('sp', 'tp'), split_axis=0, concat_axis=0, tiled...  51.2 us
    all_to_all x1, waiting for transfers between devices, local(): lax.all_to_all(answered, ('sp', 'tp'), split_axis=0, concat_axis=0, tiled...  48.2 us
    all_gather x1, waiting for transfers between devices, local(): vals_all = lax.all_gather(v_ready, 'sp', axis=0, tiled=True)  39.2 us
    all_gather x1, waiting for transfers between devices, local(): keys_all = lax.all_gather(key_prepared, 'sp', axis=0, tiled=True)  37.4 us
    dot_general x4, matrix products, one_block(): jnp.einsum('thgn,nhd->thgd', weights.astype(jnp.bfloat16), pair[1], prefe...  19.4 us
    dot_general x4, matrix products, one_block(): jnp.einsum('thgd,nhd->thgn', query_prepared, pair[0], preferred_element_t...  18.4 us
    dot_general x1, matrix products, local(): jnp.dot(expert_act, down_mat, preferred_element_type=jnp.float32)  9.89 us
    all_to_all x1, waiting for transfers between devices, local(): lax.all_to_all(attended, 'tp', split_axis=0, concat_axis=1, tiled=True)  5.88 us
  transfers between devices with their start and end apart: 4, of which 4 were waited for; matrix products, arithmetic and copies ran while one was open for 3% of the time, Pallas kernels for 0%

commit v1 on v0

v1 whole, which is shorter than its diff:
```python
import functools
import math

import jax
import jax.numpy as jnp
from jax import lax
from jax.experimental import pallas as pl
from jax.experimental.pallas import tpu as pltpu
from jax.sharding import PartitionSpec as P

HEAD_SIZE = 64
GRID_W = 64
HALF_KEYS = 256
ONES_ROWS = 16

epsilon = 1e-06
base_theta = 10000.0

VMEM = pl.BlockSpec(memory_space=pltpu.VMEM)


def unit_length_rows(values):
    values = values.astype(jnp.float32)
    return values * lax.rsqrt(jnp.mean(values * values, axis=-1, keepdims=True) + epsilon)


def rotation_tables(tok_count, offset, lanes):
    quarter = HEAD_SIZE // 4
    lane = jnp.arange(lanes, dtype=jnp.int32) % HEAD_SIZE
    places = offset + jnp.arange(tok_count, dtype=jnp.int32)
    grid_row = (places // GRID_W).astype(jnp.float32)[:, None]
    grid_col = (places % GRID_W).astype(jnp.float32)[:, None]
    frequency = base_theta ** (-(lane % quarter).astype(jnp.float32) / quarter)
    angle = jnp.where((lane < 2 * quarter)[None, :], grid_row, grid_col) * frequency[None, :]
    sign = jnp.where((lane // quarter) % 2 == 0, -1.0, 1.0).astype(jnp.float32)
    return jnp.cos(angle), jnp.sin(angle) * sign[None, :]


def prepare_kernel(q_ref, k_ref, v_ref, cos_ref, sin_ref, q_out, kv_out):
    tok_count, lanes = k_ref.shape
    rows = lax.broadcasted_iota(jnp.int32, (lanes, lanes), 0)
    cols = lax.broadcasted_iota(jnp.int32, (lanes, lanes), 1)
    same_head = (rows // HEAD_SIZE) == (cols // HEAD_SIZE)
    mean_mat = jnp.where(same_head, 1.0 / HEAD_SIZE, 0.0).astype(jnp.bfloat16)
    swap_mat = jnp.where((rows ^ (HEAD_SIZE // 4)) == cols, 1.0, 0.0).astype(jnp.bfloat16)

    def ready(raw, factor):
        wide = raw.astype(jnp.float32)
        square = wide * wide
        high = square.astype(jnp.bfloat16)
        low = (square - high.astype(jnp.float32)).astype(jnp.bfloat16)
        mean = jnp.dot(high, mean_mat, preferred_element_type=jnp.float32) + jnp.dot(
            low, mean_mat, preferred_element_type=jnp.float32
        )
        swapped = jnp.dot(raw, swap_mat, preferred_element_type=jnp.float32)
        length = lax.rsqrt(mean + epsilon) * factor
        return (wide * cos_ref[...] + swapped * sin_ref[...]) * length

    factor = math.log2(math.e) * HEAD_SIZE ** (-0.5)
    group = q_ref.shape[1] // lanes
    q_out[...] = jnp.zeros_like(q_out)
    for block in range(group):
        turned = ready(q_ref[:, block * lanes : (block + 1) * lanes], factor).T
        for inner in range(lanes // HEAD_SIZE):
            head = block * (lanes // HEAD_SIZE) + inner
            kv_head = head // group
            q_out[
                kv_head * HEAD_SIZE : (kv_head + 1) * HEAD_SIZE,
                head * tok_count : (head + 1) * tok_count,
            ] = turned[inner * HEAD_SIZE : (inner + 1) * HEAD_SIZE].astype(jnp.bfloat16)
    keys = ready(k_ref[...], 1.0).astype(jnp.bfloat16)
    for half in range(tok_count // HALF_KEYS):
        begin = half * HALF_KEYS
        kv_out[half, :HALF_KEYS, :] = keys[begin : begin + HALF_KEYS]
        for part in range(HALF_KEYS // lanes):
            start = begin + part * lanes
            at = HALF_KEYS + part * lanes
            kv_out[half, at : at + lanes, :] = (
                v_ref[start : start + lanes, :].astype(jnp.float32).T.astype(jnp.bfloat16)
            )


def attend_kernel(chunk_count, first, last, *refs):
    q_ref = refs[0]
    chunks = refs[1 : 1 + chunk_count]
    acc_in = None if first else refs[1 + chunk_count]
    out_ref = refs[-1]
    lanes, columns = q_ref.shape
    width = 256
    kv_heads = lanes // HEAD_SIZE
    halves = [(c, i) for c in chunks for i in range(c.shape[0])]
    ones = jnp.ones((ONES_ROWS, HALF_KEYS), jnp.bfloat16)
    for block in range(columns // width):
        kv_head = block // (columns // width // kv_heads)
        q_block = q_ref[:, block * width : (block + 1) * width]
        total = None if first else acc_in[:, block * width : (block + 1) * width]
        for chunk, half in halves:
            scores = jnp.dot(
                chunk[half, :HALF_KEYS, :], q_block, preferred_element_type=jnp.float32
            )
            weights = jnp.exp2(scores).astype(jnp.bfloat16)
            values = jnp.concatenate(
                [
                    chunk[
                        half,
                        pl.ds(HALF_KEYS + part * lanes + kv_head * HEAD_SIZE, HEAD_SIZE),
                        :,
                    ]
                    for part in range(HALF_KEYS // lanes)
                ],
                axis=1,
            )
            values = jnp.concatenate([values, ones], axis=0)
            piece = jnp.dot(values, weights, preferred_element_type=jnp.float32)
            total = piece if total is None else total + piece
        if not last:
            out_ref[:, block * width : (block + 1) * width] = total
        else:
            tp, head_rows, per = out_ref.shape
            tok_count = tp * per
            ready = (total[:HEAD_SIZE] / total[HEAD_SIZE : HEAD_SIZE + 1]).astype(jnp.bfloat16)
            head = block * width // tok_count
            for piece in range(width // per):
                slot = (block * width + piece * per - head * tok_count) // per
                out_ref[slot, head * HEAD_SIZE : (head + 1) * HEAD_SIZE, :] = ready[
                    :, piece * per : (piece + 1) * per
                ]


def attend(q_ready, chunks, acc, final_shape):
    first, last = acc is None, final_shape is not None
    lanes, columns = q_ready.shape
    rows = HEAD_SIZE + ONES_ROWS
    key_count = sum(c.shape[0] for c in chunks) * HALF_KEYS
    shape = (
        jax.ShapeDtypeStruct(final_shape, jnp.bfloat16)
        if last
        else jax.ShapeDtypeStruct((rows, columns), jnp.float32)
    )
    operands = [q_ready, *chunks] + ([] if first else [acc])
    aliases = {} if (first or last) else {len(operands) - 1: 0}
    return pl.pallas_call(
        functools.partial(attend_kernel, len(chunks), first, last),
        out_shape=shape,
        in_specs=[VMEM] * len(operands),
        out_specs=VMEM,
        input_output_aliases=aliases,
        cost_estimate=pl.CostEstimate(
            flops=2 * key_count * columns * (256 + 256),
            bytes_accessed=key_count * 1024,
            transcendentals=key_count * columns,
        ),
        compiler_params=pltpu.CompilerParams(vmem_limit_bytes=24 * 1024 * 1024),
    )(*operands)


def local(
    sp_size,
    tp_size,
    query_proj,
    projected_keys,
    projected_values,
    residual,
    out_weight,
    mix_gain,
    norm_gain,
    route_expert,
    route_weight,
    expert_gate,
    expert_up,
    expert_down,
):
    tok_count, lanes = projected_keys.shape
    q_heads = query_proj.shape[1] // HEAD_SIZE
    model_width = residual.shape[1]
    offset = lax.axis_index("sp") * tok_count
    cos_table, sin_table = rotation_tables(tok_count, offset, lanes)
    q_ready, kv_own = pl.pallas_call(
        prepare_kernel,
        out_shape=(
            jax.ShapeDtypeStruct((lanes, q_heads * tok_count), jnp.bfloat16),
            jax.ShapeDtypeStruct((tok_count // HALF_KEYS, 2 * HALF_KEYS, lanes), jnp.bfloat16),
        ),
        in_specs=[VMEM] * 5,
        out_specs=(VMEM, VMEM),
        cost_estimate=pl.CostEstimate(
            flops=2 * tok_count * 512 * 512, bytes_accessed=1 << 20, transcendentals=0
        ),
        compiler_params=pltpu.CompilerParams(vmem_limit_bytes=24 * 1024 * 1024),
    )(query_proj, projected_keys, projected_values, cos_table, sin_table)

    order = list(range(0, sp_size, 2)) + list(range(sp_size - 1, 0, -2))
    ahead = [(order[i], order[(i + 1) % sp_size]) for i in range(sp_size)]
    behind = [(b, a) for a, b in ahead]
    final_shape = (tp_size, q_heads * HEAD_SIZE, tok_count // tp_size)
    steps = sp_size // 2
    acc = None
    from_left = from_right = kv_own
    held = [kv_own]
    for step in range(steps):
        if step == steps - 1:
            halves = kv_own.shape[0]
            from_left, from_right = from_left[: halves // 2], from_right[halves // 2 :]
        next_left = lax.ppermute(from_left, "sp", ahead)
        next_right = lax.ppermute(from_right, "sp", behind)
        acc = attend(q_ready, held, acc, None)
        from_left, from_right = next_left, next_right
        held = [from_left, from_right]
    attended = attend(q_ready, held, acc, final_shape)
    by_token = lax.all_to_all(attended, "tp", split_axis=0, concat_axis=0, tiled=True)
    by_token = by_token.reshape(-1, by_token.shape[-1])
    mixed = lax.dot_general(
        by_token, out_weight, (((0,), (0,)), ((), ())), preferred_element_type=jnp.float32
    )
    stream = (residual.astype(jnp.float32) + unit_length_rows(mixed) * mix_gain).astype(
        jnp.bfloat16
    )
    normed = (unit_length_rows(stream) * norm_gain).astype(jnp.bfloat16)
    row_count = normed.shape[0]
    top_count = route_expert.shape[1]
    experts = sp_size * tp_size
    capacity = max(2, 2 * top_count * row_count // experts)
    flat_expert = route_expert.T.reshape(-1)
    onehot = flat_expert[:, None] == jnp.arange(experts, dtype=jnp.int32)[None, :]
    onehot_low = onehot.astype(jnp.bfloat16)
    pairs = flat_expert.shape[0]
    before = (
        jnp.arange(pairs, dtype=jnp.int32)[None, :] < jnp.arange(pairs, dtype=jnp.int32)[:, None]
    ).astype(jnp.bfloat16)
    earlier = jnp.dot(before, onehot_low, preferred_element_type=jnp.float32)
    slot_rank = jnp.sum(jnp.where(onehot, earlier, 0.0), axis=1).astype(jnp.int32)
    target = flat_expert * capacity + slot_rank
    slots_total = experts * capacity
    chosen = target[:, None] == jnp.arange(slots_total, dtype=jnp.int32)[None, :]
    chosen = chosen.reshape(top_count, row_count, slots_total)
    placing = jnp.any(chosen, axis=0).astype(jnp.bfloat16)
    outgoing = lax.dot_general(
        placing, normed, (((0,), (0,)), ((), ())), preferred_element_type=jnp.float32
    ).astype(jnp.bfloat16)
    outgoing = outgoing.reshape(experts, capacity, model_width)
    gate_mat = expert_gate[0]
    up_mat = expert_up[0]
    down_mat = expert_down[0]
    slots = lax.all_to_all(outgoing, ("sp", "tp"), split_axis=0, concat_axis=0, tiled=True)
    flat_rows = slots.reshape(-1, slots.shape[-1])
    gate_pre = jnp.dot(flat_rows, gate_mat, preferred_element_type=jnp.float32)
    up_pre = jnp.dot(flat_rows, up_mat, preferred_element_type=jnp.float32)
    expert_act = (jax.nn.silu(gate_pre) * up_pre).astype(jnp.bfloat16)
    done = jnp.dot(expert_act, down_mat, preferred_element_type=jnp.float32).astype(jnp.bfloat16)
    answered = done.reshape(slots.shape)
    returned = lax.all_to_all(answered, ("sp", "tp"), split_axis=0, concat_axis=0, tiled=True)
    returned = returned.reshape(slots_total, model_width)
    combined = stream.astype(jnp.float32)
    for k in range(top_count):
        picked = jnp.dot(
            chosen[k].astype(jnp.bfloat16), returned, preferred_element_type=jnp.float32
        )
        combined = combined + picked * route_weight[:, k : k + 1]
    return combined.astype(jnp.bfloat16)


def solution(mesh):
    return jax.shard_map(
        functools.partial(local, mesh.shape["sp"], mesh.shape["tp"]),
        mesh=mesh,
        in_specs=(
            P("sp", "tp"),
            P("sp", "tp"),
            P("sp", "tp"),
            P(("sp", "tp"), None),
            P(),
            P(),
            P(),
            P(("sp", "tp"), None),
            P(("sp", "tp"), None),
            P(("sp", "tp"), None, None),
            P(("sp", "tp"), None, None),
            P(("sp", "tp"), None, None),
        ),
        out_specs=P(("sp", "tp"), None),
        check_vma=False,
    )
```

time: 280 us -> 177 us (0.63)
  waiting for transfers between devices: 131 us -> 63.9 us
  matrix products: 55.3 us -> 19.6 us
  Pallas kernels: 0 us -> 18.6 us
  between operations: 13.7 us -> 0.24 us
  local copies, waits for them, and re-layouts: 13.3 us -> 3.08 us
  starting transfers between devices: 7.26 us -> 16.5 us
  other arithmetic: 7.73 us -> 1.7 us
    all_gather x2 -> x0, waiting for transfers between devices: 76.6 us -> none  [the longest x1 39.2 us: local(): vals_all = lax.all_gather(v_ready, 'sp', axis=0, tiled=True)]
    dot_general x10 -> x5, matrix products: 41.7 us -> 5.87 us  [the longest x1 3.07 us: local(): lax.dot_general(by_token, out_weight, (((0,), (0,)), ((), ())), preferred...]
    pallas_call x0 -> x6, Pallas kernels: none -> 18.6 us  [the longest x5 18 us: attend(): pl.pallas_call(functools.partial(attend_kernel, len(chunks), first, last)...]
    ppermute x0 -> x8, waiting for transfers between devices: none -> 9.51 us  [the longest x4 9.24 us: local(): next_left = lax.ppermute(from_left, 'sp', ahead)]
    ppermute x0 -> x8, starting transfers between devices: none -> 9.47 us  [the longest x4 8.08 us: local(): next_left = lax.ppermute(from_left, 'sp', ahead)]
    reduce_sum x2 -> x0, other arithmetic: 4.17 us -> none  [the longest x1 4.07 us: local(): jnp.sum(picked.astype(jnp.float32) * route_weight[:, :, None], axis=1)]
    gather x2 -> x0, local copies, waits for them, and re-layouts: 4.09 us -> none  [local(): jnp.take(returned.reshape(experts * capacity, D), target, axis=0)]
  transfers between devices with their start and end apart: 4 -> 10, of which waited for: 4 -> 5; matrix products, arithmetic and copies ran while one was open for 3% -> 0% of each run, Pallas kernels for 0% -> 8%
where the time goes in v1:
time: 177 us
  waiting for transfers between devices  63.9 us (36%)
  blocking collectives  53.1 us (30%)
  matrix products  19.6 us (11%)
  Pallas kernels  18.6 us (11%)
  starting transfers between devices  16.5 us (9%)
  local copies, waits for them, and re-layouts  3.08 us (2%)
    all_to_all x1, blocking collectives, local(): lax.all_to_all(outgoing, ('sp', 'tp'), split_axis=0, concat_axis=0, tiled...  53.1 us
    all_to_all x1, waiting for transfers between devices, local(): lax.all_to_all(answered, ('sp', 'tp'), split_axis=0, concat_axis=0, tiled...  48.5 us
    pallas_call x5, Pallas kernels, attend(): pl.pallas_call(functools.partial(attend_kernel, len(chunks), first, last)...  18 us
    dot_general x1, matrix products, local(): jnp.dot(expert_act, down_mat, preferred_element_type=jnp.float32)  9.97 us
    ppermute x4, waiting for transfers between devices, local(): next_left = lax.ppermute(from_left, 'sp', ahead)  9.24 us
    ppermute x4, starting transfers between devices, local(): next_left = lax.ppermute(from_left, 'sp', ahead)  8.08 us
    all_to_all x1, waiting for transfers between devices, local(): lax.all_to_all(attended, 'tp', split_axis=0, concat_axis=0, tiled=True)  5.84 us
    dot_general x1, matrix products, local(): gate_pre = jnp.dot(flat_rows, gate_mat, preferred_element_type=jnp.float32)  3.72 us
  transfers between devices with their start and end apart: 10, of which 5 were waited for; matrix products, arithmetic and copies ran while one was open for 0% of the time, Pallas kernels for 8%

profile of v1, /device:TPU:0, one launch (start us, length us, event | category | flops | bytes accessed | tf_op | source)
XLA Modules:
  0.0 176.7 jit_solution(10395617111766820444)
XLA Ops:
  0.1 1.0 sine_multiply_fusion
  1.1 0.9 copy-done
  2.0 0.9 copy-done.1
  2.9 0.9 copy-done.2
  4.5 3.1 %collective-permute-start = (bf16[2,512,128]{2,1,0:T(8,128)(2,1)S(1)}, bf16[2,512,128]{2,1,0:T(8,128)(2,1)S(1)}, u32[]{:S(2)}, u32[]{:S(2)}) collective-permute-start(bf16[2,512,128]{2,1,0:T(8,128)(2,1)S(1)} %get-tuple-element.8.refs_1_), channel_id=1, source_target_pairs={{0,8},{8,16},{16,24},{24,28},{28,20},{20,12},{12,4},{4,0},{1,9},{9... | collective-permute-start | bytes 786440 | tf_op jit(solution)/shard_map/ppermute | solution.py:204
  7.6 6.2 %collective-permute-done.refs_1_ = bf16[2,512,128]{2,1,0:T(8,128)(2,1)S(1)} collective-permute-done((bf16[2,512,128]{2,1,0:T(8,128)(2,1)S(1)}, bf16[2,512,128]{2,1,0:T(8,128)(2,1)S(1)}, u32[]{:S(2)}, u32[]{:S(2)}) %collective-permute-start) | collective-permute-done | bytes 262176 | tf_op jit(solution)/shard_map/ppermute | solution.py:204
  13.8 1.8 %collective-permute-start.1 = (bf16[2,512,128]{2,1,0:T(8,128)(2,1)S(1)}, bf16[2,512,128]{2,1,0:T(8,128)(2,1)S(1)}, u32[]{:S(2)}, u32[]{:S(2)}) collective-permute-start(bf16[2,512,128]{2,1,0:T(8,128)(2,1)S(1)} %collective-permute-done.refs_1_), channel_id=1, source_target_pairs={{0,8},{8,16},{16,24},{24,28},{28,20},{20,12},{12,4},{4,0},{1,9},{9... | collective-permute-start | bytes 786440 | tf_op jit(solution)/shard_map/ppermute | solution.py:204
  15.8 2.2 %shard_map.119.refs_3_ = f32[80,2048]{1,0:T(8,128)S(1)} custom-call(bf16[128,2048]{1,0:T(8,128)(2,1)S(1)} %get-tuple-element.7.refs_0_, bf16[2,512,128]{2,1,0:T(8,128)(2,1)S(1)} %get-tuple-element.8.refs_1_), custom_call_target="tpu_custom_call" | custom-call | flops 1073741824 | bytes 524288 | tf_op jit(solution)/shard_map/pallas_call | solution.py:142
  18.2 3.0 %collective-permute-done.1.refs_1_ = bf16[2,512,128]{2,1,0:T(8,128)(2,1)S(1)} collective-permute-done((bf16[2,512,128]{2,1,0:T(8,128)(2,1)S(1)}, bf16[2,512,128]{2,1,0:T(8,128)(2,1)S(1)}, u32[]{:S(2)}, u32[]{:S(2)}) %collective-permute-start.1) | collective-permute-done | bytes 262176 | tf_op jit(solution)/shard_map/ppermute | solution.py:204
  21.3 1.6 collective-permute-start.2
  23.3 4.2 %shard_map.120.refs_3_ = f32[80,2048]{1,0:T(8,128)S(1)} custom-call(bf16[128,2048]{1,0:T(8,128)(2,1)S(1)} %get-tuple-element.7.refs_0_, bf16[2,512,128]{2,1,0:T(8,128)(2,1)S(1)} %collective-permute-done.refs_1_, bf16[2,512,128]{2,1,0:T(8,128)(2,1)S(1)} %collective-permute-done.4.refs_2_, ...), custom_call_target="tpu_custom_call", output_to_operand_aliasing={{}: (3, {})} | custom-call | flops 2147483648 | bytes 1048576 | tf_op jit(solution)/shard_map/pallas_call | solution.py:142
  27.5 4.2 %shard_map.121.refs_3_ = f32[80,2048]{1,0:T(8,128)S(1)} custom-call(bf16[128,2048]{1,0:T(8,128)(2,1)S(1)} %get-tuple-element.7.refs_0_, bf16[2,512,128]{2,1,0:T(8,128)(2,1)S(1)} %collective-permute-done.1.refs_1_, bf16[2,512,128]{2,1,0:T(8,128)(2,1)S(1)} %collective-permute-done.5.refs_2_, ...), custom_call_target="tpu_custom_call", output_to_operand_aliasing={{}: (3, {})} | custom-call | flops 2147483648 | bytes 1048576 | tf_op jit(solution)/shard_map/pallas_call | solution.py:142
  31.8 1.6 collective-permute-start.3
  34.1 4.2 %shard_map.122.refs_3_ = f32[80,2048]{1,0:T(8,128)S(1)} custom-call(bf16[128,2048]{1,0:T(8,128)(2,1)S(1)} %get-tuple-element.7.refs_0_, bf16[2,512,128]{2,1,0:T(8,128)(2,1)S(1)} %collective-permute-done.2.refs_1_, bf16[2,512,128]{2,1,0:T(8,128)(2,1)S(1)} %collective-permute-done.6.refs_2_, ...), custom_call_target="tpu_custom_call", output_to_operand_aliasing={{}: (3, {})} | custom-call | flops 2147483648 | bytes 1048576 | tf_op jit(solution)/shard_map/pallas_call | solution.py:142
  38.6 3.1 %shard_map.123 = bf16[4,256,128]{2,1,0:T(8,128)(2,1)} custom-call(bf16[128,2048]{1,0:T(8,128)(2,1)S(1)} %get-tuple-element.7.refs_0_, bf16[1,512,128]{2,1,0:T(8,128)(2,1)S(1)} %collective-permute-done.3.refs_1_, bf16[1,512,128]{2,1,0:T(8,128)(2,1)S(1)} %collective-permute-done.7.refs_2_, f32[80,2048]{1,0:T(8,128)S(1)} %shard_map.122.refs_3_), custom_call_target="tpu_custom_call" | custom-call | flops 1073741824 | bytes 524288 | tf_op jit(solution)/shard_map/pallas_call | solution.py:142
  41.7 3.4 %all-to-all-start = ((bf16[4,256,128]{2,1,0:T(8,128)(2,1)}), bf16[4,256,128]{2,1,0:T(8,128)(2,1)S(1)}, u32[]{:S(2)}, u32[]{:S(2)}) async-start(bf16[4,256,128]{2,1,0:T(8,128)(2,1)} %shard_map.123), calls=%async_computation | async-start | bytes 524288 | tf_op jit(solution)/shard_map/all_to_all | solution.py:210
  45.2 5.8 %all-to-all-done = bf16[4,256,128]{2,1,0:T(8,128)(2,1)S(1)} async-done(((bf16[4,256,128]{2,1,0:T(8,128)(2,1)}), bf16[4,256,128]{2,1,0:T(8,128)(2,1)S(1)}, u32[]{:S(2)}, u32[]{:S(2)}) %all-to-all-start) | async-done | bytes 262176 | tf_op jit(solution)/shard_map/all_to_all | solution.py:210
  51.1 3.1 %multiply_reduce_fusion = (f32[128]{0:T(128)S(1)}, f32[128,2048]{1,0:T(8,128)S(1)}) fusion(bf16[1024,128]{1,0:T(8,128)(2,1)S(1)} %bitcast.46, bf16[1024,2048]{1,0:T(8,128)(2,1)} %param.16), kind=kOutput, calls=%fused_computation.22 | convolution fusion | flops 537395072 | bytes 5505536 | tf_op jit(solution)/shard_map/dot_general | solution.py:212
  55.7 53.1 %all_to_all.15 = bf16[32,16,2048]{2,1,0:T(8,128)(2,1)S(1)} all-to-all(bf16[32,16,2048]{2,1,0:T(8,128)(2,1)S(1)} %bitcast.42), channel_id=1, replica_groups=mesh['sp'=8,'tp'=4] {'sp','tp'}, dimensions={0} | all-to-all | bytes 4194304 | tf_op jit(solution)/shard_map/all_to_all | solution.py:244
  108.8 3.7 %fusion.4 = f32[512,1024]{1,0:T(8,128)} fusion(bf16[512,2048]{1,0:T(8,128)(2,1)S(1)} %bitcast.44, bf16[1,2048,1024]{2,1,0:T(8,128)(2,1)S(1)} %copy-done.8), kind=kOutput, calls=%fused_computation.4 | convolution fusion | flops 2147483648 | bytes 8388608 | tf_op jit(solution)/shard_map/dot_general | solution.py:246
  112.5 10.0 %fusion.6 = bf16[512,2048]{1,0:T(8,128)(2,1)} fusion(bf16[1,1024,2048]{2,1,0:T(8,128)(2,1)} %param.23, f32[512,1024]{1,0:T(8,128)} %fusion.4, bf16[512,2048]{1,0:T(8,128)(2,1)S(1)} %bitcast.45, bf16[1,2048,1024]{2,1,0:T(8,128)(2,1)} %param.22), kind=kOutput, calls=%fused_computation.6 | convolution fusion | flops 4299161600 | bytes 14680064 | tf_op jit(solution)/shard_map/dot_general | solution.py:249
  122.5 3.7 %all-to-all-start.2 = ((bf16[32,16,2048]{2,1,0:T(8,128)(2,1)}), bf16[32,16,2048]{2,1,0:T(8,128)(2,1)S(1)}, u32[]{:S(2)}, u32[]{:S(2)}) async-start(bf16[32,16,2048]{2,1,0:T(8,128)(2,1)} %bitcast.43), calls=%async_computation.2 | async-start | bytes 4194304 | tf_op jit(solution)/shard_map/all_to_all | solution.py:251
  126.3 48.5 %all-to-all-done.2 = bf16[32,16,2048]{2,1,0:T(8,128)(2,1)S(1)} async-done(((bf16[32,16,2048]{2,1,0:T(8,128)(2,1)}), bf16[32,16,2048]{2,1,0:T(8,128)(2,1)S(1)}, u32[]{:S(2)}, u32[]{:S(2)}) %all-to-all-start.2) | async-done | bytes 2097184 | tf_op jit(solution)/shard_map/all_to_all | solution.py:251
  175.3 1.3 fusion.11
  (42 shorter events, 4.8 us)
Async XLA Ops:
  1.1 1.0 copy-start
  2.0 0.9 copy-start.1
  2.9 0.9 copy-start.2
  4.5 13.6 %copy-start.6 = (s32[128,2]{0,1:T(2,128)S(1)}, s32[128,2]{0,1:T(2,128)}, u32[]{:S(2)}) copy-start(s32[128,2]{0,1:T(2,128)} %param.19) | copy-start | bytes 3076
  4.5 9.3 %collective-permute-start = (bf16[2,512,128]{2,1,0:T(8,128)(2,1)S(1)}, bf16[2,512,128]{2,1,0:T(8,128)(2,1)S(1)}, u32[]{:S(2)}, u32[]{:S(2)}) collective-permute-start(bf16[2,512,128]{2,1,0:T(8,128)(2,1)S(1)} %get-tuple-element.8.refs_1_), channel_id=1, source_target_pairs={{0,8},{8,16},{16,24},{24,28},{28,20},{20,12},{12,4},{4,0},{1,9},{9... | collective-permute-start | bytes 786440 | tf_op jit(solution)/shard_map/ppermute | solution.py:204
  7.6 8.1 %collective-permute-start.4 = (bf16[2,512,128]{2,1,0:T(8,128)(2,1)S(1)}, bf16[2,512,128]{2,1,0:T(8,128)(2,1)S(1)}, u32[]{:S(2)}, u32[]{:S(2)}) collective-permute-start(bf16[2,512,128]{2,1,0:T(8,128)(2,1)S(1)} %get-tuple-element.8.refs_1_), channel_id=1, source_target_pairs={{8,0},{16,8},{24,16},{28,24},{20,28},{12,20},{4,12},{0,4},{9,1},{1... | collective-permute-start | bytes 786440 | tf_op jit(solution)/shard_map/ppermute | solution.py:205
  13.8 7.5 %collective-permute-start.1 = (bf16[2,512,128]{2,1,0:T(8,128)(2,1)S(1)}, bf16[2,512,128]{2,1,0:T(8,128)(2,1)S(1)}, u32[]{:S(2)}, u32[]{:S(2)}) collective-permute-start(bf16[2,512,128]{2,1,0:T(8,128)(2,1)S(1)} %collective-permute-done.refs_1_), channel_id=1, source_target_pairs={{0,8},{8,16},{16,24},{24,28},{28,20},{20,12},{12,4},{4,0},{1,9},{9... | collective-permute-start | bytes 786440 | tf_op jit(solution)/shard_map/ppermute | solution.py:204
  15.6 7.2 %collective-permute-start.5 = (bf16[2,512,128]{2,1,0:T(8,128)(2,1)S(1)}, bf16[2,512,128]{2,1,0:T(8,128)(2,1)S(1)}, u32[]{:S(2)}, u32[]{:S(2)}) collective-permute-start(bf16[2,512,128]{2,1,0:T(8,128)(2,1)S(1)} %collective-permute-done.4.refs_2_), channel_id=1, source_target_pairs={{8,0},{16,8},{24,16},{28,24},{20,28},{12,20},{4,12},{0,4},{9,1},{1... | collective-permute-start | bytes 786440 | tf_op jit(solution)/shard_map/ppermute | solution.py:205
  21.3 10.5 %collective-permute-start.2 = (bf16[2,512,128]{2,1,0:T(8,128)(2,1)S(1)}, bf16[2,512,128]{2,1,0:T(8,128)(2,1)S(1)}, u32[]{:S(2)}, u32[]{:S(2)}) collective-permute-start(bf16[2,512,128]{2,1,0:T(8,128)(2,1)S(1)} %collective-permute-done.1.refs_1_), channel_id=1, source_target_pairs={{0,8},{8,16},{16,24},{24,28},{28,20},{20,12},{12,4},{4,0},{1,9},{9... | collective-permute-start | bytes 786440 | tf_op jit(solution)/shard_map/ppermute | solution.py:204
  22.8 10.5 %collective-permute-start.6 = (bf16[2,512,128]{2,1,0:T(8,128)(2,1)S(1)}, bf16[2,512,128]{2,1,0:T(8,128)(2,1)S(1)}, u32[]{:S(2)}, u32[]{:S(2)}) collective-permute-start(bf16[2,512,128]{2,1,0:T(8,128)(2,1)S(1)} %collective-permute-done.5.refs_2_), channel_id=1, source_target_pairs={{8,0},{16,8},{24,16},{28,24},{20,28},{12,20},{4,12},{0,4},{9,1},{1... | collective-permute-start | bytes 786440 | tf_op jit(solution)/shard_map/ppermute | solution.py:205
  31.8 6.6 %collective-permute-start.3 = (bf16[1,512,128]{2,1,0:T(8,128)(2,1)S(1)}, bf16[1,512,128]{2,1,0:T(8,128)(2,1)S(1)}, u32[]{:S(2)}, u32[]{:S(2)}) collective-permute-start(bf16[1,512,128]{2,1,0:T(8,128)(2,1)S(1)} %slice.26), channel_id=1, source_target_pairs={{0,8},{8,16},{16,24},{24,28},{28,20},{20,12},{12,4},{4,0},{1,9},{9... | collective-permute-start | bytes 393224 | tf_op jit(solution)/shard_map/ppermute | solution.py:204
  33.4 5.2 %collective-permute-start.7 = (bf16[1,512,128]{2,1,0:T(8,128)(2,1)S(1)}, bf16[1,512,128]{2,1,0:T(8,128)(2,1)S(1)}, u32[]{:S(2)}, u32[]{:S(2)}) collective-permute-start(bf16[1,512,128]{2,1,0:T(8,128)(2,1)S(1)} %slice.27), channel_id=1, source_target_pairs={{8,0},{16,8},{24,16},{28,24},{20,28},{12,20},{4,12},{0,4},{9,1},{1... | collective-permute-start | bytes 393224 | tf_op jit(solution)/shard_map/ppermute | solution.py:205
  41.7 9.4 %all-to-all-start = ((bf16[4,256,128]{2,1,0:T(8,128)(2,1)}), bf16[4,256,128]{2,1,0:T(8,128)(2,1)S(1)}, u32[]{:S(2)}, u32[]{:S(2)}) async-start(bf16[4,256,128]{2,1,0:T(8,128)(2,1)} %shard_map.123), calls=%async_computation | async-start | bytes 524288 | tf_op jit(solution)/shard_map/all_to_all | solution.py:210
  51.1 3.1 %copy-start.3 = (bf16[128,2048]{1,0:T(8,128)(2,1)S(1)}, bf16[128,2048]{1,0:T(8,128)(2,1)}, u32[]{:S(2)}) copy-start(bf16[128,2048]{1,0:T(8,128)(2,1)} %param.15) | copy-start | bytes 1572868
  51.1 3.1 %copy-start.4 = (f32[2048]{0:T(1024)S(1)}, f32[2048]{0:T(1024)}, u32[]{:S(2)}) copy-start(f32[2048]{0:T(1024)} %param.17) | copy-start | bytes 24580
  54.2 0.7 copy-start.5
  55.7 53.1 %copy-start.8 = (bf16[1,2048,1024]{2,1,0:T(8,128)(2,1)S(1)}, bf16[1,2048,1024]{2,1,0:T(8,128)(2,1)}, u32[]{:S(2)}) copy-start(bf16[1,2048,1024]{2,1,0:T(8,128)(2,1)} %param.21) | copy-start | bytes 12582916
  122.5 3.7 %copy-start.7 = (f32[128,2]{0,1:T(2,128)S(1)}, f32[128,2]{0,1:T(2,128)}, u32[]{:S(2)}) copy-start(f32[128,2]{0,1:T(2,128)} %param.20) | copy-start | bytes 3076
  122.5 52.4 %all-to-all-start.2 = ((bf16[32,16,2048]{2,1,0:T(8,128)(2,1)}), bf16[32,16,2048]{2,1,0:T(8,128)(2,1)S(1)}, u32[]{:S(2)}, u32[]{:S(2)}) async-start(bf16[32,16,2048]{2,1,0:T(8,128)(2,1)} %bitcast.43), calls=%async_computation.2 | async-start | bytes 4194304 | tf_op jit(solution)/shard_map/all_to_all | solution.py:251

commit v2 on v1

v2 whole, which is shorter than its diff:
```python
import functools
import math

import jax
import jax.numpy as jnp
from jax import lax
from jax.experimental import pallas as pl
from jax.experimental.pallas import tpu as pltpu
from jax.sharding import PartitionSpec as P

HEAD_SIZE = 64
GRID_W = 64
HALF_KEYS = 256
ONES_ROWS = 16

epsilon = 1e-06
base_theta = 10000.0

VMEM = pl.BlockSpec(memory_space=pltpu.VMEM)
ANY = pl.BlockSpec(memory_space=pl.ANY)


def rotation_tables(first_row, row_count, lanes):
    quarter = HEAD_SIZE // 4
    lane = jnp.arange(lanes, dtype=jnp.int32) % HEAD_SIZE
    index = jnp.arange(row_count + GRID_W, dtype=jnp.int32)
    place = jnp.where(index < row_count, first_row + index, index - row_count)
    frequency = base_theta ** (-(lane % quarter).astype(jnp.float32) / quarter)
    angle = place.astype(jnp.float32)[:, None] * frequency[None, :]
    sign = jnp.where((lane // quarter) % 2 == 0, -1.0, 1.0).astype(jnp.float32)
    return jnp.cos(angle), jnp.sin(angle) * sign[None, :]


def prepare_kernel(q_hbm, k_hbm, v_hbm, cos_ref, sin_ref, q_out, kv_out, q_ref, k_ref, v_ref, sems):
    copies = [
        pltpu.make_async_copy(src, dst, sems.at[i])
        for i, (src, dst) in enumerate(((k_hbm, k_ref), (v_hbm, v_ref), (q_hbm, q_ref)))
    ]
    for copy in copies:
        copy.start()
    tok_count, lanes = k_ref.shape
    grid_rows = tok_count // GRID_W
    rows = lax.broadcasted_iota(jnp.int32, (lanes, lanes), 0)
    cols = lax.broadcasted_iota(jnp.int32, (lanes, lanes), 1)
    same_head = (rows // HEAD_SIZE) == (cols // HEAD_SIZE)
    mean_mat = jnp.where(same_head, 1.0 / HEAD_SIZE, 0.0).astype(jnp.bfloat16)
    swap_mat = jnp.where((rows ^ (HEAD_SIZE // 4)) == cols, 1.0, 0.0).astype(jnp.bfloat16)
    lane = lax.broadcasted_iota(jnp.int32, (grid_rows, GRID_W, lanes), 2)
    by_row = (lane % HEAD_SIZE) < HEAD_SIZE // 2

    def table(ref):
        row_part = ref[:grid_rows, :][:, None, :]
        col_part = ref[grid_rows:, :][None, :, :]
        return jnp.where(by_row, row_part, col_part).reshape(tok_count, lanes)

    cos, sin = table(cos_ref), table(sin_ref)

    def ready(raw, factor):
        wide = raw.astype(jnp.float32)
        square = wide * wide
        high = square.astype(jnp.bfloat16)
        low = (square - high.astype(jnp.float32)).astype(jnp.bfloat16)
        mean = jnp.dot(high, mean_mat, preferred_element_type=jnp.float32) + jnp.dot(
            low, mean_mat, preferred_element_type=jnp.float32
        )
        swapped = jnp.dot(raw, swap_mat, preferred_element_type=jnp.float32)
        length = lax.rsqrt(mean + epsilon) * factor
        return (wide * cos + swapped * sin) * length

    for copy in copies:
        copy.wait()
    keys = ready(k_ref[...], 1.0).astype(jnp.bfloat16)
    for half in range(tok_count // HALF_KEYS):
        begin = half * HALF_KEYS
        kv_out[half, :HALF_KEYS, :] = keys[begin : begin + HALF_KEYS]
        for part in range(HALF_KEYS // lanes):
            start = begin + part * lanes
            at = HALF_KEYS + part * lanes
            kv_out[half, at : at + lanes, :] = (
                v_ref[start : start + lanes, :].astype(jnp.float32).T.astype(jnp.bfloat16)
            )
    factor = math.log2(math.e) * HEAD_SIZE ** (-0.5)
    group = q_ref.shape[1] // lanes
    q_out[...] = jnp.zeros_like(q_out)
    for block in range(group):
        turned = ready(q_ref[:, block * lanes : (block + 1) * lanes], factor).T
        for inner in range(lanes // HEAD_SIZE):
            head = block * (lanes // HEAD_SIZE) + inner
            kv_head = head // group
            q_out[
                kv_head * HEAD_SIZE : (kv_head + 1) * HEAD_SIZE,
                head * tok_count : (head + 1) * tok_count,
            ] = turned[inner * HEAD_SIZE : (inner + 1) * HEAD_SIZE].astype(jnp.bfloat16)


def attend_kernel(chunk_count, first, last, *refs):
    q_ref = refs[0]
    chunks = refs[1 : 1 + chunk_count]
    acc_in = None if first else refs[1 + chunk_count]
    out_refs = refs[1 + chunk_count + (0 if first else 1) :]
    lanes, columns = q_ref.shape
    width = min(512, columns)
    blocks = columns // width
    kv_heads = lanes // HEAD_SIZE
    halves = [(c, i) for c in chunks for i in range(c.shape[0])]
    ones = jnp.ones((ONES_ROWS, HALF_KEYS), jnp.bfloat16)
    waiting = None
    for block in range(blocks + 1):
        weights = []
        total = None
        for index, (chunk, half) in enumerate(halves):
            if block < blocks:
                scores = jnp.dot(
                    chunk[half, :HALF_KEYS, :],
                    q_ref[:, block * width : (block + 1) * width],
                    preferred_element_type=jnp.float32,
                )
                weights.append(jnp.exp2(scores).astype(jnp.bfloat16))
            if waiting is not None:
                kv_head = (block - 1) * kv_heads // blocks
                values = jnp.concatenate(
                    [
                        chunk[
                            half,
                            pl.ds(HALF_KEYS + part * lanes + kv_head * HEAD_SIZE, HEAD_SIZE),
                            :,
                        ]
                        for part in range(HALF_KEYS // lanes)
                    ],
                    axis=1,
                )
                values = jnp.concatenate([values, ones], axis=0)
                piece = jnp.dot(values, waiting[index], preferred_element_type=jnp.float32)
                total = piece if total is None else total + piece
        if waiting is not None:
            at = (block - 1) * width
            if not first:
                total = total + acc_in[:, at : at + width]
            if not last:
                out_refs[0][:, at : at + width] = total
            else:
                turn = out_refs[-1]
                tp, head_rows, per = turn.shape
                tok_count = tp * per
                ready = (total[:HEAD_SIZE] / total[HEAD_SIZE : HEAD_SIZE + 1]).astype(jnp.bfloat16)
                for piece in range(width // per):
                    head, place = divmod(at + piece * per, tok_count)
                    turn[place // per, head * HEAD_SIZE : (head + 1) * HEAD_SIZE, :] = ready[
                        :, piece * per : (piece + 1) * per
                    ]
        waiting = weights
    if last:
        me = lax.axis_index("tp")
        turn = out_refs[-1]
        rel = 0
        for out in out_refs[:-1]:
            for j in range(out.shape[0]):
                out[j] = turn[me ^ rel]
                rel += 1


def attend(q_ready, chunks, acc, tp_size=None):
    first, last = acc is None, tp_size is not None
    lanes, columns = q_ready.shape
    rows = HEAD_SIZE + ONES_ROWS
    key_count = sum(c.shape[0] for c in chunks) * HALF_KEYS
    scratch = []
    if last:
        tok_count = chunks[0].shape[0] * HALF_KEYS * 2
        head_rows = columns // tok_count * HEAD_SIZE
        block = (head_rows, tok_count // tp_size)
        sizes = [1] + [1 << b for b in range(tp_size.bit_length() - 1)]
        shape = [jax.ShapeDtypeStruct((n, *block), jnp.bfloat16) for n in sizes]
        scratch = [pltpu.VMEM((tp_size, *block), jnp.bfloat16)]
    else:
        shape = [jax.ShapeDtypeStruct((rows, columns), jnp.float32)]
    operands = [q_ready, *chunks] + ([] if first else [acc])
    aliases = {} if (first or last) else {len(operands) - 1: 0}
    out = pl.pallas_call(
        functools.partial(attend_kernel, len(chunks), first, last),
        out_shape=shape,
        in_specs=[VMEM] * len(operands),
        out_specs=[VMEM] * len(shape),
        scratch_shapes=scratch,
        input_output_aliases=aliases,
        cost_estimate=pl.CostEstimate(
            flops=2 * key_count * columns * 512,
            bytes_accessed=key_count * 1024,
            transcendentals=key_count * columns,
        ),
        compiler_params=pltpu.CompilerParams(vmem_limit_bytes=24 * 1024 * 1024),
    )(*operands)
    return out if last else out[0]


def hypercube_exchange(pieces, tp_size):
    held = []
    for bit in reversed(range(tp_size.bit_length() - 1)):
        pairs = [(i, i ^ (1 << bit)) for i in range(tp_size)]
        half = 1 << bit
        moved = [(half, lax.ppermute(pieces[1 + bit], "tp", pairs))]
        kept = []
        for source, block in held:
            moved.append((source ^ half, lax.ppermute(block[half:], "tp", pairs)))
            kept.append((source, block[:half]))
        held = kept + moved
    return [pieces[0]] + [block for _, block in sorted(held, key=lambda item: item[0])]


def out_kernel(tp_size, *refs):
    blocks = refs[:tp_size]
    w_ref, res_ref, mix_ref, norm_ref, target_ref = refs[tp_size : tp_size + 5]
    stream_ref, out_ref, mixed_ref, normed_ref = refs[tp_size + 5 :]
    me = lax.axis_index("tp")
    _, head_rows, row_count = blocks[0].shape
    width = w_ref.shape[1]
    step = min(512, width)
    turned = [b[0].astype(jnp.float32).T.astype(jnp.bfloat16) for b in blocks]
    power = jnp.zeros((row_count, 1), jnp.float32)
    for at in range(0, width, step):
        mixed = jnp.zeros((row_count, step), jnp.float32)
        for rel in range(tp_size):
            begin = pl.multiple_of((me ^ rel) * head_rows, head_rows)
            mixed = mixed + jnp.dot(
                turned[rel],
                w_ref[pl.ds(begin, head_rows), at : at + step],
                preferred_element_type=jnp.float32,
            )
        mixed_ref[:, at : at + step] = mixed
        power = power + jnp.sum(mixed * mixed, axis=1, keepdims=True)
    scale = lax.rsqrt(power / width + epsilon)
    power = jnp.zeros((row_count, 1), jnp.float32)
    for at in range(0, width, step):
        cols = slice(at, at + step)
        stream = (
            res_ref[:, cols].astype(jnp.float32) + mixed_ref[:, cols] * scale * mix_ref[:, cols]
        ).astype(jnp.bfloat16)
        stream_ref[:, cols] = stream
        wide = stream.astype(jnp.float32)
        power = power + jnp.sum(wide * wide, axis=1, keepdims=True)
    scale = lax.rsqrt(power / width + epsilon)
    for at in range(0, width, step):
        cols = slice(at, at + step)
        wide = stream_ref[:, cols].astype(jnp.float32)
        normed_ref[:, cols] = (wide * scale * norm_ref[:, cols]).astype(jnp.bfloat16)
    slots = lax.broadcasted_iota(jnp.int32, (out_ref.shape[0], row_count), 0)
    hit = slots == target_ref[0:1, :]
    for k in range(1, target_ref.shape[0]):
        hit = hit | (slots == target_ref[k : k + 1, :])
    placing = jnp.where(hit, 1.0, 0.0).astype(jnp.bfloat16)
    for at in range(0, width, step):
        cols = slice(at, at + step)
        out_ref[:, cols] = jnp.dot(
            placing, normed_ref[:, cols], preferred_element_type=jnp.float32
        ).astype(jnp.bfloat16)


def expert_kernel(rows_ref, gate_ref, up_ref, down_ref, out_ref, act_ref):
    hidden = gate_ref.shape[1]
    width = down_ref.shape[1]
    step = min(256, hidden)
    for at in range(0, hidden, step):
        cols = slice(at, at + step)
        gate = jnp.dot(rows_ref[...], gate_ref[:, cols], preferred_element_type=jnp.float32)
        up = jnp.dot(rows_ref[...], up_ref[:, cols], preferred_element_type=jnp.float32)
        act_ref[:, cols] = (gate / (1.0 + jnp.exp(-gate)) * up).astype(jnp.bfloat16)
    step = min(512, width)
    for at in range(0, width, step):
        cols = slice(at, at + step)
        out_ref[:, cols] = jnp.dot(
            act_ref[...], down_ref[:, cols], preferred_element_type=jnp.float32
        ).astype(jnp.bfloat16)


def local(
    sp_size,
    tp_size,
    query_proj,
    projected_keys,
    projected_values,
    residual,
    out_weight,
    mix_gain,
    norm_gain,
    route_expert,
    route_weight,
    expert_gate,
    expert_up,
    expert_down,
):
    tok_count, lanes = projected_keys.shape
    q_heads = query_proj.shape[1] // HEAD_SIZE
    model_width = residual.shape[1]
    grid_rows = tok_count // GRID_W
    cos_table, sin_table = rotation_tables(lax.axis_index("sp") * grid_rows, grid_rows, lanes)
    q_ready, kv_own = pl.pallas_call(
        prepare_kernel,
        out_shape=(
            jax.ShapeDtypeStruct((lanes, q_heads * tok_count), jnp.bfloat16),
            jax.ShapeDtypeStruct((tok_count // HALF_KEYS, 2 * HALF_KEYS, lanes), jnp.bfloat16),
        ),
        in_specs=[ANY] * 3 + [VMEM] * 2,
        out_specs=(VMEM, VMEM),
        scratch_shapes=[
            pltpu.VMEM(query_proj.shape, jnp.bfloat16),
            pltpu.VMEM(projected_keys.shape, jnp.bfloat16),
            pltpu.VMEM(projected_values.shape, jnp.bfloat16),
            pltpu.SemaphoreType.DMA((3,)),
        ],
        cost_estimate=pl.CostEstimate(
            flops=2 * tok_count * 512 * 512, bytes_accessed=1 << 20, transcendentals=0
        ),
        compiler_params=pltpu.CompilerParams(vmem_limit_bytes=32 * 1024 * 1024),
    )(query_proj, projected_keys, projected_values, cos_table, sin_table)

    order = list(range(0, sp_size, 2)) + list(range(sp_size - 1, 0, -2))
    ahead = [(order[i], order[(i + 1) % sp_size]) for i in range(sp_size)]
    behind = [(b, a) for a, b in ahead]
    steps = sp_size // 2
    acc = None
    from_left = from_right = kv_own
    held = [kv_own]
    for step in range(steps):
        if step == steps - 1:
            halves = kv_own.shape[0]
            from_left, from_right = from_left[: halves // 2], from_right[halves // 2 :]
        next_left = lax.ppermute(from_left, "sp", ahead)
        next_right = lax.ppermute(from_right, "sp", behind)
        acc = attend(q_ready, held, acc)
        from_left, from_right = next_left, next_right
        held = [from_left, from_right]
    pieces = attend(q_ready, held, acc, tp_size)
    blocks = hypercube_exchange(pieces, tp_size)

    row_count = residual.shape[0]
    top_count = route_expert.shape[1]
    experts = sp_size * tp_size
    capacity = max(2, 2 * top_count * row_count // experts)
    slots_total = experts * capacity
    flat_expert = route_expert.T.reshape(-1)
    onehot = flat_expert[:, None] == jnp.arange(experts, dtype=jnp.int32)[None, :]
    pairs = flat_expert.shape[0]
    before = (
        jnp.arange(pairs, dtype=jnp.int32)[None, :] < jnp.arange(pairs, dtype=jnp.int32)[:, None]
    ).astype(jnp.bfloat16)
    earlier = jnp.dot(before, onehot.astype(jnp.bfloat16), preferred_element_type=jnp.float32)
    slot_rank = jnp.sum(jnp.where(onehot, earlier, 0.0), axis=1).astype(jnp.int32)
    target = (flat_expert * capacity + slot_rank).reshape(top_count, row_count)

    stream, outgoing = pl.pallas_call(
        functools.partial(out_kernel, tp_size),
        out_shape=(
            jax.ShapeDtypeStruct((row_count, model_width), jnp.bfloat16),
            jax.ShapeDtypeStruct((slots_total, model_width), jnp.bfloat16),
        ),
        in_specs=[VMEM] * (tp_size + 5),
        out_specs=(VMEM, VMEM),
        scratch_shapes=[
            pltpu.VMEM((row_count, model_width), jnp.float32),
            pltpu.VMEM((row_count, model_width), jnp.bfloat16),
        ],
        cost_estimate=pl.CostEstimate(
            flops=2 * row_count * model_width * (out_weight.shape[0] + slots_total),
            bytes_accessed=8 << 20,
            transcendentals=0,
        ),
        compiler_params=pltpu.CompilerParams(vmem_limit_bytes=12 * 1024 * 1024),
    )(*blocks, out_weight, residual, mix_gain[None, :], norm_gain[None, :], target)

    outgoing = outgoing.reshape(experts, capacity, model_width)
    slots = lax.all_to_all(outgoing, ("sp", "tp"), split_axis=0, concat_axis=0, tiled=True)
    flat_rows = slots.reshape(-1, model_width)
    hidden = expert_gate.shape[2]
    done = pl.pallas_call(
        expert_kernel,
        out_shape=jax.ShapeDtypeStruct(flat_rows.shape, jnp.bfloat16),
        in_specs=[VMEM] * 4,
        out_specs=VMEM,
        scratch_shapes=[pltpu.VMEM((flat_rows.shape[0], hidden), jnp.bfloat16)],
        cost_estimate=pl.CostEstimate(
            flops=6 * flat_rows.shape[0] * model_width * hidden,
            bytes_accessed=16 << 20,
            transcendentals=flat_rows.shape[0] * hidden,
        ),
        compiler_params=pltpu.CompilerParams(vmem_limit_bytes=24 * 1024 * 1024),
    )(flat_rows, expert_gate[0], expert_up[0], expert_down[0])
    answered = done.reshape(slots.shape)
    returned = lax.all_to_all(answered, ("sp", "tp"), split_axis=0, concat_axis=0, tiled=True)
    returned = returned.reshape(slots_total, model_width)
    chosen = target[:, :, None] == jnp.arange(slots_total, dtype=jnp.int32)[None, None, :]
    combined = stream.astype(jnp.float32)
    for k in range(top_count):
        picked = jnp.dot(
            chosen[k].astype(jnp.bfloat16), returned, preferred_element_type=jnp.float32
        )
        combined = combined + picked * route_weight[:, k : k + 1]
    return combined.astype(jnp.bfloat16)


def solution(mesh):
    return jax.shard_map(
        functools.partial(local, mesh.shape["sp"], mesh.shape["tp"]),
        mesh=mesh,
        in_specs=(
            P("sp", "tp"),
            P("sp", "tp"),
            P("sp", "tp"),
            P(("sp", "tp"), None),
            P(),
            P(),
            P(),
            P(("sp", "tp"), None),
            P(("sp", "tp"), None),
            P(("sp", "tp"), None, None),
            P(("sp", "tp"), None, None),
            P(("sp", "tp"), None, None),
        ),
        out_specs=P(("sp", "tp"), None),
        check_vma=False,
    )
```

time: 177 us -> 160 us (0.904)
  matrix products: 19.6 us -> 1.14 us
  waiting for transfers between devices: 63.9 us -> 67.1 us
  starting transfers between devices: 16.5 us -> 14.7 us
    dot_general x5 -> x1, matrix products: 17.8 us -> 0.2 us  [local(): jnp.dot(before, onehot.astype(jnp.bfloat16), preferred_element_type=jnp.f...]
    pallas_call x5, Pallas kernels: 18 us -> 7.71 us  [attend(): pl.pallas_call(functools.partial(attend_kernel, len(chunks), first, last)...]
    pallas_call x0 -> x2, Pallas kernels: none -> 9.9 us  [the longest x1 8.03 us: local(): pl.pallas_call(expert_kernel, out_shape=jax.ShapeDtypeStruct(flat_rows.sh...]
    all_to_all x1 -> x0, waiting for transfers between devices: 5.84 us -> none  [local(): lax.all_to_all(attended, 'tp', split_axis=0, concat_axis=0, tiled=True)]
    ppermute x0 -> x3, waiting for transfers between devices: none -> 4.38 us  [the longest x2 3.16 us: hypercube_exchange(): moved = [(half, lax.ppermute(pieces[1 + bit], 'tp', pairs))]]
    all_to_all x1 -> x0, starting transfers between devices: 3.41 us -> none  [local(): lax.all_to_all(attended, 'tp', split_axis=0, concat_axis=0, tiled=True)]
    ppermute x4, waiting for transfers between devices: 9.24 us -> 12.4 us  [local(): next_left = lax.ppermute(from_left, 'sp', ahead)]
  transfers between devices with their start and end apart: 10 -> 12, of which waited for: 5 -> 8; matrix products, arithmetic and copies ran while one was open for 0% -> 0% of each run, Pallas kernels for 8% -> 4%
where the time goes in v2:
time: 160 us; the launch traced here: 159 us
  waiting for transfers between devices  67.1 us (42%)
  blocking collectives  53.3 us (33%)
  Pallas kernels  18.6 us (12%)
  starting transfers between devices  14.7 us (9%)
  local copies, waits for them, and re-layouts  2.83 us (2%)
    all_to_all x1, blocking collectives, local(): lax.all_to_all(outgoing, ('sp', 'tp'), split_axis=0, concat_axis=0, tiled...  53.3 us
    all_to_all x1, waiting for transfers between devices, local(): lax.all_to_all(answered, ('sp', 'tp'), split_axis=0, concat_axis=0, tiled...  48.5 us
    ppermute x4, waiting for transfers between devices, local(): next_left = lax.ppermute(from_left, 'sp', ahead)  12.4 us
    ppermute x4, starting transfers between devices, local(): next_left = lax.ppermute(from_left, 'sp', ahead)  8.19 us
    pallas_call x1, Pallas kernels, local(): pl.pallas_call(expert_kernel, out_shape=jax.ShapeDtypeStruct(flat_rows.sh...  8.03 us
    pallas_call x5, Pallas kernels, attend(): pl.pallas_call(functools.partial(attend_kernel, len(chunks), first, last)...  7.71 us
    all_to_all x1, starting transfers between devices, local(): lax.all_to_all(answered, ('sp', 'tp'), split_axis=0, concat_axis=0, tiled...  3.67 us
  transfers between devices with their start and end apart: 12, of which 8 were waited for; matrix products, arithmetic and copies ran while one was open for 0% of the time, Pallas kernels for 4%

profile of v2, /device:TPU:0, one launch (start us, length us, event | category | flops | bytes accessed | tf_op | source)
XLA Modules:
  0.0 159.3 jit_solution(555725357809806948)
XLA Ops:
  0.3 0.9 copy-done.7
  3.0 1.0 shard_map.118
  4.0 3.1 %collective-permute-start = (bf16[2,512,128]{2,1,0:T(8,128)(2,1)S(1)}, bf16[2,512,128]{2,1,0:T(8,128)(2,1)S(1)}, u32[]{:S(2)}, u32[]{:S(2)}) collective-permute-start(bf16[2,512,128]{2,1,0:T(8,128)(2,1)S(1)} %get-tuple-element.13.refs_1_), channel_id=1, source_target_pairs={{0,8},{8,16},{16,24},{24,28},{28,20},{20,12},{12,4},{4,0},{1,9},{9... | collective-permute-start | bytes 786440 | tf_op jit(solution)/shard_map/ppermute | solution.py:327
  7.1 6.2 %collective-permute-done.refs_1_ = bf16[2,512,128]{2,1,0:T(8,128)(2,1)S(1)} collective-permute-done((bf16[2,512,128]{2,1,0:T(8,128)(2,1)S(1)}, bf16[2,512,128]{2,1,0:T(8,128)(2,1)S(1)}, u32[]{:S(2)}, u32[]{:S(2)}) %collective-permute-start) | collective-permute-done | bytes 262176 | tf_op jit(solution)/shard_map/ppermute | solution.py:327
  13.4 1.8 %collective-permute-start.1 = (bf16[2,512,128]{2,1,0:T(8,128)(2,1)S(1)}, bf16[2,512,128]{2,1,0:T(8,128)(2,1)S(1)}, u32[]{:S(2)}, u32[]{:S(2)}) collective-permute-start(bf16[2,512,128]{2,1,0:T(8,128)(2,1)S(1)} %collective-permute-done.refs_1_), channel_id=1, source_target_pairs={{0,8},{8,16},{16,24},{24,28},{28,20},{20,12},{12,4},{4,0},{1,9},{9... | collective-permute-start | bytes 786440 | tf_op jit(solution)/shard_map/ppermute | solution.py:327
  15.4 1.1 shard_map.119.refs_3_
  16.4 4.4 %collective-permute-done.1.refs_1_ = bf16[2,512,128]{2,1,0:T(8,128)(2,1)S(1)} collective-permute-done((bf16[2,512,128]{2,1,0:T(8,128)(2,1)S(1)}, bf16[2,512,128]{2,1,0:T(8,128)(2,1)S(1)}, u32[]{:S(2)}, u32[]{:S(2)}) %collective-permute-start.1) | collective-permute-done | bytes 262176 | tf_op jit(solution)/shard_map/ppermute | solution.py:327
  20.8 1.5 collective-permute-start.2
  22.9 1.9 %shard_map.120.refs_3_ = f32[80,2048]{1,0:T(8,128)S(1)} custom-call(bf16[128,2048]{1,0:T(8,128)(2,1)S(1)} %get-tuple-element.12.refs_0_, bf16[2,512,128]{2,1,0:T(8,128)(2,1)S(1)} %collective-permute-done.refs_1_, bf16[2,512,128]{2,1,0:T(8,128)(2,1)S(1)} %collective-permute-done.4.refs_2_, ...), custom_call_target="tpu_custom_call", output_to_operand_aliasing={{}: (3, {})} | custom-call | flops 2147483648 | bytes 1048576 | tf_op jit(solution)/shard_map/pallas_call | solution.py:179
  24.7 1.9 %shard_map.121.refs_3_ = f32[80,2048]{1,0:T(8,128)S(1)} custom-call(bf16[128,2048]{1,0:T(8,128)(2,1)S(1)} %get-tuple-element.12.refs_0_, bf16[2,512,128]{2,1,0:T(8,128)(2,1)S(1)} %collective-permute-done.1.refs_1_, bf16[2,512,128]{2,1,0:T(8,128)(2,1)S(1)} %collective-permute-done.5.refs_2_, ...), custom_call_target="tpu_custom_call", output_to_operand_aliasing={{}: (3, {})} | custom-call | flops 2147483648 | bytes 1048576 | tf_op jit(solution)/shard_map/pallas_call | solution.py:179
  27.5 1.7 %collective-permute-start.3 = (bf16[1,512,128]{2,1,0:T(8,128)(2,1)S(1)}, bf16[1,512,128]{2,1,0:T(8,128)(2,1)S(1)}, u32[]{:S(2)}, u32[]{:S(2)}) collective-permute-start(bf16[1,512,128]{2,1,0:T(8,128)(2,1)S(1)} %slice.32), channel_id=1, source_target_pairs={{0,8},{8,16},{16,24},{24,28},{28,20},{20,12},{12,4},{4,0},{1,9},{9... | collective-permute-start | bytes 393224 | tf_op jit(solution)/shard_map/ppermute | solution.py:327
  29.6 1.9 %shard_map.122.refs_3_ = f32[80,2048]{1,0:T(8,128)S(1)} custom-call(bf16[128,2048]{1,0:T(8,128)(2,1)S(1)} %get-tuple-element.12.refs_0_, bf16[2,512,128]{2,1,0:T(8,128)(2,1)S(1)} %collective-permute-done.2.refs_1_, bf16[2,512,128]{2,1,0:T(8,128)(2,1)S(1)} %collective-permute-done.6.refs_2_, ...), custom_call_target="tpu_custom_call", output_to_operand_aliasing={{}: (3, {})} | custom-call | flops 2147483648 | bytes 1048576 | tf_op jit(solution)/shard_map/pallas_call | solution.py:179
  31.5 1.0 collective-permute-done.3.refs_1_
  32.5 1.7 %collective-permute-done.7.refs_2_ = bf16[1,512,128]{2,1,0:T(8,128)(2,1)S(1)} collective-permute-done((bf16[1,512,128]{2,1,0:T(8,128)(2,1)S(1)}, bf16[1,512,128]{2,1,0:T(8,128)(2,1)S(1)}, u32[]{:S(2)}, u32[]{:S(2)}) %collective-permute-start.7) | collective-permute-done | bytes 131104 | tf_op jit(solution)/shard_map/ppermute | solution.py:328
  34.2 1.1 shard_map.123
  35.3 1.6 collective-permute-start.9
  37.2 3.2 %collective-permute-done.9 = bf16[2,256,128]{2,1,0:T(8,128)(2,1)S(1)} collective-permute-done((bf16[2,256,128]{2,1,0:T(8,128)(2,1)S(1)}, bf16[2,256,128]{2,1,0:T(8,128)(2,1)S(1)}, u32[]{:S(2)}, u32[]{:S(2)}) %collective-permute-start.9) | collective-permute-done | bytes 131104 | tf_op jit(solution)/shard_map/ppermute | solution.py:201
  40.5 1.2 collective-permute-done.10.refs_3_
  41.7 1.9 %shard_map.124 = (bf16[128,2048]{1,0:T(8,128)(2,1)S(1)}, bf16[512,2048]{1,0:T(8,128)(2,1)S(1)}) custom-call(bf16[1,256,128]{2,1,0:T(8,128)(2,1)S(1)} %get-tuple-element.14.refs_0_, bf16[1,256,128]{2,1,0:T(8,128)(2,1)S(1)} %collective-permute-done.8.refs_1_, bf16[1,256,128]{2,1,0:T(8,128)(2,1)S(1)} %get-tuple-element.20.refs_2_, ...), custom_call_target="tpu_custom_call" | custom-call | flops 805306368 | bytes 8388608 | tf_op jit(solution)/shard_map/pallas_call | solution.py:350
  43.6 53.3 %all_to_all.10 = bf16[32,16,2048]{2,1,0:T(8,128)(2,1)S(1)} all-to-all(bf16[32,16,2048]{2,1,0:T(8,128)(2,1)S(1)} %bitcast.29), channel_id=1, replica_groups=mesh['sp'=8,'tp'=4] {'sp','tp'}, dimensions={0} | all-to-all | bytes 4194304 | tf_op jit(solution)/shard_map/all_to_all | solution.py:371
  96.9 8.0 %shard_map.125 = bf16[512,2048]{1,0:T(8,128)(2,1)} custom-call(bf16[512,2048]{1,0:T(8,128)(2,1)S(1)} %bitcast.30, bf16[2048,1024]{1,0:T(8,128)(2,1)S(1)} %bitcast.33, bf16[2048,1024]{1,0:T(8,128)(2,1)S(1)} %bitcast.34, bf16[1024,2048]{1,0:T(8,128)(2,1)S(1)} %bitcast.35), custom_call_target="tpu_custom_call" | custom-call | flops 6442450944 | bytes 16777216 | tf_op jit(solution)/shard_map/pallas_call | solution.py:374
  105.0 3.7 %all-to-all-start.1 = ((bf16[32,16,2048]{2,1,0:T(8,128)(2,1)}), bf16[32,16,2048]{2,1,0:T(8,128)(2,1)S(1)}, u32[]{:S(2)}, u32[]{:S(2)}) async-start(bf16[32,16,2048]{2,1,0:T(8,128)(2,1)} %bitcast.11), calls=%async_computation.1 | async-start | bytes 4194304 | tf_op jit(solution)/shard_map/all_to_all | solution.py:388
  108.8 48.5 %all-to-all-done.1 = bf16[32,16,2048]{2,1,0:T(8,128)(2,1)S(1)} async-done(((bf16[32,16,2048]{2,1,0:T(8,128)(2,1)}), bf16[32,16,2048]{2,1,0:T(8,128)(2,1)S(1)}, u32[]{:S(2)}, u32[]{:S(2)}) %all-to-all-start.1) | async-done | bytes 2097184 | tf_op jit(solution)/shard_map/all_to_all | solution.py:388
  158.3 1.0 add_convert_fusion
  (46 shorter events, 5.5 us)
Async XLA Ops:
  0.2 1.0 copy-start.7
  1.2 0.9 copy-start.8
  2.1 0.9 copy-start.9
  4.0 9.3 %collective-permute-start = (bf16[2,512,128]{2,1,0:T(8,128)(2,1)S(1)}, bf16[2,512,128]{2,1,0:T(8,128)(2,1)S(1)}, u32[]{:S(2)}, u32[]{:S(2)}) collective-permute-start(bf16[2,512,128]{2,1,0:T(8,128)(2,1)S(1)} %get-tuple-element.13.refs_1_), channel_id=1, source_target_pairs={{0,8},{8,16},{16,24},{24,28},{28,20},{20,12},{12,4},{4,0},{1,9},{9... | collective-permute-start | bytes 786440 | tf_op jit(solution)/shard_map/ppermute | solution.py:327
  7.1 8.0 %collective-permute-start.4 = (bf16[2,512,128]{2,1,0:T(8,128)(2,1)S(1)}, bf16[2,512,128]{2,1,0:T(8,128)(2,1)S(1)}, u32[]{:S(2)}, u32[]{:S(2)}) collective-permute-start(bf16[2,512,128]{2,1,0:T(8,128)(2,1)S(1)} %get-tuple-element.13.refs_1_), channel_id=1, source_target_pairs={{8,0},{16,8},{24,16},{28,24},{20,28},{12,20},{4,12},{0,4},{9,1},{1... | collective-permute-start | bytes 786440 | tf_op jit(solution)/shard_map/ppermute | solution.py:328
  13.4 7.5 %collective-permute-start.1 = (bf16[2,512,128]{2,1,0:T(8,128)(2,1)S(1)}, bf16[2,512,128]{2,1,0:T(8,128)(2,1)S(1)}, u32[]{:S(2)}, u32[]{:S(2)}) collective-permute-start(bf16[2,512,128]{2,1,0:T(8,128)(2,1)S(1)} %collective-permute-done.refs_1_), channel_id=1, source_target_pairs={{0,8},{8,16},{16,24},{24,28},{28,20},{20,12},{12,4},{4,0},{1,9},{9... | collective-permute-start | bytes 786440 | tf_op jit(solution)/shard_map/ppermute | solution.py:327
  15.2 7.2 %collective-permute-start.5 = (bf16[2,512,128]{2,1,0:T(8,128)(2,1)S(1)}, bf16[2,512,128]{2,1,0:T(8,128)(2,1)S(1)}, u32[]{:S(2)}, u32[]{:S(2)}) collective-permute-start(bf16[2,512,128]{2,1,0:T(8,128)(2,1)S(1)} %collective-permute-done.4.refs_2_), channel_id=1, source_target_pairs={{8,0},{16,8},{24,16},{28,24},{20,28},{12,20},{4,12},{0,4},{9,1},{1... | collective-permute-start | bytes 786440 | tf_op jit(solution)/shard_map/ppermute | solution.py:328
  20.8 6.6 %collective-permute-start.2 = (bf16[2,512,128]{2,1,0:T(8,128)(2,1)S(1)}, bf16[2,512,128]{2,1,0:T(8,128)(2,1)S(1)}, u32[]{:S(2)}, u32[]{:S(2)}) collective-permute-start(bf16[2,512,128]{2,1,0:T(8,128)(2,1)S(1)} %collective-permute-done.1.refs_1_), channel_id=1, source_target_pairs={{0,8},{8,16},{16,24},{24,28},{28,20},{20,12},{12,4},{4,0},{1,9},{9... | collective-permute-start | bytes 786440 | tf_op jit(solution)/shard_map/ppermute | solution.py:327
  22.4 6.8 %collective-permute-start.6 = (bf16[2,512,128]{2,1,0:T(8,128)(2,1)S(1)}, bf16[2,512,128]{2,1,0:T(8,128)(2,1)S(1)}, u32[]{:S(2)}, u32[]{:S(2)}) collective-permute-start(bf16[2,512,128]{2,1,0:T(8,128)(2,1)S(1)} %collective-permute-done.5.refs_2_), channel_id=1, source_target_pairs={{8,0},{16,8},{24,16},{28,24},{20,28},{12,20},{4,12},{0,4},{9,1},{1... | collective-permute-start | bytes 786440 | tf_op jit(solution)/shard_map/ppermute | solution.py:328
  27.5 5.0 %collective-permute-start.3 = (bf16[1,512,128]{2,1,0:T(8,128)(2,1)S(1)}, bf16[1,512,128]{2,1,0:T(8,128)(2,1)S(1)}, u32[]{:S(2)}, u32[]{:S(2)}) collective-permute-start(bf16[1,512,128]{2,1,0:T(8,128)(2,1)S(1)} %slice.32), channel_id=1, source_target_pairs={{0,8},{8,16},{16,24},{24,28},{28,20},{20,12},{12,4},{4,0},{1,9},{9... | collective-permute-start | bytes 393224 | tf_op jit(solution)/shard_map/ppermute | solution.py:327
  29.2 5.0 %collective-permute-start.7 = (bf16[1,512,128]{2,1,0:T(8,128)(2,1)S(1)}, bf16[1,512,128]{2,1,0:T(8,128)(2,1)S(1)}, u32[]{:S(2)}, u32[]{:S(2)}) collective-permute-start(bf16[1,512,128]{2,1,0:T(8,128)(2,1)S(1)} %slice.33), channel_id=1, source_target_pairs={{8,0},{16,8},{24,16},{28,24},{20,28},{12,20},{4,12},{0,4},{9,1},{1... | collective-permute-start | bytes 393224 | tf_op jit(solution)/shard_map/ppermute | solution.py:328
  29.6 7.3 %copy-start.10 = (s32[128,2]{0,1:T(2,128)S(1)}, s32[128,2]{0,1:T(2,128)}, u32[]{:S(2)}) copy-start(s32[128,2]{0,1:T(2,128)} %param.19) | copy-start | bytes 3076
  29.6 12.1 %copy-start.1 = (bf16[128,2048]{1,0:T(8,128)(2,1)S(1)}, bf16[128,2048]{1,0:T(8,128)(2,1)}, u32[]{:S(2)}) copy-start(bf16[128,2048]{1,0:T(8,128)(2,1)} %refs_5_.1) | copy-start | bytes 1572868
  29.6 67.3 %copy-start.6 = (bf16[1,1024,2048]{2,1,0:T(8,128)(2,1)S(1)}, bf16[1,1024,2048]{2,1,0:T(8,128)(2,1)}, u32[]{:S(2)}) copy-start(bf16[1,1024,2048]{2,1,0:T(8,128)(2,1)} %param.23) | copy-start | bytes 12582916
  31.5 10.2 %copy-start = (bf16[1024,2048]{1,0:T(8,128)(2,1)S(1)}, bf16[1024,2048]{1,0:T(8,128)(2,1)}, u32[]{:S(2)}) copy-start(bf16[1024,2048]{1,0:T(8,128)(2,1)} %refs_4_.1) | copy-start | bytes 12582916
  31.5 10.2 %copy-start.2 = (f32[2048]{0:T(1024)S(1)}, f32[2048]{0:T(1024)}, u32[]{:S(2)}) copy-start(f32[2048]{0:T(1024)} %param.17) | copy-start | bytes 24580
  31.5 10.2 %copy-start.3 = (f32[2048]{0:T(1024)S(1)}, f32[2048]{0:T(1024)}, u32[]{:S(2)}) copy-start(f32[2048]{0:T(1024)} %param.18) | copy-start | bytes 24580
  35.3 5.0 %collective-permute-start.9 = (bf16[2,256,128]{2,1,0:T(8,128)(2,1)S(1)}, bf16[2,256,128]{2,1,0:T(8,128)(2,1)S(1)}, u32[]{:S(2)}, u32[]{:S(2)}) collective-permute-start(bf16[2,256,128]{2,1,0:T(8,128)(2,1)S(1)} %get-tuple-element.16), channel_id=1, source_target_pairs={{0,2},{1,3},{2,0},{3,1},{4,6},{5,7},{6,4},{7,5},{8,10},{9,11},{10,... | collective-permute-start | bytes 393224 | tf_op jit(solution)/shard_map/ppermute | solution.py:201
  37.1 3.3 %collective-permute-start.8 = (bf16[1,256,128]{2,1,0:T(8,128)(2,1)S(1)}, bf16[1,256,128]{2,1,0:T(8,128)(2,1)S(1)}, u32[]{:S(2)}, u32[]{:S(2)}) collective-permute-start(bf16[1,256,128]{2,1,0:T(8,128)(2,1)S(1)} %get-tuple-element.15), channel_id=1, source_target_pairs={{0,1},{1,0},{2,3},{3,2},{4,5},{5,4},{6,7},{7,6},{8,9},{9,8},{10,11... | collective-permute-start | bytes 196616 | tf_op jit(solution)/shard_map/ppermute | solution.py:201
  40.4 1.3 collective-permute-start.10
  41.7 55.2 %copy-start.5 = (bf16[1,2048,1024]{2,1,0:T(8,128)(2,1)S(1)}, bf16[1,2048,1024]{2,1,0:T(8,128)(2,1)}, u32[]{:S(2)}) copy-start(bf16[1,2048,1024]{2,1,0:T(8,128)(2,1)} %param.22) | copy-start | bytes 12582916
  43.6 53.3 %copy-start.4 = (bf16[1,2048,1024]{2,1,0:T(8,128)(2,1)S(1)}, bf16[1,2048,1024]{2,1,0:T(8,128)(2,1)}, u32[]{:S(2)}) copy-start(bf16[1,2048,1024]{2,1,0:T(8,128)(2,1)} %param.21) | copy-start | bytes 12582916
  105.0 3.7 %copy-start.11 = (f32[128,2]{0,1:T(2,128)S(1)}, f32[128,2]{0,1:T(2,128)}, u32[]{:S(2)}) copy-start(f32[128,2]{0,1:T(2,128)} %param.20) | copy-start | bytes 3076
  105.0 52.4 %all-to-all-start.1 = ((bf16[32,16,2048]{2,1,0:T(8,128)(2,1)}), bf16[32,16,2048]{2,1,0:T(8,128)(2,1)S(1)}, u32[]{:S(2)}, u32[]{:S(2)}) async-start(bf16[32,16,2048]{2,1,0:T(8,128)(2,1)} %bitcast.11), calls=%async_computation.1 | async-start | bytes 4194304 | tf_op jit(solution)/shard_map/all_to_all | solution.py:388

commit v3 on v2

--- a/solution.py
+++ b/solution.py
@@ -6,6 +6,7 @@
 from jax import lax
 from jax.experimental import pallas as pl
 from jax.experimental.pallas import tpu as pltpu
+from jax.sharding import Mesh
 from jax.sharding import PartitionSpec as P
 
 HEAD_SIZE = 64
@@ -16,8 +17,12 @@
 epsilon = 1e-06
 base_theta = 10000.0
 
+SP = ("hf", "q")
+ALL = ("hf", "q", "tp")
+HALF = ("q", "tp")
+
 VMEM = pl.BlockSpec(memory_space=pltpu.VMEM)
-ANY = pl.BlockSpec(memory_space=pl.ANY)
+HBM = pl.BlockSpec(memory_space=pltpu.HBM)
 
 
 def rotation_tables(first_row, row_count, lanes):
@@ -210,7 +215,7 @@
 def out_kernel(tp_size, *refs):
     blocks = refs[:tp_size]
     w_ref, res_ref, mix_ref, norm_ref, target_ref = refs[tp_size : tp_size + 5]
-    stream_ref, out_ref, mixed_ref, normed_ref = refs[tp_size + 5 :]
+    stream_ref, normed_ref, out_ref, mixed_ref = refs[tp_size + 5 :]
     me = lax.axis_index("tp")
     _, head_rows, row_count = blocks[0].shape
     width = w_ref.shape[1]
@@ -243,7 +248,13 @@
         cols = slice(at, at + step)
         wide = stream_ref[:, cols].astype(jnp.float32)
         normed_ref[:, cols] = (wide * scale * norm_ref[:, cols]).astype(jnp.bfloat16)
-    slots = lax.broadcasted_iota(jnp.int32, (out_ref.shape[0], row_count), 0)
+    fill_slots(normed_ref, target_ref, out_ref)
+
+
+def fill_slots(rows_ref, target_ref, out_ref):
+    row_count, width = rows_ref.shape
+    step = min(512, width)
+    slots = lax.broadcasted_iota(jnp.int32, (out_ref.shape[0], row_count), 0).astype(jnp.float32)
     hit = slots == target_ref[0:1, :]
     for k in range(1, target_ref.shape[0]):
         hit = hit | (slots == target_ref[k : k + 1, :])
@@ -251,8 +262,32 @@
     for at in range(0, width, step):
         cols = slice(at, at + step)
         out_ref[:, cols] = jnp.dot(
-            placing, normed_ref[:, cols], preferred_element_type=jnp.float32
+            placing, rows_ref[:, cols], preferred_element_type=jnp.float32
         ).astype(jnp.bfloat16)
+
+
+def gather_kernel(base_count, *refs):
+    bases = refs[:base_count]
+    slots_ref, target_ref, weight_ref, out_ref = refs[base_count:]
+    row_count, width = out_ref.shape
+    step = min(512, width)
+    slots = lax.broadcasted_iota(jnp.int32, (row_count, slots_ref.shape[0]), 1).astype(jnp.float32)
+    top_count = target_ref.shape[1]
+    picks = [
+        jnp.where(slots == target_ref[:, k : k + 1], 1.0, 0.0).astype(jnp.bfloat16)
+        for k in range(top_count)
+    ]
+    for at in range(0, width, step):
+        cols = slice(at, at + step)
+        total = None
+        for base in bases:
+            piece = base[:, cols].astype(jnp.float32)
+            total = piece if total is None else total + piece
+        for k in range(top_count):
+            row = jnp.dot(picks[k], slots_ref[:, cols], preferred_element_type=jnp.float32)
+            row = row * weight_ref[:, k : k + 1]
+            total = row if total is None else total + row
+        out_ref[:, cols] = total.astype(out_ref.dtype)
 
 
 def expert_kernel(rows_ref, gate_ref, up_ref, down_ref, out_ref, act_ref):
@@ -292,14 +327,14 @@
     q_heads = query_proj.shape[1] // HEAD_SIZE
     model_width = residual.shape[1]
     grid_rows = tok_count // GRID_W
-    cos_table, sin_table = rotation_tables(lax.axis_index("sp") * grid_rows, grid_rows, lanes)
+    cos_table, sin_table = rotation_tables(lax.axis_index(SP) * grid_rows, grid_rows, lanes)
     q_ready, kv_own = pl.pallas_call(
         prepare_kernel,
         out_shape=(
             jax.ShapeDtypeStruct((lanes, q_heads * tok_count), jnp.bfloat16),
             jax.ShapeDtypeStruct((tok_count // HALF_KEYS, 2 * HALF_KEYS, lanes), jnp.bfloat16),
         ),
-        in_specs=[ANY] * 3 + [VMEM] * 2,
+        in_specs=[HBM] * 3 + [VMEM] * 2,
         out_specs=(VMEM, VMEM),
         scratch_shapes=[
             pltpu.VMEM(query_proj.shape, jnp.bfloat16),
@@ -324,8 +359,8 @@
         if step == steps - 1:
             halves = kv_own.shape[0]
             from_left, from_right = from_left[: halves // 2], from_right[halves // 2 :]
-        next_left = lax.ppermute(from_left, "sp", ahead)
-        next_right = lax.ppermute(from_right, "sp", behind)
+        next_left = lax.ppermute(from_left, SP, ahead)
+        next_right = lax.ppermute(from_right, SP, behind)
         acc = attend(q_ready, held, acc)
         from_left, from_right = next_left, next_right
         held = [from_left, from_right]
@@ -345,76 +380,118 @@
     ).astype(jnp.bfloat16)
     earlier = jnp.dot(before, onehot.astype(jnp.bfloat16), preferred_element_type=jnp.float32)
     slot_rank = jnp.sum(jnp.where(onehot, earlier, 0.0), axis=1).astype(jnp.int32)
-    target = (flat_expert * capacity + slot_rank).reshape(top_count, row_count)
-
-    stream, outgoing = pl.pallas_call(
+    half_slots = slots_total // 2
+    target = (flat_expert * capacity + slot_rank).astype(jnp.float32)
+    target = target.reshape(top_count, row_count)
+    first_slot = (lax.axis_index("hf") * half_slots).astype(jnp.float32)
+    mirror = [(0, 1), (1, 0)]
+    with jax.named_scope("tables"):
+        far = lax.ppermute(jnp.concatenate([target, route_weight.T], axis=0), "hf", mirror)
+    far_target = far[:top_count] - first_slot
+    far_weight = far[top_count:].T
+    own_target = target - first_slot
+
+    rows_shape = jax.ShapeDtypeStruct((row_count, model_width), jnp.bfloat16)
+    slots_shape = jax.ShapeDtypeStruct((half_slots, model_width), jnp.bfloat16)
+    stream, normed, own_out = pl.pallas_call(
         functools.partial(out_kernel, tp_size),
-        out_shape=(
-            jax.ShapeDtypeStruct((row_count, model_width), jnp.bfloat16),
-            jax.ShapeDtypeStruct((slots_total, model_width), jnp.bfloat16),
-        ),
+        out_shape=(rows_shape, rows_shape, slots_shape),
         in_specs=[VMEM] * (tp_size + 5),
-        out_specs=(VMEM, VMEM),
-        scratch_shapes=[
-            pltpu.VMEM((row_count, model_width), jnp.float32),
-            pltpu.VMEM((row_count, model_width), jnp.bfloat16),
-        ],
+        out_specs=(VMEM, VMEM, VMEM),
+        scratch_shapes=[pltpu.VMEM((row_count, model_width), jnp.float32)],
         cost_estimate=pl.CostEstimate(
-            flops=2 * row_count * model_width * (out_weight.shape[0] + slots_total),
+            flops=2 * row_count * model_width * (out_weight.shape[0] + half_slots),
             bytes_accessed=8 << 20,
             transcendentals=0,
         ),
         compiler_params=pltpu.CompilerParams(vmem_limit_bytes=12 * 1024 * 1024),
-    )(*blocks, out_weight, residual, mix_gain[None, :], norm_gain[None, :], target)
-
-    outgoing = outgoing.reshape(experts, capacity, model_width)
-    slots = lax.all_to_all(outgoing, ("sp", "tp"), split_axis=0, concat_axis=0, tiled=True)
-    flat_rows = slots.reshape(-1, model_width)
-    hidden = expert_gate.shape[2]
-    done = pl.pallas_call(
-        expert_kernel,
-        out_shape=jax.ShapeDtypeStruct(flat_rows.shape, jnp.bfloat16),
-        in_specs=[VMEM] * 4,
+    )(*blocks, out_weight, residual, mix_gain[None, :], norm_gain[None, :], own_target)
+
+    def exchange(slots):
+        blocks = slots.reshape(experts // 2, capacity, model_width)
+        blocks = lax.all_to_all(blocks, HALF, split_axis=0, concat_axis=0, tiled=True)
+        return blocks.reshape(half_slots, model_width)
+
+    def expert(slots):
+        hidden = expert_gate.shape[2]
+        return pl.pallas_call(
+            expert_kernel,
+            out_shape=slots_shape,
+            in_specs=[VMEM] * 4,
+            out_specs=VMEM,
+            scratch_shapes=[pltpu.VMEM((half_slots, hidden), jnp.bfloat16)],
+            cost_estimate=pl.CostEstimate(
+                flops=6 * half_slots * model_width * hidden,
+                bytes_accessed=14 << 20,
+                transcendentals=half_slots * hidden,
+            ),
+            compiler_params=pltpu.CompilerParams(vmem_limit_bytes=16 * 1024 * 1024),
+        )(slots, expert_gate[0], expert_up[0], expert_down[0])
+
+    def gather(bases, slots, target, weight):
+        return pl.pallas_call(
+            functools.partial(gather_kernel, len(bases)),
+            out_shape=rows_shape,
+            in_specs=[VMEM] * (len(bases) + 3),
+            out_specs=VMEM,
+            cost_estimate=pl.CostEstimate(
+                flops=4 * row_count * half_slots * model_width,
+                bytes_accessed=3 << 20,
+                transcendentals=0,
+            ),
+            compiler_params=pltpu.CompilerParams(vmem_limit_bytes=12 * 1024 * 1024),
+        )(*bases, slots, target.T, weight)
+
+    with jax.named_scope("mirror_out"):
+        far_rows = lax.ppermute(normed, "hf", mirror)
+    with jax.named_scope("own_out"):
+        own_in = exchange(own_out)
+    far_out = pl.pallas_call(
+        fill_slots,
+        out_shape=slots_shape,
+        in_specs=[VMEM] * 2,
         out_specs=VMEM,
-        scratch_shapes=[pltpu.VMEM((flat_rows.shape[0], hidden), jnp.bfloat16)],
         cost_estimate=pl.CostEstimate(
-            flops=6 * flat_rows.shape[0] * model_width * hidden,
-            bytes_accessed=16 << 20,
-            transcendentals=flat_rows.shape[0] * hidden,
-        ),
-        compiler_params=pltpu.CompilerParams(vmem_limit_bytes=24 * 1024 * 1024),
-    )(flat_rows, expert_gate[0], expert_up[0], expert_down[0])
-    answered = done.reshape(slots.shape)
-    returned = lax.all_to_all(answered, ("sp", "tp"), split_axis=0, concat_axis=0, tiled=True)
-    returned = returned.reshape(slots_total, model_width)
-    chosen = target[:, :, None] == jnp.arange(slots_total, dtype=jnp.int32)[None, None, :]
-    combined = stream.astype(jnp.float32)
-    for k in range(top_count):
-        picked = jnp.dot(
-            chosen[k].astype(jnp.bfloat16), returned, preferred_element_type=jnp.float32
-        )
-        combined = combined + picked * route_weight[:, k : k + 1]
-    return combined.astype(jnp.bfloat16)
+            flops=2 * row_count * half_slots * model_width,
+            bytes_accessed=2 << 20,
+            transcendentals=0,
+        ),
+        compiler_params=pltpu.CompilerParams(vmem_limit_bytes=12 * 1024 * 1024),
+    )(far_rows, far_target)
+    with jax.named_scope("far_out"):
+        far_in = exchange(far_out)
+    own_done = expert(own_in)
+    far_done = expert(far_in)
+    with jax.named_scope("far_back"):
+        far_answer = exchange(far_done)
+    far_sum = gather([], far_answer, far_target, far_weight)
+    with jax.named_scope("mirror_back"):
+        returned = lax.ppermute(far_sum, "hf", mirror)
+    with jax.named_scope("own_back"):
+        own_answer = exchange(own_done)
+    return gather([stream, returned], own_answer, own_target, route_weight)
 
 
 def solution(mesh):
+    sp_size, tp_size = mesh.shape["sp"], mesh.shape["tp"]
+    split = Mesh(mesh.devices.reshape(2, sp_size // 2, tp_size), ALL)
     return jax.shard_map(
-        functools.partial(local, mesh.shape["sp"], mesh.shape["tp"]),
-        mesh=mesh,
+        functools.partial(local, sp_size, tp_size),
+        mesh=split,
         in_specs=(
-            P("sp", "tp"),
-            P("sp", "tp"),
-            P("sp", "tp"),
-            P(("sp", "tp"), None),
+            P(SP, "tp"),
+            P(SP, "tp"),
+            P(SP, "tp"),
+            P(ALL, None),
             P(),
             P(),
             P(),
-            P(("sp", "tp"), None),
-            P(("sp", "tp"), None),
-            P(("sp", "tp"), None, None),
-            P(("sp", "tp"), None, None),
-            P(("sp", "tp"), None, None),
-        ),
-        out_specs=P(("sp", "tp"), None),
+            P(ALL, None),
+            P(ALL, None),
+            P(ALL, None, None),
+            P(ALL, None, None),
+            P(ALL, None, None),
+        ),
+        out_specs=P(ALL, None),
         check_vma=False,
     )

time: 160 us -> 168 us (1.050)
  blocking collectives: 53.3 us -> 19.9 us
  local copies, waits for them, and re-layouts: 2.83 us -> 19.3 us
  starting transfers between devices: 14.7 us -> 27.8 us
  waiting for transfers between devices: 67.1 us -> 77.4 us
  Pallas kernels: 18.6 us -> 22.5 us
    all_to_all x1, blocking collectives: 53.3 us -> 19.9 us  [exchange(): lax.all_to_all(blocks, HALF, split_axis=0, concat_axis=0, tiled=True)]
    ppermute x8 -> x11, waiting for transfers between devices: 14.2 us -> 38.7 us  [the longest x1 25.7 us: local(): lax.ppermute(jnp.concatenate([target, route_weight.T], axis=0), 'hf', mir...]
    unnamed x24 -> x30, local copies, waits for them, and re-layouts: 2.8 us -> 19 us
    all_to_all x1 -> x3, waiting for transfers between devices: 48.5 us -> 34.3 us  [exchange(): lax.all_to_all(blocks, HALF, split_axis=0, concat_axis=0, tiled=True)]
    all_to_all x1 -> x3, starting transfers between devices: 3.67 us -> 11.1 us  [exchange(): lax.all_to_all(blocks, HALF, split_axis=0, concat_axis=0, tiled=True)]
    ppermute x8 -> x11, starting transfers between devices: 9.29 us -> 15 us  [the longest x4 7.6 us: local(): next_right = lax.ppermute(from_right, SP, behind)]
    pallas_call x2 -> x6, Pallas kernels: 9.9 us -> 13.8 us  [the longest x2 8.89 us: expert(): pl.pallas_call(expert_kernel, out_shape=slots_shape, in_specs=[VMEM] * 4,...]
  transfers between devices with their start and end apart: 12 -> 17, of which waited for: 8 -> 11; matrix products, arithmetic and copies ran while one was open for 0% -> 1% of each run, Pallas kernels for 4% -> 10%
where the time goes in v3:
time: 168 us
  waiting for transfers between devices  77.4 us (46%)
  starting transfers between devices  27.8 us (17%)
  Pallas kernels  22.5 us (13%)
  blocking collectives  19.9 us (12%)
  local copies, waits for them, and re-layouts  19.3 us (11%)
    all_to_all x3, waiting for transfers between devices, exchange(): lax.all_to_all(blocks, HALF, split_axis=0, concat_axis=0, tiled=True)  34.3 us
    ppermute x1, waiting for transfers between devices, local(): lax.ppermute(jnp.concatenate([target, route_weight.T], axis=0), 'hf', mir...  25.7 us
    all_to_all x1, blocking collectives, exchange(): lax.all_to_all(blocks, HALF, split_axis=0, concat_axis=0, tiled=True)  19.9 us
    unnamed x30, local copies, waits for them, and re-layouts  19 us
    ppermute x4, waiting for transfers between devices, local(): next_right = lax.ppermute(from_right, SP, behind)  11.4 us
    all_to_all x3, starting transfers between devices, exchange(): lax.all_to_all(blocks, HALF, split_axis=0, concat_axis=0, tiled=True)  11.1 us
    pallas_call x2, Pallas kernels, expert(): pl.pallas_call(expert_kernel, out_shape=slots_shape, in_specs=[VMEM] * 4,...  8.89 us
    pallas_call x5, Pallas kernels, attend(): pl.pallas_call(functools.partial(attend_kernel, len(chunks), first, last)...  7.71 us
  transfers between devices with their start and end apart: 17, of which 11 were waited for; matrix products, arithmetic and copies ran while one was open for 1% of the time, Pallas kernels for 10%

profile of v3, /device:TPU:0, one launch (start us, length us, event | category | flops | bytes accessed | tf_op | source)
XLA Modules:
  0.0 167.7 jit_solution(3395062402494659367)
XLA Ops:
  4.0 3.0 %collective-permute-start.4 = (bf16[2,512,128]{2,1,0:T(8,128)(2,1)S(1)}, bf16[2,512,128]{2,1,0:T(8,128)(2,1)S(1)}, u32[]{:S(2)}, u32[]{:S(2)}) collective-permute-start(bf16[2,512,128]{2,1,0:T(8,128)(2,1)S(1)} %get-tuple-element.14.refs_1_), channel_id=1, source_target_pairs={{8,0},{16,8},{24,16},{28,24},{20,28},{12,20},{4,12},{0,4},{9,1},{1... | collective-permute-start | bytes 786440 | tf_op jit(solution)/shard_map/ppermute | solution.py:363
  7.2 6.2 %collective-permute-done.4.refs_2_ = bf16[2,512,128]{2,1,0:T(8,128)(2,1)S(1)} collective-permute-done((bf16[2,512,128]{2,1,0:T(8,128)(2,1)S(1)}, bf16[2,512,128]{2,1,0:T(8,128)(2,1)S(1)}, u32[]{:S(2)}, u32[]{:S(2)}) %collective-permute-start.4) | collective-permute-done | bytes 262176 | tf_op jit(solution)/shard_map/ppermute | solution.py:363
  17.6 3.3 %collective-permute-done.5.refs_2_ = bf16[2,512,128]{2,1,0:T(8,128)(2,1)S(1)} collective-permute-done((bf16[2,512,128]{2,1,0:T(8,128)(2,1)S(1)}, bf16[2,512,128]{2,1,0:T(8,128)(2,1)S(1)}, u32[]{:S(2)}, u32[]{:S(2)}) %collective-permute-start.5) | collective-permute-done | bytes 262176 | tf_op jit(solution)/shard_map/ppermute | solution.py:363
  24.8 1.9 %shard_map.121.refs_3_ = f32[80,2048]{1,0:T(8,128)S(1)} custom-call(bf16[128,2048]{1,0:T(8,128)(2,1)S(1)} %get-tuple-element.13.refs_0_, bf16[2,512,128]{2,1,0:T(8,128)(2,1)S(1)} %collective-permute-done.1.refs_1_, bf16[2,512,128]{2,1,0:T(8,128)(2,1)S(1)} %collective-permute-done.5.refs_2_, ...), custom_call_target="tpu_custom_call", output_to_operand_aliasing={{}: (3, {})} | custom-call | flops 2147483648 | bytes 1048576 | tf_op jit(solution)/shard_map/pallas_call | solution.py:184
  37.0 3.3 %collective-permute-done.9 = bf16[2,256,128]{2,1,0:T(8,128)(2,1)S(1)} collective-permute-done((bf16[2,256,128]{2,1,0:T(8,128)(2,1)S(1)}, bf16[2,256,128]{2,1,0:T(8,128)(2,1)S(1)}, u32[]{:S(2)}, u32[]{:S(2)}) %collective-permute-start.9) | collective-permute-done | bytes 131104 | tf_op jit(solution)/shard_map/ppermute | solution.py:206
  41.6 2.2 %copy-done.6 = bf16[1024,2048]{1,0:T(8,128)(2,1)S(1)} copy-done((bf16[1024,2048]{1,0:T(8,128)(2,1)S(1)}, bf16[1024,2048]{1,0:T(8,128)(2,1)}, u32[]{:S(2)}) %copy-start.6) | copy-done | bytes 4194328
  43.8 2.6 %shard_map.124 = (bf16[128,2048]{1,0:T(8,128)(2,1)S(1)}, bf16[128,2048]{1,0:T(8,128)(2,1)S(1)}, bf16[256,2048]{1,0:T(8,128)(2,1)}) custom-call(bf16[1,256,128]{2,1,0:T(8,128)(2,1)S(1)} %get-tuple-element.15.refs_0_, bf16[1,256,128]{2,1,0:T(8,128)(2,1)S(1)} %collective-permute-done.8.refs_1_, bf16[1,256,128]{2,1,0:T(8,128)(2,1)S(1)} %get-tuple-element.24.refs_2_, ...), custom_call_target="tpu_custom_call" | custom-call | flops 671088640 | bytes 8388608 | tf_op jit(solution)/shard_map/pallas_call | solution.py:396
  49.6 25.7 %collective-permute-done.12 = f32[4,128]{0,1:T(8,128)S(1)} collective-permute-done((f32[4,128]{0,1:T(8,128)S(1)}, f32[4,128]{0,1:T(8,128)S(1)}, u32[]{:S(2)}, u32[]{:S(2)}) %collective-permute-start.12) | collective-permute-done | bytes 2080 | tf_op jit(solution)/shard_map/tables/ppermute | solution.py:389
  75.9 19.9 %all_to_all.20 = bf16[16,16,2048]{2,1,0:T(8,128)(2,1)S(1)} all-to-all(bf16[16,16,2048]{2,1,0:T(8,128)(2,1)S(1)} %bitcast.33), channel_id=1, replica_groups=mesh['hf'=2,'q'=4,'tp'=4] {'q','tp'}, dimensions={0} | all-to-all | bytes 2097152 | tf_op jit(solution)/shard_map/far_out/all_to_all | solution.py:412
  95.8 3.8 %all-to-all-start.2 = ((bf16[16,16,2048]{2,1,0:T(8,128)(2,1)}), bf16[16,16,2048]{2,1,0:T(8,128)(2,1)S(1)}, u32[]{:S(2)}, u32[]{:S(2)}) async-start(bf16[16,16,2048]{2,1,0:T(8,128)(2,1)} %bitcast.15), calls=%async_computation.2 | async-start | bytes 2097152 | tf_op jit(solution)/shard_map/own_out/all_to_all | solution.py:412
  99.6 2.2 %copy-done = bf16[1,2048,1024]{2,1,0:T(8,128)(2,1)S(1)} copy-done((bf16[1,2048,1024]{2,1,0:T(8,128)(2,1)S(1)}, bf16[1,2048,1024]{2,1,0:T(8,128)(2,1)}, u32[]{:S(2)}) %copy-start) | copy-done | bytes 4194328
  101.8 2.2 %copy-done.2 = bf16[1,2048,1024]{2,1,0:T(8,128)(2,1)S(1)} copy-done((bf16[1,2048,1024]{2,1,0:T(8,128)(2,1)S(1)}, bf16[1,2048,1024]{2,1,0:T(8,128)(2,1)}, u32[]{:S(2)}) %copy-start.2) | copy-done | bytes 4194328
  104.0 2.2 %copy-done.4 = bf16[1,1024,2048]{2,1,0:T(8,128)(2,1)S(1)} copy-done((bf16[1,1024,2048]{2,1,0:T(8,128)(2,1)S(1)}, bf16[1,1024,2048]{2,1,0:T(8,128)(2,1)}, u32[]{:S(2)}) %copy-start.4) | copy-done | bytes 4194328
  106.2 4.4 %shard_map.126 = bf16[256,2048]{1,0:T(8,128)(2,1)} custom-call(bf16[256,2048]{1,0:T(8,128)(2,1)S(1)} %bitcast.31, bf16[2048,1024]{1,0:T(8,128)(2,1)S(1)} %bitcast.24, bf16[2048,1024]{1,0:T(8,128)(2,1)S(1)} %bitcast.26, bf16[1024,2048]{1,0:T(8,128)(2,1)S(1)} %bitcast.28), custom_call_target="tpu_custom_call" | custom-call | flops 3221225472 | bytes 14680064 | tf_op jit(solution)/shard_map/pallas_call | solution.py:417
  110.6 5.0 %all-to-all-done.2 = bf16[16,16,2048]{2,1,0:T(8,128)(2,1)S(1)} async-done(((bf16[16,16,2048]{2,1,0:T(8,128)(2,1)}), bf16[16,16,2048]{2,1,0:T(8,128)(2,1)S(1)}, u32[]{:S(2)}, u32[]{:S(2)}) %all-to-all-start.2) | async-done | bytes 1048608 | tf_op jit(solution)/shard_map/own_out/all_to_all | solution.py:412
  115.6 3.7 %all-to-all-start.1 = ((bf16[16,16,2048]{2,1,0:T(8,128)(2,1)}), bf16[16,16,2048]{2,1,0:T(8,128)(2,1)S(1)}, u32[]{:S(2)}, u32[]{:S(2)}) async-start(bf16[16,16,2048]{2,1,0:T(8,128)(2,1)} %bitcast.11), calls=%async_computation.1 | async-start | bytes 2097152 | tf_op jit(solution)/shard_map/far_back/all_to_all | solution.py:412
  119.3 2.2 %copy-done.1 = bf16[1,2048,1024]{2,1,0:T(8,128)(2,1)S(1)} copy-done((bf16[1,2048,1024]{2,1,0:T(8,128)(2,1)S(1)}, bf16[1,2048,1024]{2,1,0:T(8,128)(2,1)}, u32[]{:S(2)}) %copy-start.1) | copy-done | bytes 4194328
  121.4 2.2 %copy-done.3 = bf16[1,2048,1024]{2,1,0:T(8,128)(2,1)S(1)} copy-done((bf16[1,2048,1024]{2,1,0:T(8,128)(2,1)S(1)}, bf16[1,2048,1024]{2,1,0:T(8,128)(2,1)}, u32[]{:S(2)}) %copy-start.3) | copy-done | bytes 4194328
  123.6 2.2 %copy-done.5 = bf16[1,1024,2048]{2,1,0:T(8,128)(2,1)S(1)} copy-done((bf16[1,1024,2048]{2,1,0:T(8,128)(2,1)S(1)}, bf16[1,1024,2048]{2,1,0:T(8,128)(2,1)}, u32[]{:S(2)}) %copy-start.5) | copy-done | bytes 4194328
  125.8 4.4 %shard_map.128 = bf16[256,2048]{1,0:T(8,128)(2,1)} custom-call(bf16[256,2048]{1,0:T(8,128)(2,1)S(1)} %bitcast.30, bf16[2048,1024]{1,0:T(8,128)(2,1)S(1)} %bitcast.25, bf16[2048,1024]{1,0:T(8,128)(2,1)S(1)} %bitcast.27, bf16[1024,2048]{1,0:T(8,128)(2,1)S(1)} %bitcast.29), custom_call_target="tpu_custom_call" | custom-call | flops 3221225472 | bytes 14680064 | tf_op jit(solution)/shard_map/pallas_call | solution.py:417
  130.3 5.1 %all-to-all-done.1 = bf16[16,16,2048]{2,1,0:T(8,128)(2,1)S(1)} async-done(((bf16[16,16,2048]{2,1,0:T(8,128)(2,1)}), bf16[16,16,2048]{2,1,0:T(8,128)(2,1)S(1)}, u32[]{:S(2)}, u32[]{:S(2)}) %all-to-all-start.1) | async-done | bytes 1048608 | tf_op jit(solution)/shard_map/far_back/all_to_all | solution.py:412
  135.4 3.7 %all-to-all-start.3 = ((bf16[16,16,2048]{2,1,0:T(8,128)(2,1)}), bf16[16,16,2048]{2,1,0:T(8,128)(2,1)S(1)}, u32[]{:S(2)}, u32[]{:S(2)}) async-start(bf16[16,16,2048]{2,1,0:T(8,128)(2,1)} %bitcast.17), calls=%async_computation.3 | async-start | bytes 2097152 | tf_op jit(solution)/shard_map/own_back/all_to_all | solution.py:412
  139.6 2.6 %collective-permute-start.13 = (bf16[128,2048]{1,0:T(8,128)(2,1)S(1)}, bf16[128,2048]{1,0:T(8,128)(2,1)S(1)}, u32[]{:S(2)}, u32[]{:S(2)}) collective-permute-start(bf16[128,2048]{1,0:T(8,128)(2,1)S(1)} %shard_map.127), channel_id=1, source_target_pairs={{0,16},{16,0},{1,17},{17,1},{2,18},{18,2},{3,19},{19,3},{4,20},{20... | collective-permute-start | bytes 1572872 | tf_op jit(solution)/shard_map/mirror_back/ppermute | solution.py:469
  142.2 24.2 %all-to-all-done.3 = bf16[16,16,2048]{2,1,0:T(8,128)(2,1)S(1)} async-done(((bf16[16,16,2048]{2,1,0:T(8,128)(2,1)}), bf16[16,16,2048]{2,1,0:T(8,128)(2,1)S(1)}, u32[]{:S(2)}, u32[]{:S(2)}) %all-to-all-start.3) | async-done | bytes 1048608 | tf_op jit(solution)/shard_map/own_back/all_to_all | solution.py:412
  (68 shorter events, 29.4 us)
Async XLA Ops:
  4.0 9.4 %collective-permute-start.4 = (bf16[2,512,128]{2,1,0:T(8,128)(2,1)S(1)}, bf16[2,512,128]{2,1,0:T(8,128)(2,1)S(1)}, u32[]{:S(2)}, u32[]{:S(2)}) collective-permute-start(bf16[2,512,128]{2,1,0:T(8,128)(2,1)S(1)} %get-tuple-element.14.refs_1_), channel_id=1, source_target_pairs={{8,0},{16,8},{24,16},{28,24},{20,28},{12,20},{4,12},{0,4},{9,1},{1... | collective-permute-start | bytes 786440 | tf_op jit(solution)/shard_map/ppermute | solution.py:363
  7.1 8.0 %collective-permute-start = (bf16[2,512,128]{2,1,0:T(8,128)(2,1)S(1)}, bf16[2,512,128]{2,1,0:T(8,128)(2,1)S(1)}, u32[]{:S(2)}, u32[]{:S(2)}) collective-permute-start(bf16[2,512,128]{2,1,0:T(8,128)(2,1)S(1)} %get-tuple-element.14.refs_1_), channel_id=1, source_target_pairs={{0,8},{8,16},{16,24},{24,28},{28,20},{20,12},{12,4},{4,0},{1,9},{9... | collective-permute-start | bytes 786440 | tf_op jit(solution)/shard_map/ppermute | solution.py:362
  13.4 7.5 %collective-permute-start.5 = (bf16[2,512,128]{2,1,0:T(8,128)(2,1)S(1)}, bf16[2,512,128]{2,1,0:T(8,128)(2,1)S(1)}, u32[]{:S(2)}, u32[]{:S(2)}) collective-permute-start(bf16[2,512,128]{2,1,0:T(8,128)(2,1)S(1)} %collective-permute-done.4.refs_2_), channel_id=1, source_target_pairs={{8,0},{16,8},{24,16},{28,24},{20,28},{12,20},{4,12},{0,4},{9,1},{1... | collective-permute-start | bytes 786440 | tf_op jit(solution)/shard_map/ppermute | solution.py:363
  15.1 7.2 %collective-permute-start.1 = (bf16[2,512,128]{2,1,0:T(8,128)(2,1)S(1)}, bf16[2,512,128]{2,1,0:T(8,128)(2,1)S(1)}, u32[]{:S(2)}, u32[]{:S(2)}) collective-permute-start(bf16[2,512,128]{2,1,0:T(8,128)(2,1)S(1)} %collective-permute-done.refs_1_), channel_id=1, source_target_pairs={{0,8},{8,16},{16,24},{24,28},{28,20},{20,12},{12,4},{4,0},{1,9},{9... | collective-permute-start | bytes 786440 | tf_op jit(solution)/shard_map/ppermute | solution.py:362
  20.9 6.6 %collective-permute-start.6 = (bf16[2,512,128]{2,1,0:T(8,128)(2,1)S(1)}, bf16[2,512,128]{2,1,0:T(8,128)(2,1)S(1)}, u32[]{:S(2)}, u32[]{:S(2)}) collective-permute-start(bf16[2,512,128]{2,1,0:T(8,128)(2,1)S(1)} %collective-permute-done.5.refs_2_), channel_id=1, source_target_pairs={{8,0},{16,8},{24,16},{28,24},{20,28},{12,20},{4,12},{0,4},{9,1},{1... | collective-permute-start | bytes 786440 | tf_op jit(solution)/shard_map/ppermute | solution.py:363
  22.3 6.8 %collective-permute-start.2 = (bf16[2,512,128]{2,1,0:T(8,128)(2,1)S(1)}, bf16[2,512,128]{2,1,0:T(8,128)(2,1)S(1)}, u32[]{:S(2)}, u32[]{:S(2)}) collective-permute-start(bf16[2,512,128]{2,1,0:T(8,128)(2,1)S(1)} %collective-permute-done.1.refs_1_), channel_id=1, source_target_pairs={{0,8},{8,16},{16,24},{24,28},{28,20},{20,12},{12,4},{4,0},{1,9},{9... | collective-permute-start | bytes 786440 | tf_op jit(solution)/shard_map/ppermute | solution.py:362
  27.5 5.0 %collective-permute-start.7 = (bf16[1,512,128]{2,1,0:T(8,128)(2,1)S(1)}, bf16[1,512,128]{2,1,0:T(8,128)(2,1)S(1)}, u32[]{:S(2)}, u32[]{:S(2)}) collective-permute-start(bf16[1,512,128]{2,1,0:T(8,128)(2,1)S(1)} %slice.25), channel_id=1, source_target_pairs={{8,0},{16,8},{24,16},{28,24},{20,28},{12,20},{4,12},{0,4},{9,1},{1... | collective-permute-start | bytes 393224 | tf_op jit(solution)/shard_map/ppermute | solution.py:363
  29.1 5.0 %collective-permute-start.3 = (bf16[1,512,128]{2,1,0:T(8,128)(2,1)S(1)}, bf16[1,512,128]{2,1,0:T(8,128)(2,1)S(1)}, u32[]{:S(2)}, u32[]{:S(2)}) collective-permute-start(bf16[1,512,128]{2,1,0:T(8,128)(2,1)S(1)} %slice.24), channel_id=1, source_target_pairs={{0,8},{8,16},{16,24},{24,28},{28,20},{20,12},{12,4},{4,0},{1,9},{9... | collective-permute-start | bytes 393224 | tf_op jit(solution)/shard_map/ppermute | solution.py:362
  31.5 10.1 %copy-start.7 = (bf16[128,2048]{1,0:T(8,128)(2,1)S(1)}, bf16[128,2048]{1,0:T(8,128)(2,1)}, u32[]{:S(2)}) copy-start(bf16[128,2048]{1,0:T(8,128)(2,1)} %refs_5_.1) | copy-start | bytes 1572868
  31.6 10.1 %copy-start.8 = (f32[2048]{0:T(1024)S(1)}, f32[2048]{0:T(1024)}, u32[]{:S(2)}) copy-start(f32[2048]{0:T(1024)} %param.17) | copy-start | bytes 24580
  31.6 10.0 %copy-start.9 = (f32[2048]{0:T(1024)S(1)}, f32[2048]{0:T(1024)}, u32[]{:S(2)}) copy-start(f32[2048]{0:T(1024)} %param.18) | copy-start | bytes 24580
  31.6 16.4 %copy-start.13 = (f32[128,2]{0,1:T(2,128)S(1)}, f32[128,2]{0,1:T(2,128)}, u32[]{:S(2)}) copy-start(f32[128,2]{0,1:T(2,128)} %param.20) | copy-start | bytes 3076
  35.2 5.0 %collective-permute-start.9 = (bf16[2,256,128]{2,1,0:T(8,128)(2,1)S(1)}, bf16[2,256,128]{2,1,0:T(8,128)(2,1)S(1)}, u32[]{:S(2)}, u32[]{:S(2)}) collective-permute-start(bf16[2,256,128]{2,1,0:T(8,128)(2,1)S(1)} %get-tuple-element.17), channel_id=1, source_target_pairs={{0,2},{1,3},{2,0},{3,1},{4,6},{5,7},{6,4},{7,5},{8,10},{9,11},{10,... | collective-permute-start | bytes 393224 | tf_op jit(solution)/shard_map/ppermute | solution.py:206
  36.9 3.5 %collective-permute-start.8 = (bf16[1,256,128]{2,1,0:T(8,128)(2,1)S(1)}, bf16[1,256,128]{2,1,0:T(8,128)(2,1)S(1)}, u32[]{:S(2)}, u32[]{:S(2)}) collective-permute-start(bf16[1,256,128]{2,1,0:T(8,128)(2,1)S(1)} %get-tuple-element.16), channel_id=1, source_target_pairs={{0,1},{1,0},{2,3},{3,2},{4,5},{5,4},{6,7},{7,6},{8,9},{9,8},{10,11... | collective-permute-start | bytes 196616 | tf_op jit(solution)/shard_map/ppermute | solution.py:206
  40.3 1.3 collective-permute-start.10
  41.6 2.2 %copy-start.6 = (bf16[1024,2048]{1,0:T(8,128)(2,1)S(1)}, bf16[1024,2048]{1,0:T(8,128)(2,1)}, u32[]{:S(2)}) copy-start(bf16[1024,2048]{1,0:T(8,128)(2,1)} %refs_4_.2) | copy-start | bytes 12582916
  46.4 29.0 %collective-permute-start.11 = (bf16[128,2048]{1,0:T(8,128)(2,1)S(1)}, bf16[128,2048]{1,0:T(8,128)(2,1)S(1)}, u32[]{:S(2)}, u32[]{:S(2)}) collective-permute-start(bf16[128,2048]{1,0:T(8,128)(2,1)S(1)} %get-tuple-element.19), channel_id=1, source_target_pairs={{0,16},{16,0},{1,17},{17,1},{2,18},{18,2},{3,19},{19,3},{4,20},{20... | collective-permute-start | bytes 1572872 | tf_op jit(solution)/shard_map/mirror_out/ppermute | solution.py:446
  48.2 27.1 %collective-permute-start.12 = (f32[4,128]{0,1:T(8,128)S(1)}, f32[4,128]{0,1:T(8,128)S(1)}, u32[]{:S(2)}, u32[]{:S(2)}) collective-permute-start(f32[4,128]{0,1:T(8,128)S(1)} %pad_maximum_fusion), channel_id=1, source_target_pairs={{0,16},{16,0},{1,17},{17,1},{2,18},{18,2},{3,19},{19,3},{4,20},{20... | collective-permute-start | bytes 6152 | tf_op jit(solution)/shard_map/tables/ppermute | solution.py:389
  95.8 19.8 %all-to-all-start.2 = ((bf16[16,16,2048]{2,1,0:T(8,128)(2,1)}), bf16[16,16,2048]{2,1,0:T(8,128)(2,1)S(1)}, u32[]{:S(2)}, u32[]{:S(2)}) async-start(bf16[16,16,2048]{2,1,0:T(8,128)(2,1)} %bitcast.15), calls=%async_computation.2 | async-start | bytes 2097152 | tf_op jit(solution)/shard_map/own_out/all_to_all | solution.py:412
  99.6 2.2 %copy-start = (bf16[1,2048,1024]{2,1,0:T(8,128)(2,1)S(1)}, bf16[1,2048,1024]{2,1,0:T(8,128)(2,1)}, u32[]{:S(2)}) copy-start(bf16[1,2048,1024]{2,1,0:T(8,128)(2,1)} %param.21) | copy-start | bytes 12582916
  115.6 19.8 %all-to-all-start.1 = ((bf16[16,16,2048]{2,1,0:T(8,128)(2,1)}), bf16[16,16,2048]{2,1,0:T(8,128)(2,1)S(1)}, u32[]{:S(2)}, u32[]{:S(2)}) async-start(bf16[16,16,2048]{2,1,0:T(8,128)(2,1)} %bitcast.11), calls=%async_computation.1 | async-start | bytes 2097152 | tf_op jit(solution)/shard_map/far_back/all_to_all | solution.py:412
  119.2 2.2 %copy-start.1 = (bf16[1,2048,1024]{2,1,0:T(8,128)(2,1)S(1)}, bf16[1,2048,1024]{2,1,0:T(8,128)(2,1)}, u32[]{:S(2)}) copy-start(bf16[1,2048,1024]{2,1,0:T(8,128)(2,1)} %param.21) | copy-start | bytes 12582916
  135.4 31.0 %all-to-all-start.3 = ((bf16[16,16,2048]{2,1,0:T(8,128)(2,1)}), bf16[16,16,2048]{2,1,0:T(8,128)(2,1)S(1)}, u32[]{:S(2)}, u32[]{:S(2)}) async-start(bf16[16,16,2048]{2,1,0:T(8,128)(2,1)} %bitcast.17), calls=%async_computation.3 | async-start | bytes 2097152 | tf_op jit(solution)/shard_map/own_back/all_to_all | solution.py:412
  139.6 26.8 %collective-permute-start.13 = (bf16[128,2048]{1,0:T(8,128)(2,1)S(1)}, bf16[128,2048]{1,0:T(8,128)(2,1)S(1)}, u32[]{:S(2)}, u32[]{:S(2)}) collective-permute-start(bf16[128,2048]{1,0:T(8,128)(2,1)S(1)} %shard_map.127), channel_id=1, source_target_pairs={{0,16},{16,0},{1,17},{17,1},{2,18},{18,2},{3,19},{19,3},{4,20},{20... | collective-permute-start | bytes 1572872 | tf_op jit(solution)/shard_map/mirror_back/ppermute | solution.py:469
  (7 other events, 11.5 us)

commit v4 on v3

--- a/solution.py
+++ b/solution.py
@@ -8,6 +8,7 @@
 from jax.experimental.pallas import tpu as pltpu
 from jax.sharding import Mesh
 from jax.sharding import PartitionSpec as P
+
 
 HEAD_SIZE = 64
 GRID_W = 64
@@ -98,7 +99,13 @@
             ] = turned[inner * HEAD_SIZE : (inner + 1) * HEAD_SIZE].astype(jnp.bfloat16)
 
 
-def attend_kernel(chunk_count, first, last, *refs):
+def attend_kernel(chunk_count, first, last, staged, after, *refs):
+    if staged:
+        stage = pltpu.make_async_copy(refs[-4], refs[-2], refs[-1])
+        stage.start()
+        refs = refs[:-4] + (refs[-3],)
+    if after:
+        refs = refs[: 2 + chunk_count] + refs[3 + chunk_count :]
     q_ref = refs[0]
     chunks = refs[1 : 1 + chunk_count]
     acc_in = None if first else refs[1 + chunk_count]
@@ -145,7 +152,7 @@
                 out_refs[0][:, at : at + width] = total
             else:
                 turn = out_refs[-1]
-                tp, head_rows, per = turn.shape
+                tp, _, per = turn.shape
                 tok_count = tp * per
                 ready = (total[:HEAD_SIZE] / total[HEAD_SIZE : HEAD_SIZE + 1]).astype(jnp.bfloat16)
                 for piece in range(width // per):
@@ -154,6 +161,8 @@
                         :, piece * per : (piece + 1) * per
                     ]
         waiting = weights
+    if staged:
+        stage.wait()
     if last:
         me = lax.axis_index("tp")
         turn = out_refs[-1]
@@ -164,9 +173,9 @@
                 rel += 1
 
 
-def attend(q_ready, chunks, acc, tp_size=None):
+def attend(q_ready, chunks, acc, tp_size=None, staged=None, after=None):
     first, last = acc is None, tp_size is not None
-    lanes, columns = q_ready.shape
+    _, columns = q_ready.shape
     rows = HEAD_SIZE + ONES_ROWS
     key_count = sum(c.shape[0] for c in chunks) * HALF_KEYS
     scratch = []
@@ -180,11 +189,22 @@
     else:
         shape = [jax.ShapeDtypeStruct((rows, columns), jnp.float32)]
     operands = [q_ready, *chunks] + ([] if first else [acc])
+    specs = [VMEM] * len(operands)
     aliases = {} if (first or last) else {len(operands) - 1: 0}
+    if after is not None:
+        operands.append(after)
+        specs.append(HBM)
+    if staged is not None:
+        operands.append(staged)
+        specs.append(HBM)
+        shape.append(jax.ShapeDtypeStruct(staged.shape, staged.dtype))
+        scratch.append(pltpu.SemaphoreType.DMA)
     out = pl.pallas_call(
-        functools.partial(attend_kernel, len(chunks), first, last),
+        functools.partial(
+            attend_kernel, len(chunks), first, last, staged is not None, after is not None
+        ),
         out_shape=shape,
-        in_specs=[VMEM] * len(operands),
+        in_specs=specs,
         out_specs=[VMEM] * len(shape),
         scratch_shapes=scratch,
         input_output_aliases=aliases,
@@ -195,7 +215,7 @@
         ),
         compiler_params=pltpu.CompilerParams(vmem_limit_bytes=24 * 1024 * 1024),
     )(*operands)
-    return out if last else out[0]
+    return out if last or staged is not None else out[0]
 
 
 def hypercube_exchange(pieces, tp_size):
@@ -212,9 +232,9 @@
     return [pieces[0]] + [block for _, block in sorted(held, key=lambda item: item[0])]
 
 
-def out_kernel(tp_size, *refs):
+def out_kernel(tp_size, top_count, *refs):
     blocks = refs[:tp_size]
-    w_ref, res_ref, mix_ref, norm_ref, target_ref = refs[tp_size : tp_size + 5]
+    w_ref, res_ref, mix_ref, norm_ref, table_ref = refs[tp_size : tp_size + 5]
     stream_ref, normed_ref, out_ref, mixed_ref = refs[tp_size + 5 :]
     me = lax.axis_index("tp")
     _, head_rows, row_count = blocks[0].shape
@@ -248,16 +268,43 @@
         cols = slice(at, at + step)
         wide = stream_ref[:, cols].astype(jnp.float32)
         normed_ref[:, cols] = (wide * scale * norm_ref[:, cols]).astype(jnp.bfloat16)
-    fill_slots(normed_ref, target_ref, out_ref)
-
-
-def fill_slots(rows_ref, target_ref, out_ref):
+    fill_slots(top_count, normed_ref, table_ref, out_ref)
+
+
+def routes_kernel(capacity, expert_ref, weight_ref, out_ref):
+    row_count, top_count = expert_ref.shape
+    lanes = out_ref.shape[1]
+    lane = lax.broadcasted_iota(jnp.int32, (row_count, lanes), 1)
+    before = lax.broadcasted_iota(jnp.int32, (row_count, row_count), 0) > (
+        lax.broadcasted_iota(jnp.int32, (row_count, row_count), 1)
+    )
+    before = jnp.where(before, 1.0, 0.0).astype(jnp.bfloat16)
+    taken = jnp.zeros((1, lanes), jnp.float32)
+    table = jnp.zeros((row_count, lanes), jnp.float32)
+    for k in range(top_count):
+        expert = expert_ref[:, k : k + 1]
+        onehot = jnp.where(lane == expert, 1.0, 0.0)
+        earlier = taken + jnp.dot(
+            before, onehot.astype(jnp.bfloat16), preferred_element_type=jnp.float32
+        )
+        rank = jnp.sum(onehot * earlier, axis=1, keepdims=True)
+        slot = expert.astype(jnp.float32) * capacity + rank
+        taken = taken + jnp.sum(onehot, axis=0, keepdims=True)
+        table = jnp.where(lane == k, slot, table)
+        table = jnp.where(lane == top_count + k, weight_ref[:, k : k + 1], table)
+    out_ref[...] = table.T[: out_ref.shape[0], :row_count]
+
+
+def fill_slots(top_count, rows_ref, table_ref, *refs):
+    out_ref = refs[-1]
     row_count, width = rows_ref.shape
     step = min(512, width)
-    slots = lax.broadcasted_iota(jnp.int32, (out_ref.shape[0], row_count), 0).astype(jnp.float32)
-    hit = slots == target_ref[0:1, :]
-    for k in range(1, target_ref.shape[0]):
-        hit = hit | (slots == target_ref[k : k + 1, :])
+    slot_count = out_ref.shape[0]
+    slots = lax.broadcasted_iota(jnp.int32, (slot_count, row_count), 0)
+    slots = (slots + lax.axis_index("hf") * slot_count).astype(jnp.float32)
+    hit = slots == table_ref[0:1, :]
+    for k in range(1, top_count):
+        hit = hit | (slots == table_ref[k : k + 1, :])
     placing = jnp.where(hit, 1.0, 0.0).astype(jnp.bfloat16)
     for at in range(0, width, step):
         cols = slice(at, at + step)
@@ -266,15 +313,17 @@
         ).astype(jnp.bfloat16)
 
 
-def gather_kernel(base_count, *refs):
+def gather_kernel(base_count, top_count, *refs):
     bases = refs[:base_count]
-    slots_ref, target_ref, weight_ref, out_ref = refs[base_count:]
+    slots_ref, table_ref, out_ref = refs[base_count:]
     row_count, width = out_ref.shape
+    slot_count = slots_ref.shape[0]
     step = min(512, width)
-    slots = lax.broadcasted_iota(jnp.int32, (row_count, slots_ref.shape[0]), 1).astype(jnp.float32)
-    top_count = target_ref.shape[1]
+    table = table_ref[...].T
+    slots = lax.broadcasted_iota(jnp.int32, (row_count, slot_count), 1)
+    slots = (slots + lax.axis_index("hf") * slot_count).astype(jnp.float32)
     picks = [
-        jnp.where(slots == target_ref[:, k : k + 1], 1.0, 0.0).astype(jnp.bfloat16)
+        jnp.where(slots == table[:, k : k + 1], 1.0, 0.0).astype(jnp.bfloat16)
         for k in range(top_count)
     ]
     for at in range(0, width, step):
@@ -285,29 +334,33 @@
             total = piece if total is None else total + piece
         for k in range(top_count):
             row = jnp.dot(picks[k], slots_ref[:, cols], preferred_element_type=jnp.float32)
-            row = row * weight_ref[:, k : k + 1]
+            row = row * table[:, top_count + k : top_count + k + 1]
             total = row if total is None else total + row
         out_ref[:, cols] = total.astype(out_ref.dtype)
 
 
-def expert_kernel(rows_ref, gate_ref, up_ref, down_ref, out_ref, act_ref):
-    hidden = gate_ref.shape[1]
-    width = down_ref.shape[1]
-    step = min(256, hidden)
-    for at in range(0, hidden, step):
-        cols = slice(at, at + step)
-        gate = jnp.dot(rows_ref[...], gate_ref[:, cols], preferred_element_type=jnp.float32)
-        up = jnp.dot(rows_ref[...], up_ref[:, cols], preferred_element_type=jnp.float32)
-        act_ref[:, cols] = (gate / (1.0 + jnp.exp(-gate)) * up).astype(jnp.bfloat16)
-    step = min(512, width)
-    for at in range(0, width, step):
-        cols = slice(at, at + step)
-        out_ref[:, cols] = jnp.dot(
-            act_ref[...], down_ref[:, cols], preferred_element_type=jnp.float32
+def expert_kernel(first_steps, rows_ref, gate_ref, up_ref, down_ref, *refs):
+    out_ref, act_ref = refs[-2:]
+    index = pl.program_id(0)
+    step = gate_ref.shape[1]
+
+    for i in range(first_steps):
+
+        @pl.when(index == i)
+        def _():
+            gate = jnp.dot(rows_ref[...], gate_ref[...], preferred_element_type=jnp.float32)
+            up = jnp.dot(rows_ref[...], up_ref[...], preferred_element_type=jnp.float32)
+            act = gate / (1.0 + jnp.exp(-gate)) * up
+            act_ref[:, i * step : (i + 1) * step] = act.astype(jnp.bfloat16)
+
+    @pl.when(index >= first_steps)
+    def _():
+        out_ref[...] = jnp.dot(
+            act_ref[...], down_ref[...], preferred_element_type=jnp.float32
         ).astype(jnp.bfloat16)
 
 
-def local(
+def layer(
     sp_size,
     tp_size,
     query_proj,
@@ -345,8 +398,23 @@
         cost_estimate=pl.CostEstimate(
             flops=2 * tok_count * 512 * 512, bytes_accessed=1 << 20, transcendentals=0
         ),
-        compiler_params=pltpu.CompilerParams(vmem_limit_bytes=32 * 1024 * 1024),
     )(query_proj, projected_keys, projected_values, cos_table, sin_table)
+
+    row_count = residual.shape[0]
+    top_count = route_expert.shape[1]
+    experts = sp_size * tp_size
+    capacity = max(2, 2 * top_count * row_count // experts)
+    half_slots = experts // 2 * capacity
+    mirror = [(0, 1), (1, 0)]
+    table = pl.pallas_call(
+        functools.partial(routes_kernel, capacity),
+        out_shape=jax.ShapeDtypeStruct((8, row_count), jnp.float32),
+        in_specs=[VMEM] * 2,
+        out_specs=VMEM,
+        cost_estimate=pl.CostEstimate(flops=1 << 22, bytes_accessed=1 << 17, transcendentals=0),
+        compiler_params=pltpu.CompilerParams(vmem_limit_bytes=8 * 1024 * 1024),
+    )(route_expert, route_weight)
+    far_table = lax.ppermute(table, "hf", mirror)
 
     order = list(range(0, sp_size, 2)) + list(range(sp_size - 1, 0, -2))
     ahead = [(order[i], order[(i + 1) % sp_size]) for i in range(sp_size)]
@@ -361,40 +429,21 @@
             from_left, from_right = from_left[: halves // 2], from_right[halves // 2 :]
         next_left = lax.ppermute(from_left, SP, ahead)
         next_right = lax.ppermute(from_right, SP, behind)
-        acc = attend(q_ready, held, acc)
+        if step == steps - 1:
+            acc, staged_weight = attend(
+                q_ready, held, acc, staged=out_weight, after=far_table
+            )
+        else:
+            acc = attend(q_ready, held, acc)
         from_left, from_right = next_left, next_right
         held = [from_left, from_right]
     pieces = attend(q_ready, held, acc, tp_size)
     blocks = hypercube_exchange(pieces, tp_size)
 
-    row_count = residual.shape[0]
-    top_count = route_expert.shape[1]
-    experts = sp_size * tp_size
-    capacity = max(2, 2 * top_count * row_count // experts)
-    slots_total = experts * capacity
-    flat_expert = route_expert.T.reshape(-1)
-    onehot = flat_expert[:, None] == jnp.arange(experts, dtype=jnp.int32)[None, :]
-    pairs = flat_expert.shape[0]
-    before = (
-        jnp.arange(pairs, dtype=jnp.int32)[None, :] < jnp.arange(pairs, dtype=jnp.int32)[:, None]
-    ).astype(jnp.bfloat16)
-    earlier = jnp.dot(before, onehot.astype(jnp.bfloat16), preferred_element_type=jnp.float32)
-    slot_rank = jnp.sum(jnp.where(onehot, earlier, 0.0), axis=1).astype(jnp.int32)
-    half_slots = slots_total // 2
-    target = (flat_expert * capacity + slot_rank).astype(jnp.float32)
-    target = target.reshape(top_count, row_count)
-    first_slot = (lax.axis_index("hf") * half_slots).astype(jnp.float32)
-    mirror = [(0, 1), (1, 0)]
-    with jax.named_scope("tables"):
-        far = lax.ppermute(jnp.concatenate([target, route_weight.T], axis=0), "hf", mirror)
-    far_target = far[:top_count] - first_slot
-    far_weight = far[top_count:].T
-    own_target = target - first_slot
-
     rows_shape = jax.ShapeDtypeStruct((row_count, model_width), jnp.bfloat16)
     slots_shape = jax.ShapeDtypeStruct((half_slots, model_width), jnp.bfloat16)
     stream, normed, own_out = pl.pallas_call(
-        functools.partial(out_kernel, tp_size),
+        functools.partial(out_kernel, tp_size, top_count),
         out_shape=(rows_shape, rows_shape, slots_shape),
         in_specs=[VMEM] * (tp_size + 5),
         out_specs=(VMEM, VMEM, VMEM),
@@ -405,34 +454,51 @@
             transcendentals=0,
         ),
         compiler_params=pltpu.CompilerParams(vmem_limit_bytes=12 * 1024 * 1024),
-    )(*blocks, out_weight, residual, mix_gain[None, :], norm_gain[None, :], own_target)
+    )(*blocks, staged_weight, residual, mix_gain[None, :], norm_gain[None, :], table)
 
     def exchange(slots):
         blocks = slots.reshape(experts // 2, capacity, model_width)
         blocks = lax.all_to_all(blocks, HALF, split_axis=0, concat_axis=0, tiled=True)
         return blocks.reshape(half_slots, model_width)
 
-    def expert(slots):
+    def expert(slots, after):
         hidden = expert_gate.shape[2]
+        step = min(256, hidden)
+        first_steps = hidden // step
+        out_step = min(512, model_width)
         return pl.pallas_call(
-            expert_kernel,
+            functools.partial(expert_kernel, first_steps),
             out_shape=slots_shape,
-            in_specs=[VMEM] * 4,
-            out_specs=VMEM,
+            grid=(first_steps + model_width // out_step,),
+            in_specs=[
+                pl.BlockSpec((half_slots, model_width), lambda i: (0, 0)),
+                pl.BlockSpec(
+                    (None, model_width, step), lambda i: (0, 0, jnp.minimum(i, first_steps - 1))
+                ),
+                pl.BlockSpec(
+                    (None, model_width, step), lambda i: (0, 0, jnp.minimum(i, first_steps - 1))
+                ),
+                pl.BlockSpec(
+                    (None, hidden, out_step), lambda i: (0, 0, jnp.maximum(i - first_steps, 0))
+                ),
+            ]
+            + [HBM] * len(after),
+            out_specs=pl.BlockSpec(
+                (half_slots, out_step), lambda i: (0, jnp.maximum(i - first_steps, 0))
+            ),
             scratch_shapes=[pltpu.VMEM((half_slots, hidden), jnp.bfloat16)],
             cost_estimate=pl.CostEstimate(
                 flops=6 * half_slots * model_width * hidden,
                 bytes_accessed=14 << 20,
                 transcendentals=half_slots * hidden,
             ),
-            compiler_params=pltpu.CompilerParams(vmem_limit_bytes=16 * 1024 * 1024),
-        )(slots, expert_gate[0], expert_up[0], expert_down[0])
-
-    def gather(bases, slots, target, weight):
+        )(slots, expert_gate, expert_up, expert_down, *after)
+
+    def gather(bases, slots, table):
         return pl.pallas_call(
-            functools.partial(gather_kernel, len(bases)),
+            functools.partial(gather_kernel, len(bases), top_count),
             out_shape=rows_shape,
-            in_specs=[VMEM] * (len(bases) + 3),
+            in_specs=[VMEM] * (len(bases) + 2),
             out_specs=VMEM,
             cost_estimate=pl.CostEstimate(
                 flops=4 * row_count * half_slots * model_width,
@@ -440,16 +506,14 @@
                 transcendentals=0,
             ),
             compiler_params=pltpu.CompilerParams(vmem_limit_bytes=12 * 1024 * 1024),
-        )(*bases, slots, target.T, weight)
-
-    with jax.named_scope("mirror_out"):
-        far_rows = lax.ppermute(normed, "hf", mirror)
-    with jax.named_scope("own_out"):
-        own_in = exchange(own_out)
+        )(*bases, slots, table)
+
+    far_rows = lax.ppermute(normed, "hf", mirror)
+    own_in = exchange(own_out)
     far_out = pl.pallas_call(
-        fill_slots,
+        functools.partial(fill_slots, top_count),
         out_shape=slots_shape,
-        in_specs=[VMEM] * 2,
+        in_specs=[VMEM] * 2 + [HBM],
         out_specs=VMEM,
         cost_estimate=pl.CostEstimate(
             flops=2 * row_count * half_slots * model_width,
@@ -457,26 +521,22 @@
             transcendentals=0,
         ),
         compiler_params=pltpu.CompilerParams(vmem_limit_bytes=12 * 1024 * 1024),
-    )(far_rows, far_target)
-    with jax.named_scope("far_out"):
-        far_in = exchange(far_out)
-    own_done = expert(own_in)
-    far_done = expert(far_in)
-    with jax.named_scope("far_back"):
-        far_answer = exchange(far_done)
-    far_sum = gather([], far_answer, far_target, far_weight)
-    with jax.named_scope("mirror_back"):
-        returned = lax.ppermute(far_sum, "hf", mirror)
-    with jax.named_scope("own_back"):
-        own_answer = exchange(own_done)
-    return gather([stream, returned], own_answer, own_target, route_weight)
+    )(far_rows, far_table, own_in)
+    far_in = exchange(far_out)
+    own_done = expert(own_in, [])
+    far_done = expert(far_in, [own_done])
+    far_answer = exchange(far_done)
+    far_sum = gather([], far_answer, far_table)
+    returned = lax.ppermute(far_sum, "hf", mirror)
+    own_answer = exchange(own_done)
+    return gather([stream, returned], own_answer, table)
 
 
 def solution(mesh):
     sp_size, tp_size = mesh.shape["sp"], mesh.shape["tp"]
     split = Mesh(mesh.devices.reshape(2, sp_size // 2, tp_size), ALL)
     return jax.shard_map(
-        functools.partial(local, sp_size, tp_size),
+        functools.partial(layer, sp_size, tp_size),
         mesh=split,
         in_specs=(
             P(SP, "tp"),

time: 168 us -> 164 us (0.976)
  Pallas kernels: 22.5 us -> 39.5 us
  local copies, waits for them, and re-layouts: 19.3 us -> 4.58 us
  waiting for transfers between devices: 77.4 us -> 69.9 us
    pallas_call x12 -> x13, Pallas kernels: 22.5 us -> 39.5 us  [the longest x2 21.6 us: expert(): pl.pallas_call(functools.partial(expert_kernel, first_steps), out_shape=s...]
    unnamed x30 -> x18, local copies, waits for them, and re-layouts: 19 us -> 4.55 us
    ppermute x11, waiting for transfers between devices: 38.7 us -> 31.7 us  [the longest x1 22 us: layer(): far_rows = lax.ppermute(normed, 'hf', mirror)]
  transfers between devices with their start and end apart: 17 -> 17, of which waited for: 11 -> 10; matrix products, arithmetic and copies ran while one was open for 1% -> 1% of each run, Pallas kernels for 10% -> 12%
where the time goes in v4:
time: 164 us; the launch traced here: 163 us
  waiting for transfers between devices  69.9 us (43%)
  Pallas kernels  39.5 us (24%)
  starting transfers between devices  28.6 us (17%)
  blocking collectives  19.7 us (12%)
  local copies, waits for them, and re-layouts  4.58 us (3%)
    all_to_all x3, waiting for transfers between devices, exchange(): lax.all_to_all(blocks, HALF, split_axis=0, concat_axis=0, tiled=True)  33.5 us
    ppermute x1, waiting for transfers between devices, layer(): far_rows = lax.ppermute(normed, 'hf', mirror)  22 us
    pallas_call x2, Pallas kernels, expert(): pl.pallas_call(functools.partial(expert_kernel, first_steps), out_shape=s...  21.6 us
    all_to_all x1, blocking collectives, exchange(): lax.all_to_all(blocks, HALF, split_axis=0, concat_axis=0, tiled=True)  19.7 us
    all_to_all x3, starting transfers between devices, exchange(): lax.all_to_all(blocks, HALF, split_axis=0, concat_axis=0, tiled=True)  11.2 us
    ppermute x4, starting transfers between devices, layer(): next_left = lax.ppermute(from_left, SP, ahead)  8.19 us
    pallas_call x5, Pallas kernels, attend(): pl.pallas_call(functools.partial(attend_kernel, len(chunks), first, last,...  8.07 us
    ppermute x4, waiting for transfers between devices, layer(): next_left = lax.ppermute(from_left, SP, ahead)  8.01 us
  transfers between devices with their start and end apart: 17, of which 10 were waited for; matrix products, arithmetic and copies ran while one was open for 1% of the time, Pallas kernels for 12%

profile of v4, /device:TPU:0, one launch (start us, length us, event | category | flops | bytes accessed | tf_op | source)
XLA Modules:
  0.0 163.4 jit_solution(10695432471846464796)
XLA Ops:
  0.9 3.3 %shard_map.118 = (bf16[128,2048]{1,0:T(8,128)(2,1)}, bf16[2,512,128]{2,1,0:T(8,128)(2,1)}) custom-call(bf16[512,256]{1,0:T(8,128)(2,1)} %q_hbm.1, bf16[512,128]{1,0:T(8,128)(2,1)} %k_hbm.1, bf16[512,128]{1,0:T(8,128)(2,1)} %v_hbm.1, f32[72,128]{1,0:T(8,128)} %get-tuple-element.28.cos_ref, f32[72,128]{1,0:T(8,128)} %get-tuple-element.27.sin_ref), custom_call_target="tpu_custom_call" | custom-call | flops 268435456 | bytes 1048576 | tf_op jit(solution)/shard_map/pallas_call | solution.py:384
  4.2 3.1 %collective-permute-start = (bf16[2,512,128]{2,1,0:T(8,128)(2,1)}, bf16[2,512,128]{2,1,0:T(8,128)(2,1)S(1)}, u32[]{:S(2)}, u32[]{:S(2)}) collective-permute-start(bf16[2,512,128]{2,1,0:T(8,128)(2,1)} %get-tuple-element.16.refs_1_), channel_id=1, source_target_pairs={{0,8},{8,16},{16,24},{24,28},{28,20},{20,12},{12,4},{4,0},{1,9},{9... | collective-permute-start | bytes 786440 | tf_op jit(solution)/shard_map/ppermute | solution.py:430
  7.3 6.4 %collective-permute-done.refs_1_ = bf16[2,512,128]{2,1,0:T(8,128)(2,1)S(1)} collective-permute-done((bf16[2,512,128]{2,1,0:T(8,128)(2,1)}, bf16[2,512,128]{2,1,0:T(8,128)(2,1)S(1)}, u32[]{:S(2)}, u32[]{:S(2)}) %collective-permute-start) | collective-permute-done | bytes 262176 | tf_op jit(solution)/shard_map/ppermute | solution.py:430
  13.7 1.8 %collective-permute-start.1 = (bf16[2,512,128]{2,1,0:T(8,128)(2,1)S(1)}, bf16[2,512,128]{2,1,0:T(8,128)(2,1)S(1)}, u32[]{:S(2)}, u32[]{:S(2)}) collective-permute-start(bf16[2,512,128]{2,1,0:T(8,128)(2,1)S(1)} %collective-permute-done.refs_1_), channel_id=1, source_target_pairs={{0,8},{8,16},{16,24},{24,28},{28,20},{20,12},{12,4},{4,0},{1,9},{9... | collective-permute-start | bytes 786440 | tf_op jit(solution)/shard_map/ppermute | solution.py:430
  17.8 2.9 %collective-permute-start.8 = (f32[8,128]{1,0:T(8,128)S(1)}, f32[8,128]{1,0:T(8,128)S(1)}, u32[]{:S(2)}, u32[]{:S(2)}) collective-permute-start(f32[8,128]{1,0:T(8,128)S(1)} %shard_map.122.refs_8_.refs_3_), channel_id=1, source_target_pairs={{0,16},{16,0},{1,17},{17,1},{2,18},{18,2},{3,19},{19,3},{4,20},{20... | collective-permute-start | bytes 12296 | tf_op jit(solution)/shard_map/ppermute | solution.py:417
  23.7 1.6 collective-permute-start.2
  25.8 1.9 %shard_map.120.refs_3_ = f32[80,2048]{1,0:T(8,128)S(1)} custom-call(bf16[128,2048]{1,0:T(8,128)(2,1)S(1)} %copy-done.6, bf16[2,512,128]{2,1,0:T(8,128)(2,1)S(1)} %collective-permute-done.refs_1_, bf16[2,512,128]{2,1,0:T(8,128)(2,1)S(1)} %collective-permute-done.4.refs_2_, f32[80,2048]{1,0:T(8,128)S(1)} %shard_map.119.refs_3_), custom_call_target="tpu_custom_call", output_to_operand_aliasing={{}: (3, {})} | custom-call | flops 2147483648 | bytes 1048576 | tf_op jit(solution)/shard_map/pallas_call | solution.py:202
  27.7 1.9 %shard_map.121.refs_3_ = f32[80,2048]{1,0:T(8,128)S(1)} custom-call(bf16[128,2048]{1,0:T(8,128)(2,1)S(1)} %copy-done.6, bf16[2,512,128]{2,1,0:T(8,128)(2,1)S(1)} %collective-permute-done.1.refs_1_, bf16[2,512,128]{2,1,0:T(8,128)(2,1)S(1)} %collective-permute-done.5.refs_2_, f32[80,2048]{1,0:T(8,128)S(1)} %shard_map.120.refs_3_), custom_call_target="tpu_custom_call", output_to_operand_aliasing={{}: (3, {})} | custom-call | flops 2147483648 | bytes 1048576 | tf_op jit(solution)/shard_map/pallas_call | solution.py:202
  32.7 2.2 %shard_map.123 = (f32[80,2048]{1,0:T(8,128)S(1)}, bf16[1024,2048]{1,0:T(8,128)(2,1)S(1)}) custom-call(bf16[128,2048]{1,0:T(8,128)(2,1)S(1)} %copy-done.6, bf16[2,512,128]{2,1,0:T(8,128)(2,1)S(1)} %collective-permute-done.2.refs_1_, bf16[2,512,128]{2,1,0:T(8,128)(2,1)S(1)} %collective-permute-done.6.refs_2_, ...), custom_call_target="tpu_custom_call", output_to_operand_aliasing={{0}: (3, {})} | custom-call | flops 2147483648 | bytes 1048576 | tf_op jit(solution)/shard_map/pallas_call | solution.py:202
  35.5 1.7 %collective-permute-done.7.refs_2_ = bf16[1,512,128]{2,1,0:T(8,128)(2,1)S(1)} collective-permute-done((bf16[1,512,128]{2,1,0:T(8,128)(2,1)S(1)}, bf16[1,512,128]{2,1,0:T(8,128)(2,1)S(1)}, u32[]{:S(2)}, u32[]{:S(2)}) %collective-permute-start.7) | collective-permute-done | bytes 131104 | tf_op jit(solution)/shard_map/ppermute | solution.py:431
  39.9 3.4 %collective-permute-done.10 = bf16[2,256,128]{2,1,0:T(8,128)(2,1)S(1)} collective-permute-done((bf16[2,256,128]{2,1,0:T(8,128)(2,1)S(1)}, bf16[2,256,128]{2,1,0:T(8,128)(2,1)S(1)}, u32[]{:S(2)}, u32[]{:S(2)}) %collective-permute-start.10) | collective-permute-done | bytes 131104 | tf_op jit(solution)/shard_map/ppermute | solution.py:226
  44.7 2.6 %shard_map.125 = (bf16[128,2048]{1,0:T(8,128)(2,1)S(1)}, bf16[128,2048]{1,0:T(8,128)(2,1)S(1)}, bf16[256,2048]{1,0:T(8,128)(2,1)}) custom-call(bf16[1,256,128]{2,1,0:T(8,128)(2,1)S(1)} %get-tuple-element.18.refs_0_, bf16[1,256,128]{2,1,0:T(8,128)(2,1)S(1)} %collective-permute-done.9.refs_1_, bf16[1,256,128]{2,1,0:T(8,128)(2,1)S(1)} %get-tuple-element.26.refs_2_, ...), custom_call_target="tpu_custom_call" | custom-call | flops 671088640 | bytes 8388608 | tf_op jit(solution)/shard_map/pallas_call | solution.py:445
  47.4 3.7 %all-to-all-start = ((bf16[16,16,2048]{2,1,0:T(8,128)(2,1)}), bf16[16,16,2048]{2,1,0:T(8,128)(2,1)S(1)}, u32[]{:S(2)}, u32[]{:S(2)}) async-start(bf16[16,16,2048]{2,1,0:T(8,128)(2,1)} %bitcast.2), calls=%async_computation | async-start | bytes 2097152 | tf_op jit(solution)/shard_map/all_to_all | solution.py:461
  51.1 1.6 %collective-permute-start.12 = (bf16[128,2048]{1,0:T(8,128)(2,1)S(1)}, bf16[128,2048]{1,0:T(8,128)(2,1)S(1)}, u32[]{:S(2)}, u32[]{:S(2)}) collective-permute-start(bf16[128,2048]{1,0:T(8,128)(2,1)S(1)} %get-tuple-element.23), channel_id=1, source_target_pairs={{0,16},{16,0},{1,17},{17,1},{2,18},{18,2},{3,19},{19,3},{4,20},{20... | collective-permute-start | bytes 1572872 | tf_op jit(solution)/shard_map/ppermute | solution.py:511
  52.7 22.0 %collective-permute-done.12.rows_ref = bf16[128,2048]{1,0:T(8,128)(2,1)S(1)} collective-permute-done((bf16[128,2048]{1,0:T(8,128)(2,1)S(1)}, bf16[128,2048]{1,0:T(8,128)(2,1)S(1)}, u32[]{:S(2)}, u32[]{:S(2)}) %collective-permute-start.12) | collective-permute-done | bytes 524320 | tf_op jit(solution)/shard_map/ppermute | solution.py:511
  74.8 3.7 %all-to-all-done = bf16[16,16,2048]{2,1,0:T(8,128)(2,1)S(1)} async-done(((bf16[16,16,2048]{2,1,0:T(8,128)(2,1)}), bf16[16,16,2048]{2,1,0:T(8,128)(2,1)S(1)}, u32[]{:S(2)}, u32[]{:S(2)}) %all-to-all-start) | async-done | bytes 1048608 | tf_op jit(solution)/shard_map/all_to_all | solution.py:461
  79.9 3.8 %all-to-all-start.1 = ((bf16[16,16,2048]{2,1,0:T(8,128)(2,1)}), bf16[16,16,2048]{2,1,0:T(8,128)(2,1)S(1)}, u32[]{:S(2)}, u32[]{:S(2)}) async-start(bf16[16,16,2048]{2,1,0:T(8,128)(2,1)} %bitcast.4), calls=%async_computation.1 | async-start | bytes 2097152 | tf_op jit(solution)/shard_map/all_to_all | solution.py:461
  83.7 10.8 %shard_map.127.refs_0_ = bf16[256,2048]{1,0:T(8,128)(2,1)} custom-call(bf16[256,2048]{1,0:T(8,128)(2,1)} %bitcast.11, bf16[1,2048,1024]{2,1,0:T(8,128)(2,1)} %gate_ref.3, bf16[1,2048,1024]{2,1,0:T(8,128)(2,1)} %up_ref.3, bf16[1,1024,2048]{2,1,0:T(8,128)(2,1)} %down_ref.3), custom_call_target="tpu_custom_call" | custom-call | flops 3221225472 | bytes 14680064 | tf_op jit(solution)/shard_map/pallas_call | solution.py:469
  94.6 5.1 %all-to-all-done.1 = bf16[16,16,2048]{2,1,0:T(8,128)(2,1)S(1)} async-done(((bf16[16,16,2048]{2,1,0:T(8,128)(2,1)}), bf16[16,16,2048]{2,1,0:T(8,128)(2,1)S(1)}, u32[]{:S(2)}, u32[]{:S(2)}) %all-to-all-start.1) | async-done | bytes 1048608 | tf_op jit(solution)/shard_map/all_to_all | solution.py:461
  100.6 10.8 %shard_map.128 = bf16[256,2048]{1,0:T(8,128)(2,1)} custom-call(bf16[256,2048]{1,0:T(8,128)(2,1)} %bitcast.17, bf16[1,2048,1024]{2,1,0:T(8,128)(2,1)} %gate_ref.3, bf16[1,2048,1024]{2,1,0:T(8,128)(2,1)} %up_ref.3, bf16[1,1024,2048]{2,1,0:T(8,128)(2,1)} %down_ref.3, bf16[256,2048]{1,0:T(8,128)(2,1)} %shard_map.127.refs_0_), custom_call_target="tpu_custom_call" | custom-call | flops 3221225472 | bytes 14680064 | tf_op jit(solution)/shard_map/pallas_call | solution.py:469
  111.5 19.7 %all_to_all.20 = bf16[16,16,2048]{2,1,0:T(8,128)(2,1)S(1)} all-to-all(bf16[16,16,2048]{2,1,0:T(8,128)(2,1)} %bitcast.18), channel_id=1, replica_groups=mesh['hf'=2,'q'=4,'tp'=4] {'q','tp'}, dimensions={0} | all-to-all | bytes 2097152 | tf_op jit(solution)/shard_map/all_to_all | solution.py:461
  131.2 3.7 %all-to-all-start.3 = ((bf16[16,16,2048]{2,1,0:T(8,128)(2,1)}), bf16[16,16,2048]{2,1,0:T(8,128)(2,1)S(1)}, u32[]{:S(2)}, u32[]{:S(2)}) async-start(bf16[16,16,2048]{2,1,0:T(8,128)(2,1)} %bitcast.16), calls=%async_computation.3 | async-start | bytes 2097152 | tf_op jit(solution)/shard_map/all_to_all | solution.py:461
  135.4 1.9 %collective-permute-start.13 = (bf16[128,2048]{1,0:T(8,128)(2,1)S(1)}, bf16[128,2048]{1,0:T(8,128)(2,1)S(1)}, u32[]{:S(2)}, u32[]{:S(2)}) collective-permute-start(bf16[128,2048]{1,0:T(8,128)(2,1)S(1)} %shard_map.129), channel_id=1, source_target_pairs={{0,16},{16,0},{1,17},{17,1},{2,18},{18,2},{3,19},{19,3},{4,20},{20... | collective-permute-start | bytes 1572872 | tf_op jit(solution)/shard_map/ppermute | solution.py:530
  137.3 24.7 %all-to-all-done.3 = bf16[16,16,2048]{2,1,0:T(8,128)(2,1)S(1)} async-done(((bf16[16,16,2048]{2,1,0:T(8,128)(2,1)}), bf16[16,16,2048]{2,1,0:T(8,128)(2,1)S(1)}, u32[]{:S(2)}, u32[]{:S(2)}) %all-to-all-start.3) | async-done | bytes 1048608 | tf_op jit(solution)/shard_map/all_to_all | solution.py:461
  (48 shorter events, 18.8 us)
Async XLA Ops:
  4.2 9.5 %collective-permute-start = (bf16[2,512,128]{2,1,0:T(8,128)(2,1)}, bf16[2,512,128]{2,1,0:T(8,128)(2,1)S(1)}, u32[]{:S(2)}, u32[]{:S(2)}) collective-permute-start(bf16[2,512,128]{2,1,0:T(8,128)(2,1)} %get-tuple-element.16.refs_1_), channel_id=1, source_target_pairs={{0,8},{8,16},{16,24},{24,28},{28,20},{20,12},{12,4},{4,0},{1,9},{9... | collective-permute-start | bytes 786440 | tf_op jit(solution)/shard_map/ppermute | solution.py:430
  7.3 8.3 %collective-permute-start.4 = (bf16[2,512,128]{2,1,0:T(8,128)(2,1)}, bf16[2,512,128]{2,1,0:T(8,128)(2,1)S(1)}, u32[]{:S(2)}, u32[]{:S(2)}) collective-permute-start(bf16[2,512,128]{2,1,0:T(8,128)(2,1)} %get-tuple-element.16.refs_1_), channel_id=1, source_target_pairs={{8,0},{16,8},{24,16},{28,24},{20,28},{12,20},{4,12},{0,4},{9,1},{1... | collective-permute-start | bytes 786440 | tf_op jit(solution)/shard_map/ppermute | solution.py:431
  13.7 10.0 %collective-permute-start.1 = (bf16[2,512,128]{2,1,0:T(8,128)(2,1)S(1)}, bf16[2,512,128]{2,1,0:T(8,128)(2,1)S(1)}, u32[]{:S(2)}, u32[]{:S(2)}) collective-permute-start(bf16[2,512,128]{2,1,0:T(8,128)(2,1)S(1)} %collective-permute-done.refs_1_), channel_id=1, source_target_pairs={{0,8},{8,16},{16,24},{24,28},{28,20},{20,12},{12,4},{4,0},{1,9},{9... | collective-permute-start | bytes 786440 | tf_op jit(solution)/shard_map/ppermute | solution.py:430
  15.6 9.8 %collective-permute-start.5 = (bf16[2,512,128]{2,1,0:T(8,128)(2,1)S(1)}, bf16[2,512,128]{2,1,0:T(8,128)(2,1)S(1)}, u32[]{:S(2)}, u32[]{:S(2)}) collective-permute-start(bf16[2,512,128]{2,1,0:T(8,128)(2,1)S(1)} %collective-permute-done.4.refs_2_), channel_id=1, source_target_pairs={{8,0},{16,8},{24,16},{28,24},{20,28},{12,20},{4,12},{0,4},{9,1},{1... | collective-permute-start | bytes 786440 | tf_op jit(solution)/shard_map/ppermute | solution.py:431
  17.8 14.9 %collective-permute-start.8 = (f32[8,128]{1,0:T(8,128)S(1)}, f32[8,128]{1,0:T(8,128)S(1)}, u32[]{:S(2)}, u32[]{:S(2)}) collective-permute-start(f32[8,128]{1,0:T(8,128)S(1)} %shard_map.122.refs_8_.refs_3_), channel_id=1, source_target_pairs={{0,16},{16,0},{1,17},{17,1},{2,18},{18,2},{3,19},{19,3},{4,20},{20... | collective-permute-start | bytes 12296 | tf_op jit(solution)/shard_map/ppermute | solution.py:417
  21.6 1.0 copy-start.6
  23.7 6.8 %collective-permute-start.2 = (bf16[2,512,128]{2,1,0:T(8,128)(2,1)S(1)}, bf16[2,512,128]{2,1,0:T(8,128)(2,1)S(1)}, u32[]{:S(2)}, u32[]{:S(2)}) collective-permute-start(bf16[2,512,128]{2,1,0:T(8,128)(2,1)S(1)} %collective-permute-done.1.refs_1_), channel_id=1, source_target_pairs={{0,8},{8,16},{16,24},{24,28},{28,20},{20,12},{12,4},{4,0},{1,9},{9... | collective-permute-start | bytes 786440 | tf_op jit(solution)/shard_map/ppermute | solution.py:430
  25.4 6.8 %collective-permute-start.6 = (bf16[2,512,128]{2,1,0:T(8,128)(2,1)S(1)}, bf16[2,512,128]{2,1,0:T(8,128)(2,1)S(1)}, u32[]{:S(2)}, u32[]{:S(2)}) collective-permute-start(bf16[2,512,128]{2,1,0:T(8,128)(2,1)S(1)} %collective-permute-done.5.refs_2_), channel_id=1, source_target_pairs={{8,0},{16,8},{24,16},{28,24},{20,28},{12,20},{4,12},{0,4},{9,1},{1... | collective-permute-start | bytes 786440 | tf_op jit(solution)/shard_map/ppermute | solution.py:431
  27.7 5.0 %copy-start.4 = (bf16[1024,2048]{1,0:T(8,128)(2,1)S(1)}, bf16[1024,2048]{1,0:T(8,128)(2,1)}, u32[]{:S(2)}) copy-start(bf16[1024,2048]{1,0:T(8,128)(2,1)} %refs_5_.2) | copy-start | bytes 12582916
  30.5 5.0 %collective-permute-start.3 = (bf16[1,512,128]{2,1,0:T(8,128)(2,1)S(1)}, bf16[1,512,128]{2,1,0:T(8,128)(2,1)S(1)}, u32[]{:S(2)}, u32[]{:S(2)}) collective-permute-start(bf16[1,512,128]{2,1,0:T(8,128)(2,1)S(1)} %slice.16), channel_id=1, source_target_pairs={{0,8},{8,16},{16,24},{24,28},{28,20},{20,12},{12,4},{4,0},{1,9},{9... | collective-permute-start | bytes 393224 | tf_op jit(solution)/shard_map/ppermute | solution.py:430
  32.2 12.5 %copy-start.1 = (bf16[128,2048]{1,0:T(8,128)(2,1)S(1)}, bf16[128,2048]{1,0:T(8,128)(2,1)}, u32[]{:S(2)}) copy-start(bf16[128,2048]{1,0:T(8,128)(2,1)} %refs_5_.3) | copy-start | bytes 1572868
  32.2 12.5 %copy-start.2 = (f32[2048]{0:T(1024)S(1)}, f32[2048]{0:T(1024)}, u32[]{:S(2)}) copy-start(f32[2048]{0:T(1024)} %param.17) | copy-start | bytes 24580
  32.2 12.5 %copy-start.3 = (f32[2048]{0:T(1024)S(1)}, f32[2048]{0:T(1024)}, u32[]{:S(2)}) copy-start(f32[2048]{0:T(1024)} %param.18) | copy-start | bytes 24580
  32.2 5.0 %collective-permute-start.7 = (bf16[1,512,128]{2,1,0:T(8,128)(2,1)S(1)}, bf16[1,512,128]{2,1,0:T(8,128)(2,1)S(1)}, u32[]{:S(2)}, u32[]{:S(2)}) collective-permute-start(bf16[1,512,128]{2,1,0:T(8,128)(2,1)S(1)} %slice.17), channel_id=1, source_target_pairs={{8,0},{16,8},{24,16},{28,24},{20,28},{12,20},{4,12},{0,4},{9,1},{1... | collective-permute-start | bytes 393224 | tf_op jit(solution)/shard_map/ppermute | solution.py:431
  38.3 5.0 %collective-permute-start.10 = (bf16[2,256,128]{2,1,0:T(8,128)(2,1)S(1)}, bf16[2,256,128]{2,1,0:T(8,128)(2,1)S(1)}, u32[]{:S(2)}, u32[]{:S(2)}) collective-permute-start(bf16[2,256,128]{2,1,0:T(8,128)(2,1)S(1)} %get-tuple-element.20), channel_id=1, source_target_pairs={{0,2},{1,3},{2,0},{3,1},{4,6},{5,7},{6,4},{7,5},{8,10},{9,11},{10,... | collective-permute-start | bytes 393224 | tf_op jit(solution)/shard_map/ppermute | solution.py:226
  39.9 3.5 %collective-permute-start.9 = (bf16[1,256,128]{2,1,0:T(8,128)(2,1)S(1)}, bf16[1,256,128]{2,1,0:T(8,128)(2,1)S(1)}, u32[]{:S(2)}, u32[]{:S(2)}) collective-permute-start(bf16[1,256,128]{2,1,0:T(8,128)(2,1)S(1)} %get-tuple-element.19), channel_id=1, source_target_pairs={{0,1},{1,0},{2,3},{3,2},{4,5},{5,4},{6,7},{7,6},{8,9},{9,8},{10,11... | collective-permute-start | bytes 196616 | tf_op jit(solution)/shard_map/ppermute | solution.py:226
  43.4 1.3 collective-permute-start.11
  47.4 31.1 %all-to-all-start = ((bf16[16,16,2048]{2,1,0:T(8,128)(2,1)}), bf16[16,16,2048]{2,1,0:T(8,128)(2,1)S(1)}, u32[]{:S(2)}, u32[]{:S(2)}) async-start(bf16[16,16,2048]{2,1,0:T(8,128)(2,1)} %bitcast.2), calls=%async_computation | async-start | bytes 2097152 | tf_op jit(solution)/shard_map/all_to_all | solution.py:461
  51.1 23.7 %collective-permute-start.12 = (bf16[128,2048]{1,0:T(8,128)(2,1)S(1)}, bf16[128,2048]{1,0:T(8,128)(2,1)S(1)}, u32[]{:S(2)}, u32[]{:S(2)}) collective-permute-start(bf16[128,2048]{1,0:T(8,128)(2,1)S(1)} %get-tuple-element.23), channel_id=1, source_target_pairs={{0,16},{16,0},{1,17},{17,1},{2,18},{18,2},{3,19},{19,3},{4,20},{20... | collective-permute-start | bytes 1572872 | tf_op jit(solution)/shard_map/ppermute | solution.py:511
  78.5 5.3 %copy-start = (bf16[16,16,2048]{2,1,0:T(8,128)(2,1)}, bf16[16,16,2048]{2,1,0:T(8,128)(2,1)S(1)}, u32[]{:S(2)}) copy-start(bf16[16,16,2048]{2,1,0:T(8,128)(2,1)S(1)} %all-to-all-done) | copy-start | bytes 3145732
  79.9 19.8 %all-to-all-start.1 = ((bf16[16,16,2048]{2,1,0:T(8,128)(2,1)}), bf16[16,16,2048]{2,1,0:T(8,128)(2,1)S(1)}, u32[]{:S(2)}, u32[]{:S(2)}) async-start(bf16[16,16,2048]{2,1,0:T(8,128)(2,1)} %bitcast.4), calls=%async_computation.1 | async-start | bytes 2097152 | tf_op jit(solution)/shard_map/all_to_all | solution.py:461
  99.7 1.0 copy-start.7
  131.2 30.8 %all-to-all-start.3 = ((bf16[16,16,2048]{2,1,0:T(8,128)(2,1)}), bf16[16,16,2048]{2,1,0:T(8,128)(2,1)S(1)}, u32[]{:S(2)}, u32[]{:S(2)}) async-start(bf16[16,16,2048]{2,1,0:T(8,128)(2,1)} %bitcast.16), calls=%async_computation.3 | async-start | bytes 2097152 | tf_op jit(solution)/shard_map/all_to_all | solution.py:461
  135.4 26.6 %collective-permute-start.13 = (bf16[128,2048]{1,0:T(8,128)(2,1)S(1)}, bf16[128,2048]{1,0:T(8,128)(2,1)S(1)}, u32[]{:S(2)}, u32[]{:S(2)}) collective-permute-start(bf16[128,2048]{1,0:T(8,128)(2,1)S(1)} %shard_map.129), channel_id=1, source_target_pairs={{0,16},{16,0},{1,17},{17,1},{2,18},{18,2},{3,19},{19,3},{4,20},{20... | collective-permute-start | bytes 1572872 | tf_op jit(solution)/shard_map/ppermute | solution.py:530
  (1 other events, 0.9 us)

commit v5 on v2

v5 whole, which is shorter than its diff:
```python
import functools
import math

import jax
import jax.numpy as jnp
from jax import lax
from jax.experimental import pallas as pl
from jax.experimental.pallas import tpu as pltpu
from jax.sharding import PartitionSpec as P

HEAD_SIZE = 64
GRID_W = 64
HALF_KEYS = 256
ONES_ROWS = 16

epsilon = 1e-06
base_theta = 10000.0

VMEM = pl.BlockSpec(memory_space=pltpu.VMEM)
HBM = pl.BlockSpec(memory_space=pltpu.HBM)


def rotation_tables(row_count, lanes):
    quarter = HEAD_SIZE // 4
    lane = jnp.arange(lanes, dtype=jnp.int32) % HEAD_SIZE
    index = jnp.arange(row_count + GRID_W, dtype=jnp.int32)
    place = jnp.where(index < row_count, index, index - row_count)
    frequency = base_theta ** (-(lane % quarter).astype(jnp.float32) / quarter)
    angle = place.astype(jnp.float32)[:, None] * frequency[None, :]
    sign = jnp.where((lane // quarter) % 2 == 0, -1.0, 1.0).astype(jnp.float32)
    return jnp.cos(angle), jnp.sin(angle) * sign[None, :]


def pack_kernel(k_hbm, v_hbm, out_ref, sems):
    halves = out_ref.shape[0]
    copies = [
        pltpu.make_async_copy(
            src.at[pl.ds(half * HALF_KEYS, HALF_KEYS), :], out_ref.at[half, i], sems.at[half, i]
        )
        for half in range(halves)
        for i, src in enumerate((k_hbm, v_hbm))
    ]
    for copy in copies:
        copy.start()
    for copy in copies:
        copy.wait()


class Rotation:
    def __init__(self, cos_ref, sin_ref, lanes):
        rows = lax.broadcasted_iota(jnp.int32, (lanes, lanes), 0)
        cols = lax.broadcasted_iota(jnp.int32, (lanes, lanes), 1)
        same_head = (rows // HEAD_SIZE) == (cols // HEAD_SIZE)
        self.mean_mat = jnp.where(same_head, 1.0 / HEAD_SIZE, 0.0).astype(jnp.bfloat16)
        self.swap_mat = jnp.where((rows ^ (HEAD_SIZE // 4)) == cols, 1.0, 0.0).astype(jnp.bfloat16)
        lane = lax.broadcasted_iota(jnp.int32, (GRID_W, lanes), 1)
        self.by_row = (lane % HEAD_SIZE) < HEAD_SIZE // 2
        self.refs = (cos_ref, sin_ref)

    def table(self, ref, first_row, count):
        total = ref.shape[0] - GRID_W
        cols = ref[total:, :]
        parts = [
            jnp.where(self.by_row, ref[pl.ds(first_row + i, 1), :], cols) for i in range(count)
        ]
        return jnp.concatenate(parts, axis=0)

    def ready(self, raw, first_row, factor):
        count = raw.shape[0] // GRID_W
        cos = self.table(self.refs[0], first_row, count)
        sin = self.table(self.refs[1], first_row, count)
        wide = raw.astype(jnp.float32)
        square = wide * wide
        high = square.astype(jnp.bfloat16)
        low = (square - high.astype(jnp.float32)).astype(jnp.bfloat16)
        mean = jnp.dot(high, self.mean_mat, preferred_element_type=jnp.float32) + jnp.dot(
            low, self.mean_mat, preferred_element_type=jnp.float32
        )
        swapped = jnp.dot(raw, self.swap_mat, preferred_element_type=jnp.float32)
        length = lax.rsqrt(mean + epsilon) * factor
        return (wide * cos + swapped * sin) * length


def ring_place(index, count):
    return jnp.where(index % 2 == 0, index // 2, count - (index + 1) // 2)


def ring_member(place, count):
    place = lax.rem(place + count, count)
    return jnp.where(2 * place < count, 2 * place, 2 * (count - place) - 1)


def attend_kernel(sp_size, pieces, last, raw_queries, after, *refs):
    refs = list(refs)
    first_ref = refs.pop(0)
    cos_ref, sin_ref = refs.pop(0), refs.pop(0)
    chunks = [refs.pop(0) for _ in pieces]
    acc_in = None if raw_queries else refs.pop(0)
    for _ in range(after):
        refs.pop(0)
    outs = [refs.pop(0) for _ in range(2 if raw_queries else 1)] if not last else None
    if last:
        outs, refs = refs[:-3], refs[-3:]
    keys_ref, values_ref = refs[0], refs[1]
    lanes = chunks[0].shape[-1]
    rotation = Rotation(cos_ref, sin_ref, lanes)
    me = lax.axis_index("sp")
    place = ring_place(me, sp_size)
    grid_rows = (cos_ref.shape[0] - GRID_W) // sp_size
    if raw_queries:
        q_ref = outs[0]
        factor = math.log2(math.e) * HEAD_SIZE ** (-0.5)
        tok_count, q_lanes = first_ref.shape
        group = q_lanes // lanes
        q_ref[...] = jnp.zeros_like(q_ref)
        for block in range(group):
            raw = first_ref[:, block * lanes : (block + 1) * lanes]
            turned = rotation.ready(raw, me * grid_rows, factor).T
            for inner in range(lanes // HEAD_SIZE):
                head = block * (lanes // HEAD_SIZE) + inner
                kv_head = head // group
                q_ref[
                    kv_head * HEAD_SIZE : (kv_head + 1) * HEAD_SIZE,
                    head * tok_count : (head + 1) * tok_count,
                ] = turned[inner * HEAD_SIZE : (inner + 1) * HEAD_SIZE].astype(jnp.bfloat16)
    else:
        q_ref = first_ref
    _, columns = q_ref.shape
    width = min(512, columns)
    blocks = columns // width
    kv_heads = lanes // HEAD_SIZE
    ones = jnp.ones((ONES_ROWS, HALF_KEYS), jnp.bfloat16)
    rows = HEAD_SIZE + ONES_ROWS
    halves = 0
    for chunk, (distance, first_half) in zip(chunks, pieces):
        source = ring_member(place + distance, sp_size)
        for half in range(chunk.shape[0]):
            row = source * grid_rows + (first_half + half) * (HALF_KEYS // GRID_W)
            keys_ref[halves] = rotation.ready(chunk[half, 0], row, 1.0).astype(jnp.bfloat16)
            turned = chunk[half, 1].astype(jnp.float32).T.astype(jnp.bfloat16)
            for head in range(kv_heads):
                values_ref[halves, head, :HEAD_SIZE, :] = turned[
                    head * HEAD_SIZE : (head + 1) * HEAD_SIZE
                ]
                values_ref[halves, head, HEAD_SIZE:, :] = ones
            halves += 1
    waiting = None
    for block in range(blocks + 1):
        weights = []
        total = None
        for half in range(halves):
            if block < blocks:
                scores = jnp.dot(
                    keys_ref[half],
                    q_ref[:, block * width : (block + 1) * width],
                    preferred_element_type=jnp.float32,
                )
                weights.append(jnp.exp2(scores).astype(jnp.bfloat16))
            if waiting is not None:
                kv_head = (block - 1) * kv_heads // blocks
                piece = jnp.dot(
                    values_ref[half, kv_head], waiting[half], preferred_element_type=jnp.float32
                )
                total = piece if total is None else total + piece
        if waiting is not None:
            at = (block - 1) * width
            if acc_in is not None:
                total = total + acc_in[:, at : at + width]
            if not last:
                outs[-1][:, at : at + width] = total
            else:
                turn = refs[2]
                tp, head_rows, per = turn.shape
                tok_count = tp * per
                ready = (total[:HEAD_SIZE] / total[HEAD_SIZE : HEAD_SIZE + 1]).astype(jnp.bfloat16)
                for piece in range(width // per):
                    head, spot = divmod(at + piece * per, tok_count)
                    turn[spot // per, head * HEAD_SIZE : (head + 1) * HEAD_SIZE, :] = ready[
                        :, piece * per : (piece + 1) * per
                    ]
        waiting = weights
    if last:
        me = lax.axis_index("tp")
        rel = 0
        for out in outs:
            for j in range(out.shape[0]):
                out[j] = refs[2][me ^ rel]
                rel += 1


def attend(queries, tables, chunks, pieces, acc, sp_size, tp_size, last=False, after=()):
    raw_queries = acc is None
    lanes = chunks[0].shape[-1]
    rows = HEAD_SIZE + ONES_ROWS
    halves = sum(c.shape[0] for c in chunks)
    if raw_queries:
        columns = queries.shape[0] * queries.shape[1] // HEAD_SIZE
        tok_count = queries.shape[0]
    else:
        columns = queries.shape[1]
        tok_count = chunks[0].shape[0] * HALF_KEYS * 2
    scratch = [
        pltpu.VMEM((halves, HALF_KEYS, lanes), jnp.bfloat16),
        pltpu.VMEM((halves, lanes // HEAD_SIZE, rows, HALF_KEYS), jnp.bfloat16),
    ]
    if last:
        head_rows = columns // tok_count * HEAD_SIZE
        block = (head_rows, tok_count // tp_size)
        sizes = [1] + [1 << b for b in range(tp_size.bit_length() - 1)]
        shape = [jax.ShapeDtypeStruct((n, *block), jnp.bfloat16) for n in sizes]
        scratch.append(pltpu.VMEM((tp_size, *block), jnp.bfloat16))
    else:
        shape = [jax.ShapeDtypeStruct((rows, columns), jnp.float32)]
        if raw_queries:
            shape = [jax.ShapeDtypeStruct((lanes, columns), jnp.bfloat16)] + shape
    operands = [queries, *tables, *chunks] + ([] if raw_queries else [acc])
    aliases = {} if (raw_queries or last) else {len(operands) - 1: 0}
    key_count = halves * HALF_KEYS
    return pl.pallas_call(
        functools.partial(attend_kernel, sp_size, pieces, last, raw_queries, len(after)),
        out_shape=shape,
        in_specs=[VMEM] * len(operands) + [HBM] * len(after),
        out_specs=[VMEM] * len(shape),
        scratch_shapes=scratch,
        input_output_aliases=aliases,
        cost_estimate=pl.CostEstimate(
            flops=2 * key_count * columns * 512,
            bytes_accessed=key_count * 1024,
            transcendentals=key_count * columns,
        ),
        compiler_params=pltpu.CompilerParams(vmem_limit_bytes=24 * 1024 * 1024),
    )(*operands, *after)


def hypercube_exchange(pieces, tp_size):
    held = []
    for bit in reversed(range(tp_size.bit_length() - 1)):
        pairs = [(i, i ^ (1 << bit)) for i in range(tp_size)]
        half = 1 << bit
        moved = [(half, lax.ppermute(pieces[1 + bit], "tp", pairs))]
        kept = []
        for source, block in held:
            moved.append((source ^ half, lax.ppermute(block[half:], "tp", pairs)))
            kept.append((source, block[:half]))
        held = kept + moved
    return [pieces[0]] + [block for _, block in sorted(held, key=lambda item: item[0])]


def out_kernel(tp_size, top_count, *refs):
    blocks = refs[:tp_size]
    w_ref, res_ref, mix_ref, norm_ref, table_ref = refs[tp_size : tp_size + 5]
    stream_ref, out_ref, normed_ref, mixed_ref = refs[tp_size + 5 :]
    me = lax.axis_index("tp")
    _, head_rows, row_count = blocks[0].shape
    width = w_ref.shape[1]
    step = min(512, width)
    turned = [b[0].astype(jnp.float32).T.astype(jnp.bfloat16) for b in blocks]
    power = jnp.zeros((row_count, 1), jnp.float32)
    for at in range(0, width, step):
        mixed = jnp.zeros((row_count, step), jnp.float32)
        for rel in range(tp_size):
            begin = pl.multiple_of((me ^ rel) * head_rows, head_rows)
            mixed = mixed + jnp.dot(
                turned[rel],
                w_ref[pl.ds(begin, head_rows), at : at + step],
                preferred_element_type=jnp.float32,
            )
        mixed_ref[:, at : at + step] = mixed
        power = power + jnp.sum(mixed * mixed, axis=1, keepdims=True)
    scale = lax.rsqrt(power / width + epsilon)
    power = jnp.zeros((row_count, 1), jnp.float32)
    for at in range(0, width, step):
        cols = slice(at, at + step)
        stream = (
            res_ref[:, cols].astype(jnp.float32) + mixed_ref[:, cols] * scale * mix_ref[:, cols]
        ).astype(jnp.bfloat16)
        stream_ref[:, cols] = stream
        wide = stream.astype(jnp.float32)
        power = power + jnp.sum(wide * wide, axis=1, keepdims=True)
    scale = lax.rsqrt(power / width + epsilon)
    for at in range(0, width, step):
        cols = slice(at, at + step)
        wide = stream_ref[:, cols].astype(jnp.float32)
        normed_ref[:, cols] = (wide * scale * norm_ref[:, cols]).astype(jnp.bfloat16)
    fill_slots(top_count, normed_ref, table_ref, out_ref)


def routes_kernel(capacity, expert_ref, weight_ref, out_ref):
    row_count, top_count = expert_ref.shape
    lanes = out_ref.shape[1]
    lane = lax.broadcasted_iota(jnp.int32, (row_count, lanes), 1)
    before = lax.broadcasted_iota(jnp.int32, (row_count, row_count), 0) > (
        lax.broadcasted_iota(jnp.int32, (row_count, row_count), 1)
    )
    before = jnp.where(before, 1.0, 0.0).astype(jnp.bfloat16)
    taken = jnp.zeros((1, lanes), jnp.float32)
    table = jnp.zeros((row_count, lanes), jnp.float32)
    for k in range(top_count):
        expert = expert_ref[:, k : k + 1]
        onehot = jnp.where(lane == expert, 1.0, 0.0)
        earlier = taken + jnp.dot(
            before, onehot.astype(jnp.bfloat16), preferred_element_type=jnp.float32
        )
        rank = jnp.sum(onehot * earlier, axis=1, keepdims=True)
        slot = expert.astype(jnp.float32) * capacity + rank
        taken = taken + jnp.sum(onehot, axis=0, keepdims=True)
        table = jnp.where(lane == k, slot, table)
        table = jnp.where(lane == top_count + k, weight_ref[:, k : k + 1], table)
    out_ref[...] = table.T[: out_ref.shape[0], :row_count]


def fill_slots(top_count, rows_ref, table_ref, out_ref):
    row_count, width = rows_ref.shape
    step = min(512, width)
    slot_count = out_ref.shape[0]
    slots = lax.broadcasted_iota(jnp.int32, (slot_count, row_count), 0)
    slots = slots.astype(jnp.float32)
    hit = slots == table_ref[0:1, :]
    for k in range(1, top_count):
        hit = hit | (slots == table_ref[k : k + 1, :])
    placing = jnp.where(hit, 1.0, 0.0).astype(jnp.bfloat16)
    for at in range(0, width, step):
        cols = slice(at, at + step)
        out_ref[:, cols] = jnp.dot(
            placing, rows_ref[:, cols], preferred_element_type=jnp.float32
        ).astype(jnp.bfloat16)


def gather_kernel(base_count, top_count, *refs):
    bases = refs[:base_count]
    slots_ref, table_ref, out_ref = refs[base_count:]
    row_count, width = out_ref.shape
    slot_count = slots_ref.shape[0]
    step = min(512, width)
    table = table_ref[...].T
    slots = lax.broadcasted_iota(jnp.int32, (row_count, slot_count), 1)
    slots = slots.astype(jnp.float32)
    picks = [
        jnp.where(slots == table[:, k : k + 1], 1.0, 0.0).astype(jnp.bfloat16)
        for k in range(top_count)
    ]
    for at in range(0, width, step):
        cols = slice(at, at + step)
        total = None
        for base in bases:
            piece = base[:, cols].astype(jnp.float32)
            total = piece if total is None else total + piece
        for k in range(top_count):
            row = jnp.dot(picks[k], slots_ref[:, cols], preferred_element_type=jnp.float32)
            row = row * table[:, top_count + k : top_count + k + 1]
            total = row if total is None else total + row
        out_ref[:, cols] = total.astype(out_ref.dtype)


def expert_kernel(rows_ref, gate_ref, up_ref, down_ref, out_ref, act_ref):
    hidden = gate_ref.shape[1]
    width = down_ref.shape[1]
    step = min(256, hidden)
    for at in range(0, hidden, step):
        cols = slice(at, at + step)
        gate = jnp.dot(rows_ref[...], gate_ref[:, cols], preferred_element_type=jnp.float32)
        up = jnp.dot(rows_ref[...], up_ref[:, cols], preferred_element_type=jnp.float32)
        act_ref[:, cols] = (gate / (1.0 + jnp.exp(-gate)) * up).astype(jnp.bfloat16)
    step = min(512, width)
    for at in range(0, width, step):
        cols = slice(at, at + step)
        out_ref[:, cols] = jnp.dot(
            act_ref[...], down_ref[:, cols], preferred_element_type=jnp.float32
        ).astype(jnp.bfloat16)


def local(
    sp_size,
    tp_size,
    query_proj,
    projected_keys,
    projected_values,
    residual,
    out_weight,
    mix_gain,
    norm_gain,
    route_expert,
    route_weight,
    expert_gate,
    expert_up,
    expert_down,
):
    tok_count, lanes = projected_keys.shape
    q_heads = query_proj.shape[1] // HEAD_SIZE
    model_width = residual.shape[1]
    halves = tok_count // HALF_KEYS
    tables = rotation_tables(sp_size * tok_count // GRID_W, lanes)
    raw_own = pl.pallas_call(
        pack_kernel,
        out_shape=jax.ShapeDtypeStruct((halves, 2, HALF_KEYS, lanes), jnp.bfloat16),
        in_specs=[HBM, HBM],
        out_specs=VMEM,
        scratch_shapes=[pltpu.SemaphoreType.DMA((halves, 2))],
        cost_estimate=pl.CostEstimate(flops=1 << 20, bytes_accessed=1 << 19, transcendentals=0),
    )(projected_keys, projected_values)

    row_count = residual.shape[0]
    top_count = route_expert.shape[1]
    experts = sp_size * tp_size
    capacity = max(2, 2 * top_count * row_count // experts)
    slots_total = experts * capacity
    table = pl.pallas_call(
        functools.partial(routes_kernel, capacity),
        out_shape=jax.ShapeDtypeStruct((8, row_count), jnp.float32),
        in_specs=[VMEM] * 2,
        out_specs=VMEM,
        cost_estimate=pl.CostEstimate(flops=1 << 22, bytes_accessed=1 << 17, transcendentals=0),
        compiler_params=pltpu.CompilerParams(vmem_limit_bytes=8 * 1024 * 1024),
    )(route_expert, route_weight)

    order = list(range(0, sp_size, 2)) + list(range(sp_size - 1, 0, -2))
    ahead = [(order[i], order[(i + 1) % sp_size]) for i in range(sp_size)]
    behind = [(b, a) for a, b in ahead]
    steps = sp_size // 2
    acc = None
    queries = query_proj
    from_left = from_right = raw_own
    held, pieces = [raw_own], [(0, 0)]
    for step in range(steps):
        if step == steps - 1:
            from_left, from_right = from_left[: halves // 2], from_right[halves // 2 :]
        next_left = lax.ppermute(from_left, "sp", ahead)
        next_right = lax.ppermute(from_right, "sp", behind)
        after = (table,) if step == steps - 1 else ()
        out = attend(queries, tables, held, pieces, acc, sp_size, tp_size, after=after)
        if step == 0:
            queries, acc = out
        else:
            (acc,) = out
        from_left, from_right = next_left, next_right
        held = [from_left, from_right]
        pieces = [(-step - 1, 0), (step + 1, halves // 2 if step == steps - 1 else 0)]
    pieces = attend(queries, tables, held, pieces, acc, sp_size, tp_size, last=True)
    blocks = hypercube_exchange(pieces, tp_size)

    rows_shape = jax.ShapeDtypeStruct((row_count, model_width), jnp.bfloat16)
    slots_shape = jax.ShapeDtypeStruct((slots_total, model_width), jnp.bfloat16)
    stream, outgoing = pl.pallas_call(
        functools.partial(out_kernel, tp_size, top_count),
        out_shape=(rows_shape, slots_shape),
        in_specs=[VMEM] * (tp_size + 5),
        out_specs=(VMEM, VMEM),
        scratch_shapes=[
            pltpu.VMEM((row_count, model_width), jnp.bfloat16),
            pltpu.VMEM((row_count, model_width), jnp.float32),
        ],
        cost_estimate=pl.CostEstimate(
            flops=2 * row_count * model_width * (out_weight.shape[0] + slots_total),
            bytes_accessed=8 << 20,
            transcendentals=0,
        ),
        compiler_params=pltpu.CompilerParams(vmem_limit_bytes=12 * 1024 * 1024),
    )(*blocks, out_weight, residual, mix_gain[None, :], norm_gain[None, :], table)

    def exchange(slots):
        slots = slots.reshape(experts, capacity, model_width)
        slots = lax.all_to_all(slots, ("sp", "tp"), split_axis=0, concat_axis=0, tiled=True)
        return slots.reshape(slots_total, model_width)

    hidden = expert_gate.shape[2]
    done = pl.pallas_call(
        expert_kernel,
        out_shape=slots_shape,
        in_specs=[VMEM] * 4,
        out_specs=VMEM,
        scratch_shapes=[pltpu.VMEM((slots_total, hidden), jnp.bfloat16)],
        cost_estimate=pl.CostEstimate(
            flops=6 * slots_total * model_width * hidden,
            bytes_accessed=16 << 20,
            transcendentals=slots_total * hidden,
        ),
        compiler_params=pltpu.CompilerParams(vmem_limit_bytes=24 * 1024 * 1024),
    )(exchange(outgoing), expert_gate[0], expert_up[0], expert_down[0])
    return pl.pallas_call(
        functools.partial(gather_kernel, 1, top_count),
        out_shape=rows_shape,
        in_specs=[VMEM] * 3,
        out_specs=VMEM,
        cost_estimate=pl.CostEstimate(
            flops=4 * row_count * slots_total * model_width,
            bytes_accessed=3 << 20,
            transcendentals=0,
        ),
        compiler_params=pltpu.CompilerParams(vmem_limit_bytes=12 * 1024 * 1024),
    )(stream, exchange(done), table)


def solution(mesh):
    return jax.shard_map(
        functools.partial(local, mesh.shape["sp"], mesh.shape["tp"]),
        mesh=mesh,
        in_specs=(
            P("sp", "tp"),
            P("sp", "tp"),
            P("sp", "tp"),
            P(("sp", "tp"), None),
            P(),
            P(),
            P(),
            P(("sp", "tp"), None),
            P(("sp", "tp"), None),
            P(("sp", "tp"), None, None),
            P(("sp", "tp"), None, None),
            P(("sp", "tp"), None, None),
        ),
        out_specs=P(("sp", "tp"), None),
        check_vma=False,
    )
```

time: 160 us -> 156 us (0.975)
  waiting for transfers between devices: 67.1 us -> 13 us
  blocking collectives: 53.3 us -> 106 us
  starting transfers between devices: 14.7 us -> 11 us
  Pallas kernels: 18.6 us -> 21.7 us
    all_to_all x1 -> x2, blocking collectives: 53.3 us -> 106 us  [exchange(): lax.all_to_all(slots, ('sp', 'tp'), split_axis=0, concat_axis=0, tiled=True)]
    all_to_all x1 -> x0, waiting for transfers between devices: 48.5 us -> none  [local(): lax.all_to_all(answered, ('sp', 'tp'), split_axis=0, concat_axis=0, tiled...]
    ppermute x4, waiting for transfers between devices: 12.4 us -> 1.26 us  [local(): next_left = lax.ppermute(from_left, 'sp', ahead)]
    ppermute x4, starting transfers between devices: 1.1 us -> 7.23 us  [local(): next_right = lax.ppermute(from_right, 'sp', behind)]
    ppermute x4, starting transfers between devices: 8.19 us -> 2.12 us  [local(): next_left = lax.ppermute(from_left, 'sp', ahead)]
    ppermute x4, waiting for transfers between devices: 1.74 us -> 7.08 us  [local(): next_right = lax.ppermute(from_right, 'sp', behind)]
    all_to_all x1 -> x0, starting transfers between devices: 3.67 us -> none  [local(): lax.all_to_all(answered, ('sp', 'tp'), split_axis=0, concat_axis=0, tiled...]
    pallas_call x8 -> x10, Pallas kernels: 18.6 us -> 21.7 us  [the longest x5 9.2 us: attend(): pl.pallas_call(functools.partial(attend_kernel, sp_size, pieces, last, ra...]
  transfers between devices with their start and end apart: 12 -> 11, of which waited for: 8 -> 7; matrix products, arithmetic and copies ran while one was open for 0% -> 1% of each run, Pallas kernels for 4% -> 5%
where the time goes in v5:
time: 156 us; the launch traced here: 155 us
  blocking collectives  106 us (68%)
  Pallas kernels  21.7 us (14%)
  waiting for transfers between devices  13 us (8%)
  starting transfers between devices  11 us (7%)
  local copies, waits for them, and re-layouts  3.53 us (2%)
    all_to_all x2, blocking collectives, exchange(): lax.all_to_all(slots, ('sp', 'tp'), split_axis=0, concat_axis=0, tiled=True)  106 us
    pallas_call x5, Pallas kernels, attend(): pl.pallas_call(functools.partial(attend_kernel, sp_size, pieces, last, ra...  9.2 us
    ppermute x4, starting transfers between devices, local(): next_right = lax.ppermute(from_right, 'sp', behind)  7.23 us
    ppermute x4, waiting for transfers between devices, local(): next_right = lax.ppermute(from_right, 'sp', behind)  7.08 us
    pallas_call x1, Pallas kernels, local(): pl.pallas_call(expert_kernel, out_shape=slots_shape, in_specs=[VMEM] * 4,...  6.8 us
    unnamed x20, local copies, waits for them, and re-layouts  3.5 us
    ppermute x2, waiting for transfers between devices, hypercube_exchange(): moved = [(half, lax.ppermute(pieces[1 + bit], 'tp', pairs))]  3.45 us
  transfers between devices with their start and end apart: 11, of which 7 were waited for; matrix products, arithmetic and copies ran while one was open for 1% of the time, Pallas kernels for 5%

profile of v5, /device:TPU:0, one launch (start us, length us, event | category | flops | bytes accessed | tf_op | source)
XLA Modules:
  0.0 155.3 jit_solution(12966587986622901208)
XLA Ops:
  0.0 1.7 %shard_map.118.refs_3_ = bf16[2,2,256,128]{3,2,1,0:T(8,128)(2,1)} custom-call(bf16[512,128]{1,0:T(8,128)(2,1)} %k_hbm.1, bf16[512,128]{1,0:T(8,128)(2,1)} %v_hbm.1), custom_call_target="tpu_custom_call" | custom-call | flops 1048576 | bytes 524288 | tf_op jit(solution)/shard_map/pallas_call | solution.py:393
  1.7 3.0 %collective-permute-start.4 = (bf16[2,2,256,128]{3,2,1,0:T(8,128)(2,1)}, bf16[2,2,256,128]{3,2,1,0:T(8,128)(2,1)S(1)}, u32[]{:S(2)}, u32[]{:S(2)}) collective-permute-start(bf16[2,2,256,128]{3,2,1,0:T(8,128)(2,1)} %shard_map.118.refs_3_), channel_id=1, source_target_pairs={{8,0},{16,8},{24,16},{28,24},{20,28},{12,20},{4,12},{0,4},{9,1},{1... | collective-permute-start | bytes 786440 | tf_op jit(solution)/shard_map/ppermute | solution.py:428
  6.9 4.4 %collective-permute-done.4.refs_4_ = bf16[2,2,256,128]{3,2,1,0:T(8,128)(2,1)S(1)} collective-permute-done((bf16[2,2,256,128]{3,2,1,0:T(8,128)(2,1)}, bf16[2,2,256,128]{3,2,1,0:T(8,128)(2,1)S(1)}, u32[]{:S(2)}, u32[]{:S(2)}) %collective-permute-start.4) | collective-permute-done | bytes 262176 | tf_op jit(solution)/shard_map/ppermute | solution.py:428
  11.3 1.7 %collective-permute-start.5 = (bf16[2,2,256,128]{3,2,1,0:T(8,128)(2,1)S(1)}, bf16[2,2,256,128]{3,2,1,0:T(8,128)(2,1)S(1)}, u32[]{:S(2)}, u32[]{:S(2)}) collective-permute-start(bf16[2,2,256,128]{3,2,1,0:T(8,128)(2,1)S(1)} %collective-permute-done.4.refs_4_), channel_id=1, source_target_pairs={{8,0},{16,8},{24,16},{28,24},{20,28},{12,20},{4,12},{0,4},{9,1},{1... | collective-permute-start | bytes 786440 | tf_op jit(solution)/shard_map/ppermute | solution.py:428
  13.7 0.9 copy-done.2
  14.6 0.9 copy-done.8
  15.5 1.5 shard_map.119
  17.1 1.7 %collective-permute-done.5.refs_4_ = bf16[2,2,256,128]{3,2,1,0:T(8,128)(2,1)S(1)} collective-permute-done((bf16[2,2,256,128]{3,2,1,0:T(8,128)(2,1)S(1)}, bf16[2,2,256,128]{3,2,1,0:T(8,128)(2,1)S(1)}, u32[]{:S(2)}, u32[]{:S(2)}) %collective-permute-start.5) | collective-permute-done | bytes 262176 | tf_op jit(solution)/shard_map/ppermute | solution.py:428
  18.8 1.4 collective-permute-start.6
  20.8 2.1 %shard_map.120.refs_5_ = f32[80,2048]{1,0:T(8,128)S(1)} custom-call(bf16[128,2048]{1,0:T(8,128)(2,1)S(1)} %get-tuple-element.12.refs_0_, f32[128,128]{1,0:T(8,128)S(1)} %get-tuple-element.22.refs_1_, f32[128,128]{1,0:T(8,128)S(1)} %get-tuple-element.21.refs_2_, ...), custom_call_target="tpu_custom_call", output_to_operand_aliasing={{}: (5, {})} | custom-call | flops 2147483648 | bytes 1048576 | tf_op jit(solution)/shard_map/pallas_call | solution.py:219
  22.9 2.1 %shard_map.121.refs_5_ = f32[80,2048]{1,0:T(8,128)S(1)} custom-call(bf16[128,2048]{1,0:T(8,128)(2,1)S(1)} %get-tuple-element.12.refs_0_, f32[128,128]{1,0:T(8,128)S(1)} %get-tuple-element.22.refs_1_, f32[128,128]{1,0:T(8,128)S(1)} %get-tuple-element.21.refs_2_, ...), custom_call_target="tpu_custom_call", output_to_operand_aliasing={{}: (5, {})} | custom-call | flops 2147483648 | bytes 1048576 | tf_op jit(solution)/shard_map/pallas_call | solution.py:219
  25.4 1.2 collective-permute-start.7
  26.6 0.9 collective-permute-start.3
  27.6 2.1 %shard_map.123.refs_5_ = f32[80,2048]{1,0:T(8,128)S(1)} custom-call(bf16[128,2048]{1,0:T(8,128)(2,1)S(1)} %get-tuple-element.12.refs_0_, f32[128,128]{1,0:T(8,128)S(1)} %get-tuple-element.22.refs_1_, f32[128,128]{1,0:T(8,128)S(1)} %get-tuple-element.21.refs_2_, ...), custom_call_target="tpu_custom_call", output_to_operand_aliasing={{}: (5, {})} | custom-call | flops 2147483648 | bytes 1048576 | tf_op jit(solution)/shard_map/pallas_call | solution.py:219
  30.4 1.2 collective-permute-done.3.refs_3_
  31.7 1.3 shard_map.124
  33.0 1.6 %collective-permute-start.9 = (bf16[2,256,128]{2,1,0:T(8,128)(2,1)S(1)}, bf16[2,256,128]{2,1,0:T(8,128)(2,1)S(1)}, u32[]{:S(2)}, u32[]{:S(2)}) collective-permute-start(bf16[2,256,128]{2,1,0:T(8,128)(2,1)S(1)} %get-tuple-element.16), channel_id=1, source_target_pairs={{0,2},{1,3},{2,0},{3,1},{4,6},{5,7},{6,4},{7,5},{8,10},{9,11},{10,... | collective-permute-start | bytes 393224 | tf_op jit(solution)/shard_map/ppermute | solution.py:240
  34.6 3.4 %collective-permute-done.9 = bf16[2,256,128]{2,1,0:T(8,128)(2,1)S(1)} collective-permute-done((bf16[2,256,128]{2,1,0:T(8,128)(2,1)S(1)}, bf16[2,256,128]{2,1,0:T(8,128)(2,1)S(1)}, u32[]{:S(2)}, u32[]{:S(2)}) %collective-permute-start.9) | collective-permute-done | bytes 131104 | tf_op jit(solution)/shard_map/ppermute | solution.py:240
  38.1 1.2 collective-permute-done.10.refs_3_
  39.4 1.9 %shard_map.125 = (bf16[128,2048]{1,0:T(8,128)(2,1)S(1)}, bf16[512,2048]{1,0:T(8,128)(2,1)S(1)}) custom-call(bf16[1,256,128]{2,1,0:T(8,128)(2,1)S(1)} %get-tuple-element.14.refs_0_, bf16[1,256,128]{2,1,0:T(8,128)(2,1)S(1)} %collective-permute-done.8.refs_1_, bf16[1,256,128]{2,1,0:T(8,128)(2,1)S(1)} %get-tuple-element.20.refs_2_, ...), custom_call_target="tpu_custom_call" | custom-call | flops 805306368 | bytes 8388608 | tf_op jit(solution)/shard_map/pallas_call | solution.py:443
  41.3 53.4 %all_to_all.10 = bf16[32,16,2048]{2,1,0:T(8,128)(2,1)S(1)} all-to-all(bf16[32,16,2048]{2,1,0:T(8,128)(2,1)S(1)} %bitcast.10), channel_id=1, replica_groups=mesh['sp'=8,'tp'=4] {'sp','tp'}, dimensions={0} | all-to-all | bytes 4194304 | tf_op jit(solution)/shard_map/all_to_all | solution.py:462
  94.7 6.8 %shard_map.126 = bf16[512,2048]{1,0:T(8,128)(2,1)S(1)} custom-call(bf16[512,2048]{1,0:T(8,128)(2,1)S(1)} %bitcast.11, bf16[2048,1024]{1,0:T(8,128)(2,1)S(1)} %bitcast.15, bf16[2048,1024]{1,0:T(8,128)(2,1)S(1)} %bitcast.16, bf16[1024,2048]{1,0:T(8,128)(2,1)S(1)} %bitcast.17), custom_call_target="tpu_custom_call" | custom-call | flops 6442450944 | bytes 16777216 | tf_op jit(solution)/shard_map/pallas_call | solution.py:466
  101.5 52.1 %all_to_all.11 = bf16[32,16,2048]{2,1,0:T(8,128)(2,1)S(1)} all-to-all(bf16[32,16,2048]{2,1,0:T(8,128)(2,1)S(1)} %bitcast.12), channel_id=1, replica_groups=mesh['sp'=8,'tp'=4] {'sp','tp'}, dimensions={0} | all-to-all | bytes 4194304 | tf_op jit(solution)/shard_map/all_to_all | solution.py:462
  153.6 1.7 %shard_map.127 = bf16[128,2048]{1,0:T(8,128)(2,1)} custom-call(bf16[128,2048]{1,0:T(8,128)(2,1)S(1)} %get-tuple-element.17.refs_0_, bf16[512,2048]{1,0:T(8,128)(2,1)S(1)} %bitcast.9, f32[8,128]{1,0:T(8,128)S(1)} %shard_map.122.refs_6_.refs_8_.refs_2_), custom_call_target="tpu_custom_call" | custom-call | flops 536870912 | bytes 3145728 | tf_op jit(solution)/shard_map/pallas_call | solution.py:479
  (36 shorter events, 4.7 us)
Async XLA Ops:
  1.7 9.6 %collective-permute-start.4 = (bf16[2,2,256,128]{3,2,1,0:T(8,128)(2,1)}, bf16[2,2,256,128]{3,2,1,0:T(8,128)(2,1)S(1)}, u32[]{:S(2)}, u32[]{:S(2)}) collective-permute-start(bf16[2,2,256,128]{3,2,1,0:T(8,128)(2,1)} %shard_map.118.refs_3_), channel_id=1, source_target_pairs={{8,0},{16,8},{24,16},{28,24},{20,28},{12,20},{4,12},{0,4},{9,1},{1... | collective-permute-start | bytes 786440 | tf_op jit(solution)/shard_map/ppermute | solution.py:428
  4.7 8.3 %collective-permute-start = (bf16[2,2,256,128]{3,2,1,0:T(8,128)(2,1)}, bf16[2,2,256,128]{3,2,1,0:T(8,128)(2,1)S(1)}, u32[]{:S(2)}, u32[]{:S(2)}) collective-permute-start(bf16[2,2,256,128]{3,2,1,0:T(8,128)(2,1)} %shard_map.118.refs_3_), channel_id=1, source_target_pairs={{0,8},{8,16},{16,24},{24,28},{28,20},{20,12},{12,4},{4,0},{1,9},{9... | collective-permute-start | bytes 786440 | tf_op jit(solution)/shard_map/ppermute | solution.py:427
  11.3 7.5 %collective-permute-start.5 = (bf16[2,2,256,128]{3,2,1,0:T(8,128)(2,1)S(1)}, bf16[2,2,256,128]{3,2,1,0:T(8,128)(2,1)S(1)}, u32[]{:S(2)}, u32[]{:S(2)}) collective-permute-start(bf16[2,2,256,128]{3,2,1,0:T(8,128)(2,1)S(1)} %collective-permute-done.4.refs_4_), channel_id=1, source_target_pairs={{8,0},{16,8},{24,16},{28,24},{20,28},{12,20},{4,12},{0,4},{9,1},{1... | collective-permute-start | bytes 786440 | tf_op jit(solution)/shard_map/ppermute | solution.py:428
  13.0 7.2 %collective-permute-start.1 = (bf16[2,2,256,128]{3,2,1,0:T(8,128)(2,1)S(1)}, bf16[2,2,256,128]{3,2,1,0:T(8,128)(2,1)S(1)}, u32[]{:S(2)}, u32[]{:S(2)}) collective-permute-start(bf16[2,2,256,128]{3,2,1,0:T(8,128)(2,1)S(1)} %collective-permute-done.refs_3_), channel_id=1, source_target_pairs={{0,8},{8,16},{16,24},{24,28},{28,20},{20,12},{12,4},{4,0},{1,9},{9... | collective-permute-start | bytes 786440 | tf_op jit(solution)/shard_map/ppermute | solution.py:427
  13.6 1.0 copy-start.2
  14.6 0.9 copy-start.8
  18.8 6.6 %collective-permute-start.6 = (bf16[2,2,256,128]{3,2,1,0:T(8,128)(2,1)S(1)}, bf16[2,2,256,128]{3,2,1,0:T(8,128)(2,1)S(1)}, u32[]{:S(2)}, u32[]{:S(2)}) collective-permute-start(bf16[2,2,256,128]{3,2,1,0:T(8,128)(2,1)S(1)} %collective-permute-done.5.refs_4_), channel_id=1, source_target_pairs={{8,0},{16,8},{24,16},{28,24},{20,28},{12,20},{4,12},{0,4},{9,1},{1... | collective-permute-start | bytes 786440 | tf_op jit(solution)/shard_map/ppermute | solution.py:428
  20.1 6.4 %collective-permute-start.2 = (bf16[2,2,256,128]{3,2,1,0:T(8,128)(2,1)S(1)}, bf16[2,2,256,128]{3,2,1,0:T(8,128)(2,1)S(1)}, u32[]{:S(2)}, u32[]{:S(2)}) collective-permute-start(bf16[2,2,256,128]{3,2,1,0:T(8,128)(2,1)S(1)} %collective-permute-done.1.refs_3_), channel_id=1, source_target_pairs={{0,8},{8,16},{16,24},{24,28},{28,20},{20,12},{12,4},{4,0},{1,9},{9... | collective-permute-start | bytes 786440 | tf_op jit(solution)/shard_map/ppermute | solution.py:427
  25.4 5.0 %collective-permute-start.7 = (bf16[1,2,256,128]{3,2,1,0:T(8,128)(2,1)S(1)}, bf16[1,2,256,128]{3,2,1,0:T(8,128)(2,1)S(1)}, u32[]{:S(2)}, u32[]{:S(2)}) collective-permute-start(bf16[1,2,256,128]{3,2,1,0:T(8,128)(2,1)S(1)} %slice.17), channel_id=1, source_target_pairs={{8,0},{16,8},{24,16},{28,24},{20,28},{12,20},{4,12},{0,4},{9,1},{1... | collective-permute-start | bytes 393224 | tf_op jit(solution)/shard_map/ppermute | solution.py:428
  26.6 12.7 %copy-start = (bf16[1024,2048]{1,0:T(8,128)(2,1)S(1)}, bf16[1024,2048]{1,0:T(8,128)(2,1)}, u32[]{:S(2)}) copy-start(bf16[1024,2048]{1,0:T(8,128)(2,1)} %refs_4_.1) | copy-start | bytes 12582916
  26.6 12.7 %copy-start.1 = (bf16[128,2048]{1,0:T(8,128)(2,1)S(1)}, bf16[128,2048]{1,0:T(8,128)(2,1)}, u32[]{:S(2)}) copy-start(bf16[128,2048]{1,0:T(8,128)(2,1)} %refs_5_.1) | copy-start | bytes 1572868
  26.6 12.7 %copy-start.3 = (f32[2048]{0:T(1024)S(1)}, f32[2048]{0:T(1024)}, u32[]{:S(2)}) copy-start(f32[2048]{0:T(1024)} %param.17) | copy-start | bytes 24580
  26.6 12.7 %copy-start.4 = (f32[2048]{0:T(1024)S(1)}, f32[2048]{0:T(1024)}, u32[]{:S(2)}) copy-start(f32[2048]{0:T(1024)} %param.18) | copy-start | bytes 24580
  26.6 5.0 %collective-permute-start.3 = (bf16[1,2,256,128]{3,2,1,0:T(8,128)(2,1)S(1)}, bf16[1,2,256,128]{3,2,1,0:T(8,128)(2,1)S(1)}, u32[]{:S(2)}, u32[]{:S(2)}) collective-permute-start(bf16[1,2,256,128]{3,2,1,0:T(8,128)(2,1)S(1)} %slice.16), channel_id=1, source_target_pairs={{0,8},{8,16},{16,24},{24,28},{28,20},{20,12},{12,4},{4,0},{1,9},{9... | collective-permute-start | bytes 393224 | tf_op jit(solution)/shard_map/ppermute | solution.py:427
  31.7 63.0 %copy-start.7 = (bf16[1,1024,2048]{2,1,0:T(8,128)(2,1)S(1)}, bf16[1,1024,2048]{2,1,0:T(8,128)(2,1)}, u32[]{:S(2)}) copy-start(bf16[1,1024,2048]{2,1,0:T(8,128)(2,1)} %param.23) | copy-start | bytes 12582916
  33.0 5.0 %collective-permute-start.9 = (bf16[2,256,128]{2,1,0:T(8,128)(2,1)S(1)}, bf16[2,256,128]{2,1,0:T(8,128)(2,1)S(1)}, u32[]{:S(2)}, u32[]{:S(2)}) collective-permute-start(bf16[2,256,128]{2,1,0:T(8,128)(2,1)S(1)} %get-tuple-element.16), channel_id=1, source_target_pairs={{0,2},{1,3},{2,0},{3,1},{4,6},{5,7},{6,4},{7,5},{8,10},{9,11},{10,... | collective-permute-start | bytes 393224 | tf_op jit(solution)/shard_map/ppermute | solution.py:240
  34.6 3.5 %collective-permute-start.8 = (bf16[1,256,128]{2,1,0:T(8,128)(2,1)S(1)}, bf16[1,256,128]{2,1,0:T(8,128)(2,1)S(1)}, u32[]{:S(2)}, u32[]{:S(2)}) collective-permute-start(bf16[1,256,128]{2,1,0:T(8,128)(2,1)S(1)} %get-tuple-element.15), channel_id=1, source_target_pairs={{0,1},{1,0},{2,3},{3,2},{4,5},{5,4},{6,7},{7,6},{8,9},{9,8},{10,11... | collective-permute-start | bytes 196616 | tf_op jit(solution)/shard_map/ppermute | solution.py:240
  38.0 1.3 collective-permute-start.10
  39.4 55.3 %copy-start.5 = (bf16[1,2048,1024]{2,1,0:T(8,128)(2,1)S(1)}, bf16[1,2048,1024]{2,1,0:T(8,128)(2,1)}, u32[]{:S(2)}) copy-start(bf16[1,2048,1024]{2,1,0:T(8,128)(2,1)} %param.21) | copy-start | bytes 12582916
  39.4 55.3 %copy-start.6 = (bf16[1,2048,1024]{2,1,0:T(8,128)(2,1)S(1)}, bf16[1,2048,1024]{2,1,0:T(8,128)(2,1)}, u32[]{:S(2)}) copy-start(bf16[1,2048,1024]{2,1,0:T(8,128)(2,1)} %param.22) | copy-start | bytes 12582916

commit v6 on v5

--- a/solution.py
+++ b/solution.py
@@ -29,21 +29,6 @@
     angle = place.astype(jnp.float32)[:, None] * frequency[None, :]
     sign = jnp.where((lane // quarter) % 2 == 0, -1.0, 1.0).astype(jnp.float32)
     return jnp.cos(angle), jnp.sin(angle) * sign[None, :]
-
-
-def pack_kernel(k_hbm, v_hbm, out_ref, sems):
-    halves = out_ref.shape[0]
-    copies = [
-        pltpu.make_async_copy(
-            src.at[pl.ds(half * HALF_KEYS, HALF_KEYS), :], out_ref.at[half, i], sems.at[half, i]
-        )
-        for half in range(halves)
-        for i, src in enumerate((k_hbm, v_hbm))
-    ]
-    for copy in copies:
-        copy.start()
-    for copy in copies:
-        copy.wait()
 
 
 class Rotation:
@@ -181,11 +166,8 @@
         waiting = weights
     if last:
         me = lax.axis_index("tp")
-        rel = 0
-        for out in outs:
-            for j in range(out.shape[0]):
-                out[j] = refs[2][me ^ rel]
-                rel += 1
+        for rel, out in enumerate(outs):
+            out[...] = refs[2][me ^ rel]
 
 
 def attend(queries, tables, chunks, pieces, acc, sp_size, tp_size, last=False, after=()):
@@ -206,8 +188,7 @@
     if last:
         head_rows = columns // tok_count * HEAD_SIZE
         block = (head_rows, tok_count // tp_size)
-        sizes = [1] + [1 << b for b in range(tp_size.bit_length() - 1)]
-        shape = [jax.ShapeDtypeStruct((n, *block), jnp.bfloat16) for n in sizes]
+        shape = [jax.ShapeDtypeStruct(block, jnp.bfloat16)] * tp_size
         scratch.append(pltpu.VMEM((tp_size, *block), jnp.bfloat16))
     else:
         shape = [jax.ShapeDtypeStruct((rows, columns), jnp.float32)]
@@ -232,18 +213,11 @@
     )(*operands, *after)
 
 
-def hypercube_exchange(pieces, tp_size):
-    held = []
-    for bit in reversed(range(tp_size.bit_length() - 1)):
-        pairs = [(i, i ^ (1 << bit)) for i in range(tp_size)]
-        half = 1 << bit
-        moved = [(half, lax.ppermute(pieces[1 + bit], "tp", pairs))]
-        kept = []
-        for source, block in held:
-            moved.append((source ^ half, lax.ppermute(block[half:], "tp", pairs)))
-            kept.append((source, block[:half]))
-        held = kept + moved
-    return [pieces[0]] + [block for _, block in sorted(held, key=lambda item: item[0])]
+def direct_exchange(pieces, tp_size):
+    held = {0: pieces[0]}
+    for rel in reversed(range(1, tp_size)):
+        held[rel] = lax.ppermute(pieces[rel], "tp", [(i, i ^ rel) for i in range(tp_size)])
+    return [held[rel] for rel in range(tp_size)]
 
 
 def out_kernel(tp_size, top_count, *refs):
@@ -251,10 +225,10 @@
     w_ref, res_ref, mix_ref, norm_ref, table_ref = refs[tp_size : tp_size + 5]
     stream_ref, out_ref, normed_ref, mixed_ref = refs[tp_size + 5 :]
     me = lax.axis_index("tp")
-    _, head_rows, row_count = blocks[0].shape
+    head_rows, row_count = blocks[0].shape
     width = w_ref.shape[1]
     step = min(512, width)
-    turned = [b[0].astype(jnp.float32).T.astype(jnp.bfloat16) for b in blocks]
+    turned = [b[...].astype(jnp.float32).T.astype(jnp.bfloat16) for b in blocks]
     power = jnp.zeros((row_count, 1), jnp.float32)
     for at in range(0, width, step):
         mixed = jnp.zeros((row_count, step), jnp.float32)
@@ -326,30 +300,33 @@
         ).astype(jnp.bfloat16)
 
 
-def gather_kernel(base_count, top_count, *refs):
-    bases = refs[:base_count]
-    slots_ref, table_ref, out_ref = refs[base_count:]
-    row_count, width = out_ref.shape
-    slot_count = slots_ref.shape[0]
-    step = min(512, width)
+def gather_kernel(top_count, base_ref, slots_ref, table_ref, out_hbm, out_ref, sems):
+    row_count, width = base_ref.shape
+    step = width // sems.shape[0]
     table = table_ref[...].T
-    slots = lax.broadcasted_iota(jnp.int32, (row_count, slot_count), 1)
+    slots = lax.broadcasted_iota(jnp.int32, (row_count, slots_ref.shape[0]), 1)
     slots = slots.astype(jnp.float32)
     picks = [
         jnp.where(slots == table[:, k : k + 1], 1.0, 0.0).astype(jnp.bfloat16)
         for k in range(top_count)
     ]
-    for at in range(0, width, step):
-        cols = slice(at, at + step)
+    picks = jnp.concatenate(picks, axis=0)
+    copies = []
+    for i in range(sems.shape[0]):
+        cols = pl.ds(i * step, step)
+        rows = jnp.dot(picks, slots_ref[:, cols], preferred_element_type=jnp.float32)
         total = None
-        for base in bases:
-            piece = base[:, cols].astype(jnp.float32)
-            total = piece if total is None else total + piece
         for k in range(top_count):
-            row = jnp.dot(picks[k], slots_ref[:, cols], preferred_element_type=jnp.float32)
+            row = rows[k * row_count : (k + 1) * row_count]
             row = row * table[:, top_count + k : top_count + k + 1]
             total = row if total is None else total + row
-        out_ref[:, cols] = total.astype(out_ref.dtype)
+        out_ref[:, cols] = (base_ref[:, cols].astype(jnp.float32) + total).astype(out_ref.dtype)
+        copies.append(
+            pltpu.make_async_copy(out_ref.at[:, cols], out_hbm.at[:, cols], sems.at[i])
+        )
+        copies[-1].start()
+    for copy in copies:
+        copy.wait()
 
 
 def expert_kernel(rows_ref, gate_ref, up_ref, down_ref, out_ref, act_ref):
@@ -390,14 +367,10 @@
     model_width = residual.shape[1]
     halves = tok_count // HALF_KEYS
     tables = rotation_tables(sp_size * tok_count // GRID_W, lanes)
-    raw_own = pl.pallas_call(
-        pack_kernel,
-        out_shape=jax.ShapeDtypeStruct((halves, 2, HALF_KEYS, lanes), jnp.bfloat16),
-        in_specs=[HBM, HBM],
-        out_specs=VMEM,
-        scratch_shapes=[pltpu.SemaphoreType.DMA((halves, 2))],
-        cost_estimate=pl.CostEstimate(flops=1 << 20, bytes_accessed=1 << 19, transcendentals=0),
-    )(projected_keys, projected_values)
+    raw_own = jnp.stack(
+        [part.reshape(halves, HALF_KEYS, lanes) for part in (projected_keys, projected_values)],
+        axis=1,
+    )
 
     row_count = residual.shape[0]
     top_count = route_expert.shape[1]
@@ -436,7 +409,7 @@
         held = [from_left, from_right]
         pieces = [(-step - 1, 0), (step + 1, halves // 2 if step == steps - 1 else 0)]
     pieces = attend(queries, tables, held, pieces, acc, sp_size, tp_size, last=True)
-    blocks = hypercube_exchange(pieces, tp_size)
+    blocks = direct_exchange(pieces, tp_size)
 
     rows_shape = jax.ShapeDtypeStruct((row_count, model_width), jnp.bfloat16)
     slots_shape = jax.ShapeDtypeStruct((slots_total, model_width), jnp.bfloat16)
@@ -477,10 +450,14 @@
         compiler_params=pltpu.CompilerParams(vmem_limit_bytes=24 * 1024 * 1024),
     )(exchange(outgoing), expert_gate[0], expert_up[0], expert_down[0])
     return pl.pallas_call(
-        functools.partial(gather_kernel, 1, top_count),
+        functools.partial(gather_kernel, top_count),
         out_shape=rows_shape,
         in_specs=[VMEM] * 3,
-        out_specs=VMEM,
+        out_specs=HBM,
+        scratch_shapes=[
+            pltpu.VMEM((row_count, model_width), jnp.bfloat16),
+            pltpu.SemaphoreType.DMA((4,)),
+        ],
         cost_estimate=pl.CostEstimate(
             flops=4 * row_count * slots_total * model_width,
             bytes_accessed=3 << 20,

time: 156 us -> 154 us (0.987)
  Pallas kernels: 21.7 us -> 19.9 us
    pallas_call x2 -> x1, Pallas kernels: 3.34 us -> 1.6 us  [local(): pl.pallas_call(functools.partial(gather_kernel, top_count), out_shape=row...]
    unnamed x20 -> x18, local copies, waits for them, and re-layouts: 3.5 us -> 2.56 us
where the time goes in v6:
time: 154 us
  blocking collectives  105 us (68%)
  Pallas kernels  19.9 us (13%)
  waiting for transfers between devices  12.9 us (8%)
  starting transfers between devices  11.3 us (7%)
  local copies, waits for them, and re-layouts  2.57 us (2%)
    all_to_all x2, blocking collectives, exchange(): lax.all_to_all(slots, ('sp', 'tp'), split_axis=0, concat_axis=0, tiled=True)  105 us
    pallas_call x5, Pallas kernels, attend(): pl.pallas_call(functools.partial(attend_kernel, sp_size, pieces, last, ra...  9.2 us
    ppermute x4, waiting for transfers between devices, local(): next_right = lax.ppermute(from_right, 'sp', behind)  7.83 us
    ppermute x4, starting transfers between devices, local(): next_right = lax.ppermute(from_right, 'sp', behind)  7.23 us
    pallas_call x1, Pallas kernels, local(): pl.pallas_call(expert_kernel, out_shape=slots_shape, in_specs=[VMEM] * 4,...  6.8 us
    ppermute x3, waiting for transfers between devices, direct_exchange(): lax.ppermute(pieces[rel], 'tp', [(i, i ^ rel) for i in range(tp_size)])  3.79 us
  transfers between devices with their start and end apart: 11, of which 7 were waited for; matrix products, arithmetic and copies ran while one was open for 1% of the time, Pallas kernels for 5%

profile of v6, /device:TPU:0, one launch (start us, length us, event | category | flops | bytes accessed | tf_op | source)
XLA Modules:
  0.0 153.6 jit_solution(16190259425278231605)
XLA Ops:
  0.0 1.0 pad_maximum_fusion.refs_3_
  1.0 3.0 %collective-permute-start.4 = (bf16[2,2,256,128]{3,2,1,0:T(8,128)(2,1)S(1)}, bf16[2,2,256,128]{3,2,1,0:T(8,128)(2,1)S(1)}, u32[]{:S(2)}, u32[]{:S(2)}) collective-permute-start(bf16[2,2,256,128]{3,2,1,0:T(8,128)(2,1)S(1)} %pad_maximum_fusion.refs_3_), channel_id=1, source_target_pairs={{8,0},{16,8},{24,16},{28,24},{20,28},{12,20},{4,12},{0,4},{9,1},{1... | collective-permute-start | bytes 786440 | tf_op jit(solution)/shard_map/ppermute | solution.py:401
  4.2 0.8 copy.16.expert_ref
  6.2 4.2 %collective-permute-done.4.refs_4_ = bf16[2,2,256,128]{3,2,1,0:T(8,128)(2,1)S(1)} collective-permute-done((bf16[2,2,256,128]{3,2,1,0:T(8,128)(2,1)S(1)}, bf16[2,2,256,128]{3,2,1,0:T(8,128)(2,1)S(1)}, u32[]{:S(2)}, u32[]{:S(2)}) %collective-permute-start.4) | collective-permute-done | bytes 262176 | tf_op jit(solution)/shard_map/ppermute | solution.py:401
  10.4 1.7 %collective-permute-start.5 = (bf16[2,2,256,128]{3,2,1,0:T(8,128)(2,1)S(1)}, bf16[2,2,256,128]{3,2,1,0:T(8,128)(2,1)S(1)}, u32[]{:S(2)}, u32[]{:S(2)}) collective-permute-start(bf16[2,2,256,128]{3,2,1,0:T(8,128)(2,1)S(1)} %collective-permute-done.4.refs_4_), channel_id=1, source_target_pairs={{8,0},{16,8},{24,16},{28,24},{20,28},{12,20},{4,12},{0,4},{9,1},{1... | collective-permute-start | bytes 786440 | tf_op jit(solution)/shard_map/ppermute | solution.py:401
  12.8 0.9 copy-done.7
  13.7 1.5 shard_map.118
  15.2 2.6 %collective-permute-done.5.refs_4_ = bf16[2,2,256,128]{3,2,1,0:T(8,128)(2,1)S(1)} collective-permute-done((bf16[2,2,256,128]{3,2,1,0:T(8,128)(2,1)S(1)}, bf16[2,2,256,128]{3,2,1,0:T(8,128)(2,1)S(1)}, u32[]{:S(2)}, u32[]{:S(2)}) %collective-permute-start.5) | collective-permute-done | bytes 262176 | tf_op jit(solution)/shard_map/ppermute | solution.py:401
  17.9 1.4 collective-permute-start.6
  19.9 2.1 %shard_map.119.refs_5_ = f32[80,2048]{1,0:T(8,128)S(1)} custom-call(bf16[128,2048]{1,0:T(8,128)(2,1)S(1)} %get-tuple-element.13.refs_0_, f32[128,128]{1,0:T(8,128)S(1)} %get-tuple-element.22.refs_1_, f32[128,128]{1,0:T(8,128)S(1)} %get-tuple-element.21.refs_2_, ...), custom_call_target="tpu_custom_call", output_to_operand_aliasing={{}: (5, {})} | custom-call | flops 2147483648 | bytes 1048576 | tf_op jit(solution)/shard_map/pallas_call | solution.py:200
  22.0 2.1 %shard_map.120.refs_5_ = f32[80,2048]{1,0:T(8,128)S(1)} custom-call(bf16[128,2048]{1,0:T(8,128)(2,1)S(1)} %get-tuple-element.13.refs_0_, f32[128,128]{1,0:T(8,128)S(1)} %get-tuple-element.22.refs_1_, f32[128,128]{1,0:T(8,128)S(1)} %get-tuple-element.21.refs_2_, ...), custom_call_target="tpu_custom_call", output_to_operand_aliasing={{}: (5, {})} | custom-call | flops 2147483648 | bytes 1048576 | tf_op jit(solution)/shard_map/pallas_call | solution.py:200
  24.5 1.2 collective-permute-start.7
  25.8 0.9 collective-permute-start.3
  26.7 2.1 %shard_map.122.refs_5_ = f32[80,2048]{1,0:T(8,128)S(1)} custom-call(bf16[128,2048]{1,0:T(8,128)(2,1)S(1)} %get-tuple-element.13.refs_0_, f32[128,128]{1,0:T(8,128)S(1)} %get-tuple-element.22.refs_1_, f32[128,128]{1,0:T(8,128)S(1)} %get-tuple-element.21.refs_2_, ...), custom_call_target="tpu_custom_call", output_to_operand_aliasing={{}: (5, {})} | custom-call | flops 2147483648 | bytes 1048576 | tf_op jit(solution)/shard_map/pallas_call | solution.py:200
  29.5 1.2 collective-permute-done.3.refs_3_
  30.8 1.3 shard_map.123
  32.2 1.6 %collective-permute-start.9 = (bf16[256,128]{1,0:T(8,128)(2,1)S(1)}, bf16[256,128]{1,0:T(8,128)(2,1)S(1)}, u32[]{:S(2)}, u32[]{:S(2)}) collective-permute-start(bf16[256,128]{1,0:T(8,128)(2,1)S(1)} %get-tuple-element.17), channel_id=1, source_target_pairs={{0,2},{1,3},{2,0},{3,1},{4,6},{5,7},{6,4},{7,5},{8,10},{9,11},{10,... | collective-permute-start | bytes 196616 | tf_op jit(solution)/shard_map/ppermute | solution.py:219
  34.0 2.6 %collective-permute-done.9.refs_2_ = bf16[256,128]{1,0:T(8,128)(2,1)S(1)} collective-permute-done((bf16[256,128]{1,0:T(8,128)(2,1)S(1)}, bf16[256,128]{1,0:T(8,128)(2,1)S(1)}, u32[]{:S(2)}, u32[]{:S(2)}) %collective-permute-start.9) | collective-permute-done | bytes 65568 | tf_op jit(solution)/shard_map/ppermute | solution.py:219
  36.7 1.1 collective-permute-done.10.refs_3_
  37.8 1.9 %shard_map.124 = (bf16[128,2048]{1,0:T(8,128)(2,1)S(1)}, bf16[512,2048]{1,0:T(8,128)(2,1)S(1)}) custom-call(bf16[256,128]{1,0:T(8,128)(2,1)S(1)} %get-tuple-element.15.refs_0_, bf16[256,128]{1,0:T(8,128)(2,1)S(1)} %collective-permute-done.8.refs_1_, bf16[256,128]{1,0:T(8,128)(2,1)S(1)} %collective-permute-done.9.refs_2_, ...), custom_call_target="tpu_custom_call" | custom-call | flops 805306368 | bytes 8388608 | tf_op jit(solution)/shard_map/pallas_call | solution.py:416
  39.7 53.1 %all_to_all.10 = bf16[32,16,2048]{2,1,0:T(8,128)(2,1)S(1)} all-to-all(bf16[32,16,2048]{2,1,0:T(8,128)(2,1)S(1)} %bitcast.12), channel_id=1, replica_groups=mesh['sp'=8,'tp'=4] {'sp','tp'}, dimensions={0} | all-to-all | bytes 4194304 | tf_op jit(solution)/shard_map/all_to_all | solution.py:435
  92.9 6.8 %shard_map.125 = bf16[512,2048]{1,0:T(8,128)(2,1)S(1)} custom-call(bf16[512,2048]{1,0:T(8,128)(2,1)S(1)} %bitcast.13, bf16[2048,1024]{1,0:T(8,128)(2,1)S(1)} %bitcast.17, bf16[2048,1024]{1,0:T(8,128)(2,1)S(1)} %bitcast.18, bf16[1024,2048]{1,0:T(8,128)(2,1)S(1)} %bitcast.19), custom_call_target="tpu_custom_call" | custom-call | flops 6442450944 | bytes 16777216 | tf_op jit(solution)/shard_map/pallas_call | solution.py:439
  99.7 52.1 %all_to_all.11 = bf16[32,16,2048]{2,1,0:T(8,128)(2,1)S(1)} all-to-all(bf16[32,16,2048]{2,1,0:T(8,128)(2,1)S(1)} %bitcast.14), channel_id=1, replica_groups=mesh['sp'=8,'tp'=4] {'sp','tp'}, dimensions={0} | all-to-all | bytes 4194304 | tf_op jit(solution)/shard_map/all_to_all | solution.py:435
  151.8 1.6 %shard_map.126 = bf16[128,2048]{1,0:T(8,128)(2,1)} custom-call(bf16[128,2048]{1,0:T(8,128)(2,1)S(1)} %get-tuple-element.19.base_ref, bf16[512,2048]{1,0:T(8,128)(2,1)S(1)} %bitcast.11, f32[8,128]{1,0:T(8,128)S(1)} %shard_map.121.refs_6_.refs_8_.table_ref), custom_call_target="tpu_custom_call" | custom-call | flops 536870912 | bytes 3145728 | tf_op jit(solution)/shard_map/pallas_call | solution.py:452
  (33 shorter events, 4.2 us)
Async XLA Ops:
  1.0 9.4 %collective-permute-start.4 = (bf16[2,2,256,128]{3,2,1,0:T(8,128)(2,1)S(1)}, bf16[2,2,256,128]{3,2,1,0:T(8,128)(2,1)S(1)}, u32[]{:S(2)}, u32[]{:S(2)}) collective-permute-start(bf16[2,2,256,128]{3,2,1,0:T(8,128)(2,1)S(1)} %pad_maximum_fusion.refs_3_), channel_id=1, source_target_pairs={{8,0},{16,8},{24,16},{28,24},{20,28},{12,20},{4,12},{0,4},{9,1},{1... | collective-permute-start | bytes 786440 | tf_op jit(solution)/shard_map/ppermute | solution.py:401
  4.0 8.0 %collective-permute-start = (bf16[2,2,256,128]{3,2,1,0:T(8,128)(2,1)S(1)}, bf16[2,2,256,128]{3,2,1,0:T(8,128)(2,1)S(1)}, u32[]{:S(2)}, u32[]{:S(2)}) collective-permute-start(bf16[2,2,256,128]{3,2,1,0:T(8,128)(2,1)S(1)} %pad_maximum_fusion.refs_3_), channel_id=1, source_target_pairs={{0,8},{8,16},{16,24},{24,28},{28,20},{20,12},{12,4},{4,0},{1,9},{9... | collective-permute-start | bytes 786440 | tf_op jit(solution)/shard_map/ppermute | solution.py:400
  10.4 7.5 %collective-permute-start.5 = (bf16[2,2,256,128]{3,2,1,0:T(8,128)(2,1)S(1)}, bf16[2,2,256,128]{3,2,1,0:T(8,128)(2,1)S(1)}, u32[]{:S(2)}, u32[]{:S(2)}) collective-permute-start(bf16[2,2,256,128]{3,2,1,0:T(8,128)(2,1)S(1)} %collective-permute-done.4.refs_4_), channel_id=1, source_target_pairs={{8,0},{16,8},{24,16},{28,24},{20,28},{12,20},{4,12},{0,4},{9,1},{1... | collective-permute-start | bytes 786440 | tf_op jit(solution)/shard_map/ppermute | solution.py:401
  12.1 7.2 %collective-permute-start.1 = (bf16[2,2,256,128]{3,2,1,0:T(8,128)(2,1)S(1)}, bf16[2,2,256,128]{3,2,1,0:T(8,128)(2,1)S(1)}, u32[]{:S(2)}, u32[]{:S(2)}) collective-permute-start(bf16[2,2,256,128]{3,2,1,0:T(8,128)(2,1)S(1)} %collective-permute-done.refs_3_), channel_id=1, source_target_pairs={{0,8},{8,16},{16,24},{24,28},{28,20},{20,12},{12,4},{4,0},{1,9},{9... | collective-permute-start | bytes 786440 | tf_op jit(solution)/shard_map/ppermute | solution.py:400
  12.8 1.0 copy-start.7
  17.9 6.6 %collective-permute-start.6 = (bf16[2,2,256,128]{3,2,1,0:T(8,128)(2,1)S(1)}, bf16[2,2,256,128]{3,2,1,0:T(8,128)(2,1)S(1)}, u32[]{:S(2)}, u32[]{:S(2)}) collective-permute-start(bf16[2,2,256,128]{3,2,1,0:T(8,128)(2,1)S(1)} %collective-permute-done.5.refs_4_), channel_id=1, source_target_pairs={{8,0},{16,8},{24,16},{28,24},{20,28},{12,20},{4,12},{0,4},{9,1},{1... | collective-permute-start | bytes 786440 | tf_op jit(solution)/shard_map/ppermute | solution.py:401
  19.3 6.4 %collective-permute-start.2 = (bf16[2,2,256,128]{3,2,1,0:T(8,128)(2,1)S(1)}, bf16[2,2,256,128]{3,2,1,0:T(8,128)(2,1)S(1)}, u32[]{:S(2)}, u32[]{:S(2)}) collective-permute-start(bf16[2,2,256,128]{3,2,1,0:T(8,128)(2,1)S(1)} %collective-permute-done.1.refs_3_), channel_id=1, source_target_pairs={{0,8},{8,16},{16,24},{24,28},{28,20},{20,12},{12,4},{4,0},{1,9},{9... | collective-permute-start | bytes 786440 | tf_op jit(solution)/shard_map/ppermute | solution.py:400
  24.5 5.0 %collective-permute-start.7 = (bf16[1,2,256,128]{3,2,1,0:T(8,128)(2,1)S(1)}, bf16[1,2,256,128]{3,2,1,0:T(8,128)(2,1)S(1)}, u32[]{:S(2)}, u32[]{:S(2)}) collective-permute-start(bf16[1,2,256,128]{3,2,1,0:T(8,128)(2,1)S(1)} %slice.9), channel_id=1, source_target_pairs={{8,0},{16,8},{24,16},{28,24},{20,28},{12,20},{4,12},{0,4},{9,1},{1... | collective-permute-start | bytes 393224 | tf_op jit(solution)/shard_map/ppermute | solution.py:401
  25.7 12.1 %copy-start = (bf16[1024,2048]{1,0:T(8,128)(2,1)S(1)}, bf16[1024,2048]{1,0:T(8,128)(2,1)}, u32[]{:S(2)}) copy-start(bf16[1024,2048]{1,0:T(8,128)(2,1)} %refs_4_.1) | copy-start | bytes 12582916
  25.7 12.1 %copy-start.1 = (bf16[128,2048]{1,0:T(8,128)(2,1)S(1)}, bf16[128,2048]{1,0:T(8,128)(2,1)}, u32[]{:S(2)}) copy-start(bf16[128,2048]{1,0:T(8,128)(2,1)} %refs_5_.1) | copy-start | bytes 1572868
  25.7 12.1 %copy-start.2 = (f32[2048]{0:T(1024)S(1)}, f32[2048]{0:T(1024)}, u32[]{:S(2)}) copy-start(f32[2048]{0:T(1024)} %param.17) | copy-start | bytes 24580
  25.7 12.1 %copy-start.3 = (f32[2048]{0:T(1024)S(1)}, f32[2048]{0:T(1024)}, u32[]{:S(2)}) copy-start(f32[2048]{0:T(1024)} %param.18) | copy-start | bytes 24580
  25.8 5.0 %collective-permute-start.3 = (bf16[1,2,256,128]{3,2,1,0:T(8,128)(2,1)S(1)}, bf16[1,2,256,128]{3,2,1,0:T(8,128)(2,1)S(1)}, u32[]{:S(2)}, u32[]{:S(2)}) collective-permute-start(bf16[1,2,256,128]{3,2,1,0:T(8,128)(2,1)S(1)} %slice.8), channel_id=1, source_target_pairs={{0,8},{8,16},{16,24},{24,28},{28,20},{20,12},{12,4},{4,0},{1,9},{9... | collective-permute-start | bytes 393224 | tf_op jit(solution)/shard_map/ppermute | solution.py:400
  30.8 62.1 %copy-start.6 = (bf16[1,1024,2048]{2,1,0:T(8,128)(2,1)S(1)}, bf16[1,1024,2048]{2,1,0:T(8,128)(2,1)}, u32[]{:S(2)}) copy-start(bf16[1,1024,2048]{2,1,0:T(8,128)(2,1)} %param.23) | copy-start | bytes 12582916
  32.1 1.9 %collective-permute-start.8 = (bf16[256,128]{1,0:T(8,128)(2,1)S(1)}, bf16[256,128]{1,0:T(8,128)(2,1)S(1)}, u32[]{:S(2)}, u32[]{:S(2)}) collective-permute-start(bf16[256,128]{1,0:T(8,128)(2,1)S(1)} %get-tuple-element.16), channel_id=1, source_target_pairs={{0,1},{1,0},{2,3},{3,2},{4,5},{5,4},{6,7},{7,6},{8,9},{9,8},{10,11... | collective-permute-start | bytes 196616 | tf_op jit(solution)/shard_map/ppermute | solution.py:219
  32.2 4.5 %collective-permute-start.9 = (bf16[256,128]{1,0:T(8,128)(2,1)S(1)}, bf16[256,128]{1,0:T(8,128)(2,1)S(1)}, u32[]{:S(2)}, u32[]{:S(2)}) collective-permute-start(bf16[256,128]{1,0:T(8,128)(2,1)S(1)} %get-tuple-element.17), channel_id=1, source_target_pairs={{0,2},{1,3},{2,0},{3,1},{4,6},{5,7},{6,4},{7,5},{8,10},{9,11},{10,... | collective-permute-start | bytes 196616 | tf_op jit(solution)/shard_map/ppermute | solution.py:219
  33.7 4.1 %collective-permute-start.10 = (bf16[256,128]{1,0:T(8,128)(2,1)S(1)}, bf16[256,128]{1,0:T(8,128)(2,1)S(1)}, u32[]{:S(2)}, u32[]{:S(2)}) collective-permute-start(bf16[256,128]{1,0:T(8,128)(2,1)S(1)} %get-tuple-element.18), channel_id=1, source_target_pairs={{0,3},{1,2},{2,1},{3,0},{4,7},{5,6},{6,5},{7,4},{8,11},{9,10},{10,... | collective-permute-start | bytes 196616 | tf_op jit(solution)/shard_map/ppermute | solution.py:219
  37.8 55.0 %copy-start.4 = (bf16[1,2048,1024]{2,1,0:T(8,128)(2,1)S(1)}, bf16[1,2048,1024]{2,1,0:T(8,128)(2,1)}, u32[]{:S(2)}) copy-start(bf16[1,2048,1024]{2,1,0:T(8,128)(2,1)} %param.21) | copy-start | bytes 12582916
  37.8 55.0 %copy-start.5 = (bf16[1,2048,1024]{2,1,0:T(8,128)(2,1)S(1)}, bf16[1,2048,1024]{2,1,0:T(8,128)(2,1)}, u32[]{:S(2)}) copy-start(bf16[1,2048,1024]{2,1,0:T(8,128)(2,1)} %param.22) | copy-start | bytes 12582916

commit v7 on v6

--- a/solution.py
+++ b/solution.py
@@ -79,7 +79,7 @@
     refs = list(refs)
     first_ref = refs.pop(0)
     cos_ref, sin_ref = refs.pop(0), refs.pop(0)
-    chunks = [refs.pop(0) for _ in pieces]
+    chunks = [(refs.pop(0), refs.pop(0)) for _ in pieces]
     acc_in = None if raw_queries else refs.pop(0)
     for _ in range(after):
         refs.pop(0)
@@ -87,7 +87,7 @@
     if last:
         outs, refs = refs[:-3], refs[-3:]
     keys_ref, values_ref = refs[0], refs[1]
-    lanes = chunks[0].shape[-1]
+    lanes = chunks[0][0].shape[-1]
     rotation = Rotation(cos_ref, sin_ref, lanes)
     me = lax.axis_index("sp")
     place = ring_place(me, sp_size)
@@ -117,12 +117,13 @@
     ones = jnp.ones((ONES_ROWS, HALF_KEYS), jnp.bfloat16)
     rows = HEAD_SIZE + ONES_ROWS
     halves = 0
-    for chunk, (distance, first_half) in zip(chunks, pieces):
+    for (k_ref, v_ref), (distance, first_half) in zip(chunks, pieces):
         source = ring_member(place + distance, sp_size)
-        for half in range(chunk.shape[0]):
+        for half in range(k_ref.shape[0] // HALF_KEYS):
+            span = slice(half * HALF_KEYS, (half + 1) * HALF_KEYS)
             row = source * grid_rows + (first_half + half) * (HALF_KEYS // GRID_W)
-            keys_ref[halves] = rotation.ready(chunk[half, 0], row, 1.0).astype(jnp.bfloat16)
-            turned = chunk[half, 1].astype(jnp.float32).T.astype(jnp.bfloat16)
+            keys_ref[halves] = rotation.ready(k_ref[span, :], row, 1.0).astype(jnp.bfloat16)
+            turned = v_ref[span, :].astype(jnp.float32).T.astype(jnp.bfloat16)
             for head in range(kv_heads):
                 values_ref[halves, head, :HEAD_SIZE, :] = turned[
                     head * HEAD_SIZE : (head + 1) * HEAD_SIZE
@@ -172,15 +173,15 @@
 
 def attend(queries, tables, chunks, pieces, acc, sp_size, tp_size, last=False, after=()):
     raw_queries = acc is None
-    lanes = chunks[0].shape[-1]
+    lanes = chunks[0][0].shape[-1]
     rows = HEAD_SIZE + ONES_ROWS
-    halves = sum(c.shape[0] for c in chunks)
+    halves = sum(k.shape[0] for k, _ in chunks) // HALF_KEYS
     if raw_queries:
         columns = queries.shape[0] * queries.shape[1] // HEAD_SIZE
         tok_count = queries.shape[0]
     else:
         columns = queries.shape[1]
-        tok_count = chunks[0].shape[0] * HALF_KEYS * 2
+        tok_count = chunks[0][0].shape[0] * 2
     scratch = [
         pltpu.VMEM((halves, HALF_KEYS, lanes), jnp.bfloat16),
         pltpu.VMEM((halves, lanes // HEAD_SIZE, rows, HALF_KEYS), jnp.bfloat16),
@@ -194,7 +195,8 @@
         shape = [jax.ShapeDtypeStruct((rows, columns), jnp.float32)]
         if raw_queries:
             shape = [jax.ShapeDtypeStruct((lanes, columns), jnp.bfloat16)] + shape
-    operands = [queries, *tables, *chunks] + ([] if raw_queries else [acc])
+    operands = [queries, *tables, *(part for chunk in chunks for part in chunk)]
+    operands += [] if raw_queries else [acc]
     aliases = {} if (raw_queries or last) else {len(operands) - 1: 0}
     key_count = halves * HALF_KEYS
     return pl.pallas_call(
@@ -367,11 +369,7 @@
     model_width = residual.shape[1]
     halves = tok_count // HALF_KEYS
     tables = rotation_tables(sp_size * tok_count // GRID_W, lanes)
-    raw_own = jnp.stack(
-        [part.reshape(halves, HALF_KEYS, lanes) for part in (projected_keys, projected_values)],
-        axis=1,
-    )
-
+    raw_own = (projected_keys, projected_values)
     row_count = residual.shape[0]
     top_count = route_expert.shape[1]
     experts = sp_size * tp_size
@@ -396,9 +394,12 @@
     held, pieces = [raw_own], [(0, 0)]
     for step in range(steps):
         if step == steps - 1:
-            from_left, from_right = from_left[: halves // 2], from_right[halves // 2 :]
-        next_left = lax.ppermute(from_left, "sp", ahead)
-        next_right = lax.ppermute(from_right, "sp", behind)
+            from_left = [part[: tok_count // 2] for part in from_left]
+            from_right = [part[tok_count // 2 :] for part in from_right]
+        next_left, next_right = [], []
+        for left, right in zip(from_left, from_right):
+            next_left.append(lax.ppermute(left, "sp", ahead))
+            next_right.append(lax.ppermute(right, "sp", behind))
         after = (table,) if step == steps - 1 else ()
         out = attend(queries, tables, held, pieces, acc, sp_size, tp_size, after=after)
         if step == 0:

time: 154 us -> 156 us (1.013)
  starting transfers between devices: 11.3 us -> 19.7 us
  waiting for transfers between devices: 12.9 us -> 5.77 us
  local copies, waits for them, and re-layouts: 2.57 us -> 4.4 us
    ppermute x8 -> x16, starting transfers between devices: 9.35 us -> 17.8 us  [the longest x8 16.4 us: local(): next_right.append(lax.ppermute(right, 'sp', behind))]
    ppermute x8 -> x16, waiting for transfers between devices: 9.08 us -> 1.98 us  [the longest x8 1.96 us: local(): next_left.append(lax.ppermute(left, 'sp', ahead))]
    unnamed x18 -> x22, local copies, waits for them, and re-layouts: 2.56 us -> 4.38 us
  transfers between devices with their start and end apart: 11 -> 19, of which waited for: 7 -> 3; matrix products, arithmetic and copies ran while one was open for 1% -> 1% of each run, Pallas kernels for 5% -> 5%
where the time goes in v7:
time: 156 us
  blocking collectives  105 us (67%)
  Pallas kernels  19.9 us (13%)
  starting transfers between devices  19.7 us (13%)
  waiting for transfers between devices  5.77 us (4%)
  local copies, waits for them, and re-layouts  4.4 us (3%)
    all_to_all x2, blocking collectives, exchange(): lax.all_to_all(slots, ('sp', 'tp'), split_axis=0, concat_axis=0, tiled=True)  105 us
    ppermute x8, starting transfers between devices, local(): next_right.append(lax.ppermute(right, 'sp', behind))  16.4 us
    pallas_call x5, Pallas kernels, attend(): pl.pallas_call(functools.partial(attend_kernel, sp_size, pieces, last, ra...  9.18 us
    pallas_call x1, Pallas kernels, local(): pl.pallas_call(expert_kernel, out_shape=slots_shape, in_specs=[VMEM] * 4,...  6.8 us
    unnamed x22, local copies, waits for them, and re-layouts  4.38 us
    ppermute x3, waiting for transfers between devices, direct_exchange(): lax.ppermute(pieces[rel], 'tp', [(i, i ^ rel) for i in range(tp_size)])  3.79 us
  transfers between devices with their start and end apart: 19, of which 3 were waited for; matrix products, arithmetic and copies ran while one was open for 1% of the time, Pallas kernels for 5%

profile of v7, /device:TPU:0, one launch (start us, length us, event | category | flops | bytes accessed | tf_op | source)
XLA Modules:
  0.0 155.8 jit_solution(12366501986612387897)
XLA Ops:
  0.0 3.0 %collective-permute-start.8 = (bf16[512,128]{1,0:T(8,128)(2,1)}, bf16[512,128]{1,0:T(8,128)(2,1)S(1)}, u32[]{:S(2)}, u32[]{:S(2)}) collective-permute-start(bf16[512,128]{1,0:T(8,128)(2,1)} %refs_3_.1), channel_id=1, source_target_pairs={{8,0},{16,8},{24,16},{28,24},{20,28},{12,20},{4,12},{0,4},{9,1},{1... | collective-permute-start | bytes 393224 | tf_op jit(solution)/shard_map/ppermute | solution.py:402
  3.1 1.9 %collective-permute-start.12 = (bf16[512,128]{1,0:T(8,128)(2,1)}, bf16[512,128]{1,0:T(8,128)(2,1)S(1)}, u32[]{:S(2)}, u32[]{:S(2)}) collective-permute-start(bf16[512,128]{1,0:T(8,128)(2,1)} %refs_4_.2), channel_id=1, source_target_pairs={{8,0},{16,8},{24,16},{28,24},{20,28},{12,20},{4,12},{0,4},{9,1},{1... | collective-permute-start | bytes 393224 | tf_op jit(solution)/shard_map/ppermute | solution.py:402
  7.4 1.0 copy-done.7
  8.4 0.9 copy-done.8
  10.2 1.5 shard_map.118
  11.8 2.0 %collective-permute-start.9 = (bf16[512,128]{1,0:T(8,128)(2,1)S(1)}, bf16[512,128]{1,0:T(8,128)(2,1)S(1)}, u32[]{:S(2)}, u32[]{:S(2)}) collective-permute-start(bf16[512,128]{1,0:T(8,128)(2,1)S(1)} %collective-permute-done.8.refs_5_), channel_id=1, source_target_pairs={{8,0},{16,8},{24,16},{28,24},{20,28},{12,20},{4,12},{0,4},{9,1},{1... | collective-permute-start | bytes 393224 | tf_op jit(solution)/shard_map/ppermute | solution.py:402
  13.9 1.9 %collective-permute-start.13 = (bf16[512,128]{1,0:T(8,128)(2,1)S(1)}, bf16[512,128]{1,0:T(8,128)(2,1)S(1)}, u32[]{:S(2)}, u32[]{:S(2)}) collective-permute-start(bf16[512,128]{1,0:T(8,128)(2,1)S(1)} %collective-permute-done.12.refs_6_), channel_id=1, source_target_pairs={{8,0},{16,8},{24,16},{28,24},{20,28},{12,20},{4,12},{0,4},{9,1},{1... | collective-permute-start | bytes 393224 | tf_op jit(solution)/shard_map/ppermute | solution.py:402
  15.9 2.1 %shard_map.119.refs_7_ = f32[80,2048]{1,0:T(8,128)S(1)} custom-call(bf16[128,2048]{1,0:T(8,128)(2,1)S(1)} %get-tuple-element.13.refs_0_, f32[128,128]{1,0:T(8,128)S(1)} %get-tuple-element.22.refs_1_, f32[128,128]{1,0:T(8,128)S(1)} %get-tuple-element.21.refs_2_, bf16[512,128]{1,0:T(8,128)(2,1)S(1)} %collective-permute-done.refs_3_, ...), custom_call_target="tpu_custom_call", output_to_operand_aliasing={{}: (7, {})} | custom-call | flops 2147483648 | bytes 1048576 | tf_op jit(solution)/shard_map/pallas_call | solution.py:202
  18.1 1.9 %collective-permute-start.10 = (bf16[512,128]{1,0:T(8,128)(2,1)S(1)}, bf16[512,128]{1,0:T(8,128)(2,1)S(1)}, u32[]{:S(2)}, u32[]{:S(2)}) collective-permute-start(bf16[512,128]{1,0:T(8,128)(2,1)S(1)} %collective-permute-done.9.refs_5_), channel_id=1, source_target_pairs={{8,0},{16,8},{24,16},{28,24},{20,28},{12,20},{4,12},{0,4},{9,1},{1... | collective-permute-start | bytes 393224 | tf_op jit(solution)/shard_map/ppermute | solution.py:402
  20.2 1.9 %collective-permute-start.14 = (bf16[512,128]{1,0:T(8,128)(2,1)S(1)}, bf16[512,128]{1,0:T(8,128)(2,1)S(1)}, u32[]{:S(2)}, u32[]{:S(2)}) collective-permute-start(bf16[512,128]{1,0:T(8,128)(2,1)S(1)} %collective-permute-done.13.refs_6_), channel_id=1, source_target_pairs={{8,0},{16,8},{24,16},{28,24},{20,28},{12,20},{4,12},{0,4},{9,1},{1... | collective-permute-start | bytes 393224 | tf_op jit(solution)/shard_map/ppermute | solution.py:402
  22.2 2.1 %shard_map.120.refs_7_ = f32[80,2048]{1,0:T(8,128)S(1)} custom-call(bf16[128,2048]{1,0:T(8,128)(2,1)S(1)} %get-tuple-element.13.refs_0_, f32[128,128]{1,0:T(8,128)S(1)} %get-tuple-element.22.refs_1_, f32[128,128]{1,0:T(8,128)S(1)} %get-tuple-element.21.refs_2_, bf16[512,128]{1,0:T(8,128)(2,1)S(1)} %collective-permute-done.1.refs_3_, ...), custom_call_target="tpu_custom_call", output_to_operand_aliasing={{}: (7, {})} | custom-call | flops 2147483648 | bytes 1048576 | tf_op jit(solution)/shard_map/pallas_call | solution.py:202
  24.3 1.9 %collective-permute-start.11 = (bf16[256,128]{1,0:T(8,128)(2,1)S(1)}, bf16[256,128]{1,0:T(8,128)(2,1)S(1)}, u32[]{:S(2)}, u32[]{:S(2)}) collective-permute-start(bf16[256,128]{1,0:T(8,128)(2,1)S(1)} %slice.18), channel_id=1, source_target_pairs={{8,0},{16,8},{24,16},{28,24},{20,28},{12,20},{4,12},{0,4},{9,1},{1... | collective-permute-start | bytes 196616 | tf_op jit(solution)/shard_map/ppermute | solution.py:402
  26.5 1.9 %collective-permute-start.15 = (bf16[256,128]{1,0:T(8,128)(2,1)S(1)}, bf16[256,128]{1,0:T(8,128)(2,1)S(1)}, u32[]{:S(2)}, u32[]{:S(2)}) collective-permute-start(bf16[256,128]{1,0:T(8,128)(2,1)S(1)} %slice.19), channel_id=1, source_target_pairs={{8,0},{16,8},{24,16},{28,24},{20,28},{12,20},{4,12},{0,4},{9,1},{1... | collective-permute-start | bytes 196616 | tf_op jit(solution)/shard_map/ppermute | solution.py:402
  28.9 2.1 %shard_map.122.refs_7_ = f32[80,2048]{1,0:T(8,128)S(1)} custom-call(bf16[128,2048]{1,0:T(8,128)(2,1)S(1)} %get-tuple-element.13.refs_0_, f32[128,128]{1,0:T(8,128)S(1)} %get-tuple-element.22.refs_1_, f32[128,128]{1,0:T(8,128)S(1)} %get-tuple-element.21.refs_2_, bf16[512,128]{1,0:T(8,128)(2,1)S(1)} %collective-permute-done.2.refs_3_, ...), custom_call_target="tpu_custom_call", output_to_operand_aliasing={{}: (7, {})} | custom-call | flops 2147483648 | bytes 1048576 | tf_op jit(solution)/shard_map/pallas_call | solution.py:202
  31.0 1.9 %collective-permute-done.7.refs_4_ = bf16[256,128]{1,0:T(8,128)(2,1)S(1)} collective-permute-done((bf16[256,128]{1,0:T(8,128)(2,1)S(1)}, bf16[256,128]{1,0:T(8,128)(2,1)S(1)}, u32[]{:S(2)}, u32[]{:S(2)}) %collective-permute-start.7) | collective-permute-done | bytes 65568 | tf_op jit(solution)/shard_map/ppermute | solution.py:401
  33.0 1.3 shard_map.123
  34.4 1.6 %collective-permute-start.17 = (bf16[256,128]{1,0:T(8,128)(2,1)S(1)}, bf16[256,128]{1,0:T(8,128)(2,1)S(1)}, u32[]{:S(2)}, u32[]{:S(2)}) collective-permute-start(bf16[256,128]{1,0:T(8,128)(2,1)S(1)} %get-tuple-element.17), channel_id=1, source_target_pairs={{0,2},{1,3},{2,0},{3,1},{4,6},{5,7},{6,4},{7,5},{8,10},{9,11},{10,... | collective-permute-start | bytes 196616 | tf_op jit(solution)/shard_map/ppermute | solution.py:221
  36.2 2.6 %collective-permute-done.17.refs_2_ = bf16[256,128]{1,0:T(8,128)(2,1)S(1)} collective-permute-done((bf16[256,128]{1,0:T(8,128)(2,1)S(1)}, bf16[256,128]{1,0:T(8,128)(2,1)S(1)}, u32[]{:S(2)}, u32[]{:S(2)}) %collective-permute-start.17) | collective-permute-done | bytes 65568 | tf_op jit(solution)/shard_map/ppermute | solution.py:221
  38.9 1.1 collective-permute-done.18.refs_3_
  40.1 1.9 %shard_map.124 = (bf16[128,2048]{1,0:T(8,128)(2,1)S(1)}, bf16[512,2048]{1,0:T(8,128)(2,1)S(1)}) custom-call(bf16[256,128]{1,0:T(8,128)(2,1)S(1)} %get-tuple-element.15.refs_0_, bf16[256,128]{1,0:T(8,128)(2,1)S(1)} %collective-permute-done.16.refs_1_, bf16[256,128]{1,0:T(8,128)(2,1)S(1)} %collective-permute-done.17.refs_2_, ...), custom_call_target="tpu_custom_call" | custom-call | flops 805306368 | bytes 8388608 | tf_op jit(solution)/shard_map/pallas_call | solution.py:417
  41.9 53.1 %all_to_all.10 = bf16[32,16,2048]{2,1,0:T(8,128)(2,1)S(1)} all-to-all(bf16[32,16,2048]{2,1,0:T(8,128)(2,1)S(1)} %bitcast.10), channel_id=1, replica_groups=mesh['sp'=8,'tp'=4] {'sp','tp'}, dimensions={0} | all-to-all | bytes 4194304 | tf_op jit(solution)/shard_map/all_to_all | solution.py:436
  95.1 6.8 %shard_map.125 = bf16[512,2048]{1,0:T(8,128)(2,1)S(1)} custom-call(bf16[512,2048]{1,0:T(8,128)(2,1)S(1)} %bitcast.11, bf16[2048,1024]{1,0:T(8,128)(2,1)S(1)} %bitcast.15, bf16[2048,1024]{1,0:T(8,128)(2,1)S(1)} %bitcast.16, bf16[1024,2048]{1,0:T(8,128)(2,1)S(1)} %bitcast.17), custom_call_target="tpu_custom_call" | custom-call | flops 6442450944 | bytes 16777216 | tf_op jit(solution)/shard_map/pallas_call | solution.py:440
  101.9 52.1 %all_to_all.11 = bf16[32,16,2048]{2,1,0:T(8,128)(2,1)S(1)} all-to-all(bf16[32,16,2048]{2,1,0:T(8,128)(2,1)S(1)} %bitcast.12), channel_id=1, replica_groups=mesh['sp'=8,'tp'=4] {'sp','tp'}, dimensions={0} | all-to-all | bytes 4194304 | tf_op jit(solution)/shard_map/all_to_all | solution.py:436
  154.0 1.6 %shard_map.126 = bf16[128,2048]{1,0:T(8,128)(2,1)} custom-call(bf16[128,2048]{1,0:T(8,128)(2,1)S(1)} %get-tuple-element.19.base_ref, bf16[512,2048]{1,0:T(8,128)(2,1)S(1)} %bitcast.9, f32[8,128]{1,0:T(8,128)S(1)} %shard_map.121.refs_8_.table_ref), custom_call_target="tpu_custom_call" | custom-call | flops 536870912 | bytes 3145728 | tf_op jit(solution)/shard_map/pallas_call | solution.py:453
  (54 shorter events, 5.1 us)
Async XLA Ops:
  0.0 11.7 %collective-permute-start.8 = (bf16[512,128]{1,0:T(8,128)(2,1)}, bf16[512,128]{1,0:T(8,128)(2,1)S(1)}, u32[]{:S(2)}, u32[]{:S(2)}) collective-permute-start(bf16[512,128]{1,0:T(8,128)(2,1)} %refs_3_.1), channel_id=1, source_target_pairs={{8,0},{16,8},{24,16},{28,24},{20,28},{12,20},{4,12},{0,4},{9,1},{1... | collective-permute-start | bytes 393224 | tf_op jit(solution)/shard_map/ppermute | solution.py:402
  3.0 10.8 %collective-permute-start = (bf16[512,128]{1,0:T(8,128)(2,1)}, bf16[512,128]{1,0:T(8,128)(2,1)S(1)}, u32[]{:S(2)}, u32[]{:S(2)}) collective-permute-start(bf16[512,128]{1,0:T(8,128)(2,1)} %refs_3_.1), channel_id=1, source_target_pairs={{0,8},{8,16},{16,24},{24,28},{28,20},{20,12},{12,4},{4,0},{1,9},{9... | collective-permute-start | bytes 393224 | tf_op jit(solution)/shard_map/ppermute | solution.py:401
  3.1 10.9 %collective-permute-start.12 = (bf16[512,128]{1,0:T(8,128)(2,1)}, bf16[512,128]{1,0:T(8,128)(2,1)S(1)}, u32[]{:S(2)}, u32[]{:S(2)}) collective-permute-start(bf16[512,128]{1,0:T(8,128)(2,1)} %refs_4_.2), channel_id=1, source_target_pairs={{8,0},{16,8},{24,16},{28,24},{20,28},{12,20},{4,12},{0,4},{9,1},{1... | collective-permute-start | bytes 393224 | tf_op jit(solution)/shard_map/ppermute | solution.py:402
  5.0 10.8 %collective-permute-start.4 = (bf16[512,128]{1,0:T(8,128)(2,1)}, bf16[512,128]{1,0:T(8,128)(2,1)S(1)}, u32[]{:S(2)}, u32[]{:S(2)}) collective-permute-start(bf16[512,128]{1,0:T(8,128)(2,1)} %refs_4_.2), channel_id=1, source_target_pairs={{0,8},{8,16},{16,24},{24,28},{28,20},{20,12},{12,4},{4,0},{1,9},{9... | collective-permute-start | bytes 393224 | tf_op jit(solution)/shard_map/ppermute | solution.py:401
  11.8 6.3 %collective-permute-start.9 = (bf16[512,128]{1,0:T(8,128)(2,1)S(1)}, bf16[512,128]{1,0:T(8,128)(2,1)S(1)}, u32[]{:S(2)}, u32[]{:S(2)}) collective-permute-start(bf16[512,128]{1,0:T(8,128)(2,1)S(1)} %collective-permute-done.8.refs_5_), channel_id=1, source_target_pairs={{8,0},{16,8},{24,16},{28,24},{20,28},{12,20},{4,12},{0,4},{9,1},{1... | collective-permute-start | bytes 393224 | tf_op jit(solution)/shard_map/ppermute | solution.py:402
  13.7 6.3 %collective-permute-start.1 = (bf16[512,128]{1,0:T(8,128)(2,1)S(1)}, bf16[512,128]{1,0:T(8,128)(2,1)S(1)}, u32[]{:S(2)}, u32[]{:S(2)}) collective-permute-start(bf16[512,128]{1,0:T(8,128)(2,1)S(1)} %collective-permute-done.refs_3_), channel_id=1, source_target_pairs={{0,8},{8,16},{16,24},{24,28},{28,20},{20,12},{12,4},{4,0},{1,9},{9... | collective-permute-start | bytes 393224 | tf_op jit(solution)/shard_map/ppermute | solution.py:401
  13.9 6.3 %collective-permute-start.13 = (bf16[512,128]{1,0:T(8,128)(2,1)S(1)}, bf16[512,128]{1,0:T(8,128)(2,1)S(1)}, u32[]{:S(2)}, u32[]{:S(2)}) collective-permute-start(bf16[512,128]{1,0:T(8,128)(2,1)S(1)} %collective-permute-done.12.refs_6_), channel_id=1, source_target_pairs={{8,0},{16,8},{24,16},{28,24},{20,28},{12,20},{4,12},{0,4},{9,1},{1... | collective-permute-start | bytes 393224 | tf_op jit(solution)/shard_map/ppermute | solution.py:402
  15.8 6.3 %collective-permute-start.5 = (bf16[512,128]{1,0:T(8,128)(2,1)S(1)}, bf16[512,128]{1,0:T(8,128)(2,1)S(1)}, u32[]{:S(2)}, u32[]{:S(2)}) collective-permute-start(bf16[512,128]{1,0:T(8,128)(2,1)S(1)} %collective-permute-done.4.refs_4_), channel_id=1, source_target_pairs={{0,8},{8,16},{16,24},{24,28},{28,20},{20,12},{12,4},{4,0},{1,9},{9... | collective-permute-start | bytes 393224 | tf_op jit(solution)/shard_map/ppermute | solution.py:401
  18.1 6.2 %collective-permute-start.10 = (bf16[512,128]{1,0:T(8,128)(2,1)S(1)}, bf16[512,128]{1,0:T(8,128)(2,1)S(1)}, u32[]{:S(2)}, u32[]{:S(2)}) collective-permute-start(bf16[512,128]{1,0:T(8,128)(2,1)S(1)} %collective-permute-done.9.refs_5_), channel_id=1, source_target_pairs={{8,0},{16,8},{24,16},{28,24},{20,28},{12,20},{4,12},{0,4},{9,1},{1... | collective-permute-start | bytes 393224 | tf_op jit(solution)/shard_map/ppermute | solution.py:402
  20.0 6.3 %collective-permute-start.2 = (bf16[512,128]{1,0:T(8,128)(2,1)S(1)}, bf16[512,128]{1,0:T(8,128)(2,1)S(1)}, u32[]{:S(2)}, u32[]{:S(2)}) collective-permute-start(bf16[512,128]{1,0:T(8,128)(2,1)S(1)} %collective-permute-done.1.refs_3_), channel_id=1, source_target_pairs={{0,8},{8,16},{16,24},{24,28},{28,20},{20,12},{12,4},{4,0},{1,9},{9... | collective-permute-start | bytes 393224 | tf_op jit(solution)/shard_map/ppermute | solution.py:401
  20.2 6.3 %collective-permute-start.14 = (bf16[512,128]{1,0:T(8,128)(2,1)S(1)}, bf16[512,128]{1,0:T(8,128)(2,1)S(1)}, u32[]{:S(2)}, u32[]{:S(2)}) collective-permute-start(bf16[512,128]{1,0:T(8,128)(2,1)S(1)} %collective-permute-done.13.refs_6_), channel_id=1, source_target_pairs={{8,0},{16,8},{24,16},{28,24},{20,28},{12,20},{4,12},{0,4},{9,1},{1... | collective-permute-start | bytes 393224 | tf_op jit(solution)/shard_map/ppermute | solution.py:402
  22.0 6.4 %collective-permute-start.6 = (bf16[512,128]{1,0:T(8,128)(2,1)S(1)}, bf16[512,128]{1,0:T(8,128)(2,1)S(1)}, u32[]{:S(2)}, u32[]{:S(2)}) collective-permute-start(bf16[512,128]{1,0:T(8,128)(2,1)S(1)} %collective-permute-done.5.refs_4_), channel_id=1, source_target_pairs={{0,8},{8,16},{16,24},{24,28},{28,20},{20,12},{12,4},{4,0},{1,9},{9... | collective-permute-start | bytes 393224 | tf_op jit(solution)/shard_map/ppermute | solution.py:401
  24.3 6.7 %collective-permute-start.11 = (bf16[256,128]{1,0:T(8,128)(2,1)S(1)}, bf16[256,128]{1,0:T(8,128)(2,1)S(1)}, u32[]{:S(2)}, u32[]{:S(2)}) collective-permute-start(bf16[256,128]{1,0:T(8,128)(2,1)S(1)} %slice.18), channel_id=1, source_target_pairs={{8,0},{16,8},{24,16},{28,24},{20,28},{12,20},{4,12},{0,4},{9,1},{1... | collective-permute-start | bytes 196616 | tf_op jit(solution)/shard_map/ppermute | solution.py:402
  26.3 4.7 %collective-permute-start.3 = (bf16[256,128]{1,0:T(8,128)(2,1)S(1)}, bf16[256,128]{1,0:T(8,128)(2,1)S(1)}, u32[]{:S(2)}, u32[]{:S(2)}) collective-permute-start(bf16[256,128]{1,0:T(8,128)(2,1)S(1)} %slice.16), channel_id=1, source_target_pairs={{0,8},{8,16},{16,24},{24,28},{28,20},{20,12},{12,4},{4,0},{1,9},{9... | collective-permute-start | bytes 196616 | tf_op jit(solution)/shard_map/ppermute | solution.py:401
  26.5 4.5 %collective-permute-start.15 = (bf16[256,128]{1,0:T(8,128)(2,1)S(1)}, bf16[256,128]{1,0:T(8,128)(2,1)S(1)}, u32[]{:S(2)}, u32[]{:S(2)}) collective-permute-start(bf16[256,128]{1,0:T(8,128)(2,1)S(1)} %slice.19), channel_id=1, source_target_pairs={{8,0},{16,8},{24,16},{28,24},{20,28},{12,20},{4,12},{0,4},{9,1},{1... | collective-permute-start | bytes 196616 | tf_op jit(solution)/shard_map/ppermute | solution.py:402
  28.4 11.6 %copy-start = (bf16[1024,2048]{1,0:T(8,128)(2,1)S(1)}, bf16[1024,2048]{1,0:T(8,128)(2,1)}, u32[]{:S(2)}) copy-start(bf16[1024,2048]{1,0:T(8,128)(2,1)} %refs_4_.3) | copy-start | bytes 12582916
  28.4 11.6 %copy-start.1 = (bf16[128,2048]{1,0:T(8,128)(2,1)S(1)}, bf16[128,2048]{1,0:T(8,128)(2,1)}, u32[]{:S(2)}) copy-start(bf16[128,2048]{1,0:T(8,128)(2,1)} %refs_5_.1) | copy-start | bytes 1572868
  28.5 4.5 %collective-permute-start.7 = (bf16[256,128]{1,0:T(8,128)(2,1)S(1)}, bf16[256,128]{1,0:T(8,128)(2,1)S(1)}, u32[]{:S(2)}, u32[]{:S(2)}) collective-permute-start(bf16[256,128]{1,0:T(8,128)(2,1)S(1)} %slice.17), channel_id=1, source_target_pairs={{0,8},{8,16},{16,24},{24,28},{28,20},{20,12},{12,4},{4,0},{1,9},{9... | collective-permute-start | bytes 196616 | tf_op jit(solution)/shard_map/ppermute | solution.py:401
  33.0 62.1 %copy-start.6 = (bf16[1,1024,2048]{2,1,0:T(8,128)(2,1)S(1)}, bf16[1,1024,2048]{2,1,0:T(8,128)(2,1)}, u32[]{:S(2)}) copy-start(bf16[1,1024,2048]{2,1,0:T(8,128)(2,1)} %param.23) | copy-start | bytes 12582916
  34.3 1.9 %collective-permute-start.16 = (bf16[256,128]{1,0:T(8,128)(2,1)S(1)}, bf16[256,128]{1,0:T(8,128)(2,1)S(1)}, u32[]{:S(2)}, u32[]{:S(2)}) collective-permute-start(bf16[256,128]{1,0:T(8,128)(2,1)S(1)} %get-tuple-element.16), channel_id=1, source_target_pairs={{0,1},{1,0},{2,3},{3,2},{4,5},{5,4},{6,7},{7,6},{8,9},{9,8},{10,11... | collective-permute-start | bytes 196616 | tf_op jit(solution)/shard_map/ppermute | solution.py:221
  34.4 4.5 %collective-permute-start.17 = (bf16[256,128]{1,0:T(8,128)(2,1)S(1)}, bf16[256,128]{1,0:T(8,128)(2,1)S(1)}, u32[]{:S(2)}, u32[]{:S(2)}) collective-permute-start(bf16[256,128]{1,0:T(8,128)(2,1)S(1)} %get-tuple-element.17), channel_id=1, source_target_pairs={{0,2},{1,3},{2,0},{3,1},{4,6},{5,7},{6,4},{7,5},{8,10},{9,11},{10,... | collective-permute-start | bytes 196616 | tf_op jit(solution)/shard_map/ppermute | solution.py:221
  35.9 4.1 %collective-permute-start.18 = (bf16[256,128]{1,0:T(8,128)(2,1)S(1)}, bf16[256,128]{1,0:T(8,128)(2,1)S(1)}, u32[]{:S(2)}, u32[]{:S(2)}) collective-permute-start(bf16[256,128]{1,0:T(8,128)(2,1)S(1)} %get-tuple-element.18), channel_id=1, source_target_pairs={{0,3},{1,2},{2,1},{3,0},{4,7},{5,6},{6,5},{7,4},{8,11},{9,10},{10,... | collective-permute-start | bytes 196616 | tf_op jit(solution)/shard_map/ppermute | solution.py:221
  40.0 55.1 %copy-start.4 = (bf16[1,2048,1024]{2,1,0:T(8,128)(2,1)S(1)}, bf16[1,2048,1024]{2,1,0:T(8,128)(2,1)}, u32[]{:S(2)}) copy-start(bf16[1,2048,1024]{2,1,0:T(8,128)(2,1)} %param.21) | copy-start | bytes 12582916
  40.0 55.0 %copy-start.5 = (bf16[1,2048,1024]{2,1,0:T(8,128)(2,1)S(1)}, bf16[1,2048,1024]{2,1,0:T(8,128)(2,1)}, u32[]{:S(2)}) copy-start(bf16[1,2048,1024]{2,1,0:T(8,128)(2,1)} %param.22) | copy-start | bytes 12582916
  (5 other events, 25.9 us)

commit v8 on v6

--- a/solution.py
+++ b/solution.py
@@ -408,7 +408,8 @@
         from_left, from_right = next_left, next_right
         held = [from_left, from_right]
         pieces = [(-step - 1, 0), (step + 1, halves // 2 if step == steps - 1 else 0)]
-    pieces = attend(queries, tables, held, pieces, acc, sp_size, tp_size, last=True)
+    (acc,) = attend(queries, tables, held[1:], pieces[1:], acc, sp_size, tp_size)
+    pieces = attend(queries, tables, held[:1], pieces[:1], acc, sp_size, tp_size, last=True)
     blocks = direct_exchange(pieces, tp_size)
 
     rows_shape = jax.ShapeDtypeStruct((row_count, model_width), jnp.bfloat16)

time: 154 us -> 154 us (level)
    pallas_call x5 -> x6, Pallas kernels: 9.2 us -> 9.68 us  [attend(): pl.pallas_call(functools.partial(attend_kernel, sp_size, pieces, last, ra...]
  transfers between devices with their start and end apart: 11 -> 11, of which waited for: 7 -> 7; matrix products, arithmetic and copies ran while one was open for 1% -> 1% of each run, Pallas kernels for 5% -> 6%
where the time goes in v8:
time: 154 us; the launch traced here: 153 us
  blocking collectives  106 us (69%)
  Pallas kernels  20.4 us (13%)
  waiting for transfers between devices  12 us (8%)
  starting transfers between devices  11.3 us (7%)
  local copies, waits for them, and re-layouts  2.57 us (2%)
    all_to_all x2, blocking collectives, exchange(): lax.all_to_all(slots, ('sp', 'tp'), split_axis=0, concat_axis=0, tiled=True)  106 us
    pallas_call x6, Pallas kernels, attend(): pl.pallas_call(functools.partial(attend_kernel, sp_size, pieces, last, ra...  9.68 us
    ppermute x4, waiting for transfers between devices, local(): next_right = lax.ppermute(from_right, 'sp', behind)  7.87 us
    ppermute x4, starting transfers between devices, local(): next_right = lax.ppermute(from_right, 'sp', behind)  7.23 us
    pallas_call x1, Pallas kernels, local(): pl.pallas_call(expert_kernel, out_shape=slots_shape, in_specs=[VMEM] * 4,...  6.8 us
    ppermute x3, waiting for transfers between devices, direct_exchange(): lax.ppermute(pieces[rel], 'tp', [(i, i ^ rel) for i in range(tp_size)])  3.79 us
  transfers between devices with their start and end apart: 11, of which 7 were waited for; matrix products, arithmetic and copies ran while one was open for 1% of the time, Pallas kernels for 6%

profile of v8, /device:TPU:0, one launch (start us, length us, event | category | flops | bytes accessed | tf_op | source)
XLA Modules:
  0.0 153.4 jit_solution(6898626282859663971)
XLA Ops:
  0.0 1.0 pad_maximum_fusion.refs_3_
  1.0 3.0 %collective-permute-start.4 = (bf16[2,2,256,128]{3,2,1,0:T(8,128)(2,1)S(1)}, bf16[2,2,256,128]{3,2,1,0:T(8,128)(2,1)S(1)}, u32[]{:S(2)}, u32[]{:S(2)}) collective-permute-start(bf16[2,2,256,128]{3,2,1,0:T(8,128)(2,1)S(1)} %pad_maximum_fusion.refs_3_), channel_id=1, source_target_pairs={{8,0},{16,8},{24,16},{28,24},{20,28},{12,20},{4,12},{0,4},{9,1},{1... | collective-permute-start | bytes 786440 | tf_op jit(solution)/shard_map/ppermute | solution.py:401
  4.2 0.8 copy.17.expert_ref
  6.2 4.2 %collective-permute-done.4.refs_4_ = bf16[2,2,256,128]{3,2,1,0:T(8,128)(2,1)S(1)} collective-permute-done((bf16[2,2,256,128]{3,2,1,0:T(8,128)(2,1)S(1)}, bf16[2,2,256,128]{3,2,1,0:T(8,128)(2,1)S(1)}, u32[]{:S(2)}, u32[]{:S(2)}) %collective-permute-start.4) | collective-permute-done | bytes 262176 | tf_op jit(solution)/shard_map/ppermute | solution.py:401
  10.4 1.7 %collective-permute-start.5 = (bf16[2,2,256,128]{3,2,1,0:T(8,128)(2,1)S(1)}, bf16[2,2,256,128]{3,2,1,0:T(8,128)(2,1)S(1)}, u32[]{:S(2)}, u32[]{:S(2)}) collective-permute-start(bf16[2,2,256,128]{3,2,1,0:T(8,128)(2,1)S(1)} %collective-permute-done.4.refs_4_), channel_id=1, source_target_pairs={{8,0},{16,8},{24,16},{28,24},{20,28},{12,20},{4,12},{0,4},{9,1},{1... | collective-permute-start | bytes 786440 | tf_op jit(solution)/shard_map/ppermute | solution.py:401
  12.8 0.9 copy-done.7
  13.7 1.5 shard_map.118
  15.2 2.7 %collective-permute-done.5.refs_4_ = bf16[2,2,256,128]{3,2,1,0:T(8,128)(2,1)S(1)} collective-permute-done((bf16[2,2,256,128]{3,2,1,0:T(8,128)(2,1)S(1)}, bf16[2,2,256,128]{3,2,1,0:T(8,128)(2,1)S(1)}, u32[]{:S(2)}, u32[]{:S(2)}) %collective-permute-start.5) | collective-permute-done | bytes 262176 | tf_op jit(solution)/shard_map/ppermute | solution.py:401
  17.9 1.4 collective-permute-start.6
  19.9 2.1 %shard_map.119.refs_5_ = f32[80,2048]{1,0:T(8,128)S(1)} custom-call(bf16[128,2048]{1,0:T(8,128)(2,1)S(1)} %get-tuple-element.13.refs_0_, f32[128,128]{1,0:T(8,128)S(1)} %get-tuple-element.22.refs_1_, f32[128,128]{1,0:T(8,128)S(1)} %get-tuple-element.21.refs_2_, ...), custom_call_target="tpu_custom_call", output_to_operand_aliasing={{}: (5, {})} | custom-call | flops 2147483648 | bytes 1048576 | tf_op jit(solution)/shard_map/pallas_call | solution.py:200
  22.0 2.1 %shard_map.120.refs_5_ = f32[80,2048]{1,0:T(8,128)S(1)} custom-call(bf16[128,2048]{1,0:T(8,128)(2,1)S(1)} %get-tuple-element.13.refs_0_, f32[128,128]{1,0:T(8,128)S(1)} %get-tuple-element.22.refs_1_, f32[128,128]{1,0:T(8,128)S(1)} %get-tuple-element.21.refs_2_, ...), custom_call_target="tpu_custom_call", output_to_operand_aliasing={{}: (5, {})} | custom-call | flops 2147483648 | bytes 1048576 | tf_op jit(solution)/shard_map/pallas_call | solution.py:200
  24.5 1.2 collective-permute-start.7
  25.8 0.9 collective-permute-start.3
  26.7 2.1 %shard_map.122.refs_4_ = f32[80,2048]{1,0:T(8,128)S(1)} custom-call(bf16[128,2048]{1,0:T(8,128)(2,1)S(1)} %get-tuple-element.13.refs_0_, f32[128,128]{1,0:T(8,128)S(1)} %get-tuple-element.22.refs_1_, f32[128,128]{1,0:T(8,128)S(1)} %get-tuple-element.21.refs_2_, ...), custom_call_target="tpu_custom_call", output_to_operand_aliasing={{}: (5, {})} | custom-call | flops 2147483648 | bytes 1048576 | tf_op jit(solution)/shard_map/pallas_call | solution.py:200
  29.5 0.9 shard_map.123.refs_4_
  30.8 0.9 shard_map.124
  31.8 1.6 %collective-permute-start.9 = (bf16[256,128]{1,0:T(8,128)(2,1)S(1)}, bf16[256,128]{1,0:T(8,128)(2,1)S(1)}, u32[]{:S(2)}, u32[]{:S(2)}) collective-permute-start(bf16[256,128]{1,0:T(8,128)(2,1)S(1)} %get-tuple-element.17), channel_id=1, source_target_pairs={{0,2},{1,3},{2,0},{3,1},{4,6},{5,7},{6,4},{7,5},{8,10},{9,11},{10,... | collective-permute-start | bytes 196616 | tf_op jit(solution)/shard_map/ppermute | solution.py:219
  33.6 2.6 %collective-permute-done.9.refs_2_ = bf16[256,128]{1,0:T(8,128)(2,1)S(1)} collective-permute-done((bf16[256,128]{1,0:T(8,128)(2,1)S(1)}, bf16[256,128]{1,0:T(8,128)(2,1)S(1)}, u32[]{:S(2)}, u32[]{:S(2)}) %collective-permute-start.9) | collective-permute-done | bytes 65568 | tf_op jit(solution)/shard_map/ppermute | solution.py:219
  36.3 1.1 collective-permute-done.10.refs_3_
  37.5 1.9 %shard_map.125 = (bf16[128,2048]{1,0:T(8,128)(2,1)S(1)}, bf16[512,2048]{1,0:T(8,128)(2,1)S(1)}) custom-call(bf16[256,128]{1,0:T(8,128)(2,1)S(1)} %get-tuple-element.15.refs_0_, bf16[256,128]{1,0:T(8,128)(2,1)S(1)} %collective-permute-done.8.refs_1_, bf16[256,128]{1,0:T(8,128)(2,1)S(1)} %collective-permute-done.9.refs_2_, ...), custom_call_target="tpu_custom_call" | custom-call | flops 805306368 | bytes 8388608 | tf_op jit(solution)/shard_map/pallas_call | solution.py:417
  39.3 53.4 %all_to_all.10 = bf16[32,16,2048]{2,1,0:T(8,128)(2,1)S(1)} all-to-all(bf16[32,16,2048]{2,1,0:T(8,128)(2,1)S(1)} %bitcast.12), channel_id=1, replica_groups=mesh['sp'=8,'tp'=4] {'sp','tp'}, dimensions={0} | all-to-all | bytes 4194304 | tf_op jit(solution)/shard_map/all_to_all | solution.py:436
  92.7 6.8 %shard_map.126 = bf16[512,2048]{1,0:T(8,128)(2,1)S(1)} custom-call(bf16[512,2048]{1,0:T(8,128)(2,1)S(1)} %bitcast.13, bf16[2048,1024]{1,0:T(8,128)(2,1)S(1)} %bitcast.17, bf16[2048,1024]{1,0:T(8,128)(2,1)S(1)} %bitcast.18, bf16[1024,2048]{1,0:T(8,128)(2,1)S(1)} %bitcast.19), custom_call_target="tpu_custom_call" | custom-call | flops 6442450944 | bytes 16777216 | tf_op jit(solution)/shard_map/pallas_call | solution.py:440
  99.5 52.2 %all_to_all.11 = bf16[32,16,2048]{2,1,0:T(8,128)(2,1)S(1)} all-to-all(bf16[32,16,2048]{2,1,0:T(8,128)(2,1)S(1)} %bitcast.14), channel_id=1, replica_groups=mesh['sp'=8,'tp'=4] {'sp','tp'}, dimensions={0} | all-to-all | bytes 4194304 | tf_op jit(solution)/shard_map/all_to_all | solution.py:436
  151.7 1.6 %shard_map.127 = bf16[128,2048]{1,0:T(8,128)(2,1)} custom-call(bf16[128,2048]{1,0:T(8,128)(2,1)S(1)} %get-tuple-element.19.base_ref, bf16[512,2048]{1,0:T(8,128)(2,1)S(1)} %bitcast.11, f32[8,128]{1,0:T(8,128)S(1)} %shard_map.121.refs_6_.refs_8_.table_ref), custom_call_target="tpu_custom_call" | custom-call | flops 536870912 | bytes 3145728 | tf_op jit(solution)/shard_map/pallas_call | solution.py:453
  (34 shorter events, 4.5 us)
Async XLA Ops:
  1.0 9.4 %collective-permute-start.4 = (bf16[2,2,256,128]{3,2,1,0:T(8,128)(2,1)S(1)}, bf16[2,2,256,128]{3,2,1,0:T(8,128)(2,1)S(1)}, u32[]{:S(2)}, u32[]{:S(2)}) collective-permute-start(bf16[2,2,256,128]{3,2,1,0:T(8,128)(2,1)S(1)} %pad_maximum_fusion.refs_3_), channel_id=1, source_target_pairs={{8,0},{16,8},{24,16},{28,24},{20,28},{12,20},{4,12},{0,4},{9,1},{1... | collective-permute-start | bytes 786440 | tf_op jit(solution)/shard_map/ppermute | solution.py:401
  4.0 8.0 %collective-permute-start = (bf16[2,2,256,128]{3,2,1,0:T(8,128)(2,1)S(1)}, bf16[2,2,256,128]{3,2,1,0:T(8,128)(2,1)S(1)}, u32[]{:S(2)}, u32[]{:S(2)}) collective-permute-start(bf16[2,2,256,128]{3,2,1,0:T(8,128)(2,1)S(1)} %pad_maximum_fusion.refs_3_), channel_id=1, source_target_pairs={{0,8},{8,16},{16,24},{24,28},{28,20},{20,12},{12,4},{4,0},{1,9},{9... | collective-permute-start | bytes 786440 | tf_op jit(solution)/shard_map/ppermute | solution.py:400
  10.4 7.5 %collective-permute-start.5 = (bf16[2,2,256,128]{3,2,1,0:T(8,128)(2,1)S(1)}, bf16[2,2,256,128]{3,2,1,0:T(8,128)(2,1)S(1)}, u32[]{:S(2)}, u32[]{:S(2)}) collective-permute-start(bf16[2,2,256,128]{3,2,1,0:T(8,128)(2,1)S(1)} %collective-permute-done.4.refs_4_), channel_id=1, source_target_pairs={{8,0},{16,8},{24,16},{28,24},{20,28},{12,20},{4,12},{0,4},{9,1},{1... | collective-permute-start | bytes 786440 | tf_op jit(solution)/shard_map/ppermute | solution.py:401
  12.1 7.2 %collective-permute-start.1 = (bf16[2,2,256,128]{3,2,1,0:T(8,128)(2,1)S(1)}, bf16[2,2,256,128]{3,2,1,0:T(8,128)(2,1)S(1)}, u32[]{:S(2)}, u32[]{:S(2)}) collective-permute-start(bf16[2,2,256,128]{3,2,1,0:T(8,128)(2,1)S(1)} %collective-permute-done.refs_3_), channel_id=1, source_target_pairs={{0,8},{8,16},{16,24},{24,28},{28,20},{20,12},{12,4},{4,0},{1,9},{9... | collective-permute-start | bytes 786440 | tf_op jit(solution)/shard_map/ppermute | solution.py:400
  12.8 1.0 copy-start.7
  17.9 6.6 %collective-permute-start.6 = (bf16[2,2,256,128]{3,2,1,0:T(8,128)(2,1)S(1)}, bf16[2,2,256,128]{3,2,1,0:T(8,128)(2,1)S(1)}, u32[]{:S(2)}, u32[]{:S(2)}) collective-permute-start(bf16[2,2,256,128]{3,2,1,0:T(8,128)(2,1)S(1)} %collective-permute-done.5.refs_4_), channel_id=1, source_target_pairs={{8,0},{16,8},{24,16},{28,24},{20,28},{12,20},{4,12},{0,4},{9,1},{1... | collective-permute-start | bytes 786440 | tf_op jit(solution)/shard_map/ppermute | solution.py:401
  19.3 6.4 %collective-permute-start.2 = (bf16[2,2,256,128]{3,2,1,0:T(8,128)(2,1)S(1)}, bf16[2,2,256,128]{3,2,1,0:T(8,128)(2,1)S(1)}, u32[]{:S(2)}, u32[]{:S(2)}) collective-permute-start(bf16[2,2,256,128]{3,2,1,0:T(8,128)(2,1)S(1)} %collective-permute-done.1.refs_3_), channel_id=1, source_target_pairs={{0,8},{8,16},{16,24},{24,28},{28,20},{20,12},{12,4},{4,0},{1,9},{9... | collective-permute-start | bytes 786440 | tf_op jit(solution)/shard_map/ppermute | solution.py:400
  24.5 5.0 %collective-permute-start.7 = (bf16[1,2,256,128]{3,2,1,0:T(8,128)(2,1)S(1)}, bf16[1,2,256,128]{3,2,1,0:T(8,128)(2,1)S(1)}, u32[]{:S(2)}, u32[]{:S(2)}) collective-permute-start(bf16[1,2,256,128]{3,2,1,0:T(8,128)(2,1)S(1)} %slice.9), channel_id=1, source_target_pairs={{8,0},{16,8},{24,16},{28,24},{20,28},{12,20},{4,12},{0,4},{9,1},{1... | collective-permute-start | bytes 393224 | tf_op jit(solution)/shard_map/ppermute | solution.py:401
  25.7 11.7 %copy-start = (bf16[1024,2048]{1,0:T(8,128)(2,1)S(1)}, bf16[1024,2048]{1,0:T(8,128)(2,1)}, u32[]{:S(2)}) copy-start(bf16[1024,2048]{1,0:T(8,128)(2,1)} %refs_4_.1) | copy-start | bytes 12582916
  25.7 11.7 %copy-start.1 = (bf16[128,2048]{1,0:T(8,128)(2,1)S(1)}, bf16[128,2048]{1,0:T(8,128)(2,1)}, u32[]{:S(2)}) copy-start(bf16[128,2048]{1,0:T(8,128)(2,1)} %refs_5_.1) | copy-start | bytes 1572868
  25.7 11.7 %copy-start.2 = (f32[2048]{0:T(1024)S(1)}, f32[2048]{0:T(1024)}, u32[]{:S(2)}) copy-start(f32[2048]{0:T(1024)} %param.17) | copy-start | bytes 24580
  25.7 11.7 %copy-start.3 = (f32[2048]{0:T(1024)S(1)}, f32[2048]{0:T(1024)}, u32[]{:S(2)}) copy-start(f32[2048]{0:T(1024)} %param.18) | copy-start | bytes 24580
  25.8 5.0 %collective-permute-start.3 = (bf16[1,2,256,128]{3,2,1,0:T(8,128)(2,1)S(1)}, bf16[1,2,256,128]{3,2,1,0:T(8,128)(2,1)S(1)}, u32[]{:S(2)}, u32[]{:S(2)}) collective-permute-start(bf16[1,2,256,128]{3,2,1,0:T(8,128)(2,1)S(1)} %slice.8), channel_id=1, source_target_pairs={{0,8},{8,16},{16,24},{24,28},{28,20},{20,12},{12,4},{4,0},{1,9},{9... | collective-permute-start | bytes 393224 | tf_op jit(solution)/shard_map/ppermute | solution.py:400
  29.5 63.2 %copy-start.6 = (bf16[1,1024,2048]{2,1,0:T(8,128)(2,1)S(1)}, bf16[1,1024,2048]{2,1,0:T(8,128)(2,1)}, u32[]{:S(2)}) copy-start(bf16[1,1024,2048]{2,1,0:T(8,128)(2,1)} %param.23) | copy-start | bytes 12582916
  31.7 1.9 %collective-permute-start.8 = (bf16[256,128]{1,0:T(8,128)(2,1)S(1)}, bf16[256,128]{1,0:T(8,128)(2,1)S(1)}, u32[]{:S(2)}, u32[]{:S(2)}) collective-permute-start(bf16[256,128]{1,0:T(8,128)(2,1)S(1)} %get-tuple-element.16), channel_id=1, source_target_pairs={{0,1},{1,0},{2,3},{3,2},{4,5},{5,4},{6,7},{7,6},{8,9},{9,8},{10,11... | collective-permute-start | bytes 196616 | tf_op jit(solution)/shard_map/ppermute | solution.py:219
  31.8 4.5 %collective-permute-start.9 = (bf16[256,128]{1,0:T(8,128)(2,1)S(1)}, bf16[256,128]{1,0:T(8,128)(2,1)S(1)}, u32[]{:S(2)}, u32[]{:S(2)}) collective-permute-start(bf16[256,128]{1,0:T(8,128)(2,1)S(1)} %get-tuple-element.17), channel_id=1, source_target_pairs={{0,2},{1,3},{2,0},{3,1},{4,6},{5,7},{6,4},{7,5},{8,10},{9,11},{10,... | collective-permute-start | bytes 196616 | tf_op jit(solution)/shard_map/ppermute | solution.py:219
  33.4 4.1 %collective-permute-start.10 = (bf16[256,128]{1,0:T(8,128)(2,1)S(1)}, bf16[256,128]{1,0:T(8,128)(2,1)S(1)}, u32[]{:S(2)}, u32[]{:S(2)}) collective-permute-start(bf16[256,128]{1,0:T(8,128)(2,1)S(1)} %get-tuple-element.18), channel_id=1, source_target_pairs={{0,3},{1,2},{2,1},{3,0},{4,7},{5,6},{6,5},{7,4},{8,11},{9,10},{10,... | collective-permute-start | bytes 196616 | tf_op jit(solution)/shard_map/ppermute | solution.py:219
  37.4 55.3 %copy-start.4 = (bf16[1,2048,1024]{2,1,0:T(8,128)(2,1)S(1)}, bf16[1,2048,1024]{2,1,0:T(8,128)(2,1)}, u32[]{:S(2)}) copy-start(bf16[1,2048,1024]{2,1,0:T(8,128)(2,1)} %param.21) | copy-start | bytes 12582916
  37.4 55.3 %copy-start.5 = (bf16[1,2048,1024]{2,1,0:T(8,128)(2,1)S(1)}, bf16[1,2048,1024]{2,1,0:T(8,128)(2,1)}, u32[]{:S(2)}) copy-start(bf16[1,2048,1024]{2,1,0:T(8,128)(2,1)} %param.22) | copy-start | bytes 12582916

commit v9 on v8

--- a/solution.py
+++ b/solution.py
@@ -7,6 +7,7 @@
 from jax.experimental import pallas as pl
 from jax.experimental.pallas import tpu as pltpu
 from jax.sharding import PartitionSpec as P
+
 
 HEAD_SIZE = 64
 GRID_W = 64
@@ -115,7 +116,6 @@
     blocks = columns // width
     kv_heads = lanes // HEAD_SIZE
     ones = jnp.ones((ONES_ROWS, HALF_KEYS), jnp.bfloat16)
-    rows = HEAD_SIZE + ONES_ROWS
     halves = 0
     for chunk, (distance, first_half) in zip(chunks, pieces):
         source = ring_member(place + distance, sp_size)
@@ -155,7 +155,7 @@
                 outs[-1][:, at : at + width] = total
             else:
                 turn = refs[2]
-                tp, head_rows, per = turn.shape
+                tp, _, per = turn.shape
                 tok_count = tp * per
                 ready = (total[:HEAD_SIZE] / total[HEAD_SIZE : HEAD_SIZE + 1]).astype(jnp.bfloat16)
                 for piece in range(width // per):
@@ -346,7 +346,7 @@
         ).astype(jnp.bfloat16)
 
 
-def local(
+def layer(
     sp_size,
     tp_size,
     query_proj,
@@ -363,7 +363,6 @@
     expert_down,
 ):
     tok_count, lanes = projected_keys.shape
-    q_heads = query_proj.shape[1] // HEAD_SIZE
     model_width = residual.shape[1]
     halves = tok_count // HALF_KEYS
     tables = rotation_tables(sp_size * tok_count // GRID_W, lanes)
@@ -470,7 +469,7 @@
 
 def solution(mesh):
     return jax.shard_map(
-        functools.partial(local, mesh.shape["sp"], mesh.shape["tp"]),
+        functools.partial(layer, mesh.shape["sp"], mesh.shape["tp"]),
         mesh=mesh,
         in_specs=(
             P("sp", "tp"),

time: 154 us -> 154 us (level)
  no operation moved by 1% of the time
where the time goes in v9:
time: 154 us; the launch traced here: 153 us
  blocking collectives  106 us (69%)
  Pallas kernels  20.4 us (13%)
  waiting for transfers between devices  12 us (8%)
  starting transfers between devices  11.3 us (7%)
  local copies, waits for them, and re-layouts  2.57 us (2%)
    all_to_all x2, blocking collectives, exchange(): lax.all_to_all(slots, ('sp', 'tp'), split_axis=0, concat_axis=0, tiled=True)  106 us
    pallas_call x6, Pallas kernels, attend(): pl.pallas_call(functools.partial(attend_kernel, sp_size, pieces, last, ra...  9.68 us
    ppermute x4, waiting for transfers between devices, layer(): next_right = lax.ppermute(from_right, 'sp', behind)  7.87 us
    ppermute x4, starting transfers between devices, layer(): next_right = lax.ppermute(from_right, 'sp', behind)  7.23 us
    pallas_call x1, Pallas kernels, layer(): pl.pallas_call(expert_kernel, out_shape=slots_shape, in_specs=[VMEM] * 4,...  6.8 us
    ppermute x3, waiting for transfers between devices, direct_exchange(): lax.ppermute(pieces[rel], 'tp', [(i, i ^ rel) for i in range(tp_size)])  3.79 us
  transfers between devices with their start and end apart: 11, of which 7 were waited for; matrix products, arithmetic and copies ran while one was open for 1% of the time, Pallas kernels for 6%

profile of v9, /device:TPU:0, one launch (start us, length us, event | category | flops | bytes accessed | tf_op | source)
XLA Modules:
  0.0 153.4 jit_solution(6898626282859663971)
XLA Ops:
  0.0 1.0 pad_maximum_fusion.refs_3_
  1.0 3.0 %collective-permute-start.4 = (bf16[2,2,256,128]{3,2,1,0:T(8,128)(2,1)S(1)}, bf16[2,2,256,128]{3,2,1,0:T(8,128)(2,1)S(1)}, u32[]{:S(2)}, u32[]{:S(2)}) collective-permute-start(bf16[2,2,256,128]{3,2,1,0:T(8,128)(2,1)S(1)} %pad_maximum_fusion.refs_3_), channel_id=1, source_target_pairs={{8,0},{16,8},{24,16},{28,24},{20,28},{12,20},{4,12},{0,4},{9,1},{1... | collective-permute-start | bytes 786440 | tf_op jit(solution)/shard_map/ppermute | solution.py:400
  4.2 0.8 copy.17.expert_ref
  6.2 4.2 %collective-permute-done.4.refs_4_ = bf16[2,2,256,128]{3,2,1,0:T(8,128)(2,1)S(1)} collective-permute-done((bf16[2,2,256,128]{3,2,1,0:T(8,128)(2,1)S(1)}, bf16[2,2,256,128]{3,2,1,0:T(8,128)(2,1)S(1)}, u32[]{:S(2)}, u32[]{:S(2)}) %collective-permute-start.4) | collective-permute-done | bytes 262176 | tf_op jit(solution)/shard_map/ppermute | solution.py:400
  10.4 1.7 %collective-permute-start.5 = (bf16[2,2,256,128]{3,2,1,0:T(8,128)(2,1)S(1)}, bf16[2,2,256,128]{3,2,1,0:T(8,128)(2,1)S(1)}, u32[]{:S(2)}, u32[]{:S(2)}) collective-permute-start(bf16[2,2,256,128]{3,2,1,0:T(8,128)(2,1)S(1)} %collective-permute-done.4.refs_4_), channel_id=1, source_target_pairs={{8,0},{16,8},{24,16},{28,24},{20,28},{12,20},{4,12},{0,4},{9,1},{1... | collective-permute-start | bytes 786440 | tf_op jit(solution)/shard_map/ppermute | solution.py:400
  12.8 0.9 copy-done.7
  13.7 1.5 shard_map.118
  15.2 2.7 %collective-permute-done.5.refs_4_ = bf16[2,2,256,128]{3,2,1,0:T(8,128)(2,1)S(1)} collective-permute-done((bf16[2,2,256,128]{3,2,1,0:T(8,128)(2,1)S(1)}, bf16[2,2,256,128]{3,2,1,0:T(8,128)(2,1)S(1)}, u32[]{:S(2)}, u32[]{:S(2)}) %collective-permute-start.5) | collective-permute-done | bytes 262176 | tf_op jit(solution)/shard_map/ppermute | solution.py:400
  17.9 1.4 collective-permute-start.6
  19.9 2.1 %shard_map.119.refs_5_ = f32[80,2048]{1,0:T(8,128)S(1)} custom-call(bf16[128,2048]{1,0:T(8,128)(2,1)S(1)} %get-tuple-element.13.refs_0_, f32[128,128]{1,0:T(8,128)S(1)} %get-tuple-element.22.refs_1_, f32[128,128]{1,0:T(8,128)S(1)} %get-tuple-element.21.refs_2_, ...), custom_call_target="tpu_custom_call", output_to_operand_aliasing={{}: (5, {})} | custom-call | flops 2147483648 | bytes 1048576 | tf_op jit(solution)/shard_map/pallas_call | solution.py:200
  22.0 2.1 %shard_map.120.refs_5_ = f32[80,2048]{1,0:T(8,128)S(1)} custom-call(bf16[128,2048]{1,0:T(8,128)(2,1)S(1)} %get-tuple-element.13.refs_0_, f32[128,128]{1,0:T(8,128)S(1)} %get-tuple-element.22.refs_1_, f32[128,128]{1,0:T(8,128)S(1)} %get-tuple-element.21.refs_2_, ...), custom_call_target="tpu_custom_call", output_to_operand_aliasing={{}: (5, {})} | custom-call | flops 2147483648 | bytes 1048576 | tf_op jit(solution)/shard_map/pallas_call | solution.py:200
  24.5 1.2 collective-permute-start.7
  25.8 0.9 collective-permute-start.3
  26.7 2.1 %shard_map.122.refs_4_ = f32[80,2048]{1,0:T(8,128)S(1)} custom-call(bf16[128,2048]{1,0:T(8,128)(2,1)S(1)} %get-tuple-element.13.refs_0_, f32[128,128]{1,0:T(8,128)S(1)} %get-tuple-element.22.refs_1_, f32[128,128]{1,0:T(8,128)S(1)} %get-tuple-element.21.refs_2_, ...), custom_call_target="tpu_custom_call", output_to_operand_aliasing={{}: (5, {})} | custom-call | flops 2147483648 | bytes 1048576 | tf_op jit(solution)/shard_map/pallas_call | solution.py:200
  29.5 0.9 shard_map.123.refs_4_
  30.8 0.9 shard_map.124
  31.8 1.6 %collective-permute-start.9 = (bf16[256,128]{1,0:T(8,128)(2,1)S(1)}, bf16[256,128]{1,0:T(8,128)(2,1)S(1)}, u32[]{:S(2)}, u32[]{:S(2)}) collective-permute-start(bf16[256,128]{1,0:T(8,128)(2,1)S(1)} %get-tuple-element.17), channel_id=1, source_target_pairs={{0,2},{1,3},{2,0},{3,1},{4,6},{5,7},{6,4},{7,5},{8,10},{9,11},{10,... | collective-permute-start | bytes 196616 | tf_op jit(solution)/shard_map/ppermute | solution.py:219
  33.6 2.6 %collective-permute-done.9.refs_2_ = bf16[256,128]{1,0:T(8,128)(2,1)S(1)} collective-permute-done((bf16[256,128]{1,0:T(8,128)(2,1)S(1)}, bf16[256,128]{1,0:T(8,128)(2,1)S(1)}, u32[]{:S(2)}, u32[]{:S(2)}) %collective-permute-start.9) | collective-permute-done | bytes 65568 | tf_op jit(solution)/shard_map/ppermute | solution.py:219
  36.3 1.1 collective-permute-done.10.refs_3_
  37.5 1.9 %shard_map.125 = (bf16[128,2048]{1,0:T(8,128)(2,1)S(1)}, bf16[512,2048]{1,0:T(8,128)(2,1)S(1)}) custom-call(bf16[256,128]{1,0:T(8,128)(2,1)S(1)} %get-tuple-element.15.refs_0_, bf16[256,128]{1,0:T(8,128)(2,1)S(1)} %collective-permute-done.8.refs_1_, bf16[256,128]{1,0:T(8,128)(2,1)S(1)} %collective-permute-done.9.refs_2_, ...), custom_call_target="tpu_custom_call" | custom-call | flops 805306368 | bytes 8388608 | tf_op jit(solution)/shard_map/pallas_call | solution.py:416
  39.3 53.4 %all_to_all.10 = bf16[32,16,2048]{2,1,0:T(8,128)(2,1)S(1)} all-to-all(bf16[32,16,2048]{2,1,0:T(8,128)(2,1)S(1)} %bitcast.12), channel_id=1, replica_groups=mesh['sp'=8,'tp'=4] {'sp','tp'}, dimensions={0} | all-to-all | bytes 4194304 | tf_op jit(solution)/shard_map/all_to_all | solution.py:435
  92.7 6.8 %shard_map.126 = bf16[512,2048]{1,0:T(8,128)(2,1)S(1)} custom-call(bf16[512,2048]{1,0:T(8,128)(2,1)S(1)} %bitcast.13, bf16[2048,1024]{1,0:T(8,128)(2,1)S(1)} %bitcast.17, bf16[2048,1024]{1,0:T(8,128)(2,1)S(1)} %bitcast.18, bf16[1024,2048]{1,0:T(8,128)(2,1)S(1)} %bitcast.19), custom_call_target="tpu_custom_call" | custom-call | flops 6442450944 | bytes 16777216 | tf_op jit(solution)/shard_map/pallas_call | solution.py:439
  99.5 52.2 %all_to_all.11 = bf16[32,16,2048]{2,1,0:T(8,128)(2,1)S(1)} all-to-all(bf16[32,16,2048]{2,1,0:T(8,128)(2,1)S(1)} %bitcast.14), channel_id=1, replica_groups=mesh['sp'=8,'tp'=4] {'sp','tp'}, dimensions={0} | all-to-all | bytes 4194304 | tf_op jit(solution)/shard_map/all_to_all | solution.py:435
  151.7 1.6 %shard_map.127 = bf16[128,2048]{1,0:T(8,128)(2,1)} custom-call(bf16[128,2048]{1,0:T(8,128)(2,1)S(1)} %get-tuple-element.19.base_ref, bf16[512,2048]{1,0:T(8,128)(2,1)S(1)} %bitcast.11, f32[8,128]{1,0:T(8,128)S(1)} %shard_map.121.refs_6_.refs_8_.table_ref), custom_call_target="tpu_custom_call" | custom-call | flops 536870912 | bytes 3145728 | tf_op jit(solution)/shard_map/pallas_call | solution.py:452
  (34 shorter events, 4.5 us)
Async XLA Ops:
  1.0 9.4 %collective-permute-start.4 = (bf16[2,2,256,128]{3,2,1,0:T(8,128)(2,1)S(1)}, bf16[2,2,256,128]{3,2,1,0:T(8,128)(2,1)S(1)}, u32[]{:S(2)}, u32[]{:S(2)}) collective-permute-start(bf16[2,2,256,128]{3,2,1,0:T(8,128)(2,1)S(1)} %pad_maximum_fusion.refs_3_), channel_id=1, source_target_pairs={{8,0},{16,8},{24,16},{28,24},{20,28},{12,20},{4,12},{0,4},{9,1},{1... | collective-permute-start | bytes 786440 | tf_op jit(solution)/shard_map/ppermute | solution.py:400
  4.0 8.0 %collective-permute-start = (bf16[2,2,256,128]{3,2,1,0:T(8,128)(2,1)S(1)}, bf16[2,2,256,128]{3,2,1,0:T(8,128)(2,1)S(1)}, u32[]{:S(2)}, u32[]{:S(2)}) collective-permute-start(bf16[2,2,256,128]{3,2,1,0:T(8,128)(2,1)S(1)} %pad_maximum_fusion.refs_3_), channel_id=1, source_target_pairs={{0,8},{8,16},{16,24},{24,28},{28,20},{20,12},{12,4},{4,0},{1,9},{9... | collective-permute-start | bytes 786440 | tf_op jit(solution)/shard_map/ppermute | solution.py:399
  10.4 7.5 %collective-permute-start.5 = (bf16[2,2,256,128]{3,2,1,0:T(8,128)(2,1)S(1)}, bf16[2,2,256,128]{3,2,1,0:T(8,128)(2,1)S(1)}, u32[]{:S(2)}, u32[]{:S(2)}) collective-permute-start(bf16[2,2,256,128]{3,2,1,0:T(8,128)(2,1)S(1)} %collective-permute-done.4.refs_4_), channel_id=1, source_target_pairs={{8,0},{16,8},{24,16},{28,24},{20,28},{12,20},{4,12},{0,4},{9,1},{1... | collective-permute-start | bytes 786440 | tf_op jit(solution)/shard_map/ppermute | solution.py:400
  12.1 7.2 %collective-permute-start.1 = (bf16[2,2,256,128]{3,2,1,0:T(8,128)(2,1)S(1)}, bf16[2,2,256,128]{3,2,1,0:T(8,128)(2,1)S(1)}, u32[]{:S(2)}, u32[]{:S(2)}) collective-permute-start(bf16[2,2,256,128]{3,2,1,0:T(8,128)(2,1)S(1)} %collective-permute-done.refs_3_), channel_id=1, source_target_pairs={{0,8},{8,16},{16,24},{24,28},{28,20},{20,12},{12,4},{4,0},{1,9},{9... | collective-permute-start | bytes 786440 | tf_op jit(solution)/shard_map/ppermute | solution.py:399
  12.8 1.0 copy-start.7
  17.9 6.6 %collective-permute-start.6 = (bf16[2,2,256,128]{3,2,1,0:T(8,128)(2,1)S(1)}, bf16[2,2,256,128]{3,2,1,0:T(8,128)(2,1)S(1)}, u32[]{:S(2)}, u32[]{:S(2)}) collective-permute-start(bf16[2,2,256,128]{3,2,1,0:T(8,128)(2,1)S(1)} %collective-permute-done.5.refs_4_), channel_id=1, source_target_pairs={{8,0},{16,8},{24,16},{28,24},{20,28},{12,20},{4,12},{0,4},{9,1},{1... | collective-permute-start | bytes 786440 | tf_op jit(solution)/shard_map/ppermute | solution.py:400
  19.3 6.4 %collective-permute-start.2 = (bf16[2,2,256,128]{3,2,1,0:T(8,128)(2,1)S(1)}, bf16[2,2,256,128]{3,2,1,0:T(8,128)(2,1)S(1)}, u32[]{:S(2)}, u32[]{:S(2)}) collective-permute-start(bf16[2,2,256,128]{3,2,1,0:T(8,128)(2,1)S(1)} %collective-permute-done.1.refs_3_), channel_id=1, source_target_pairs={{0,8},{8,16},{16,24},{24,28},{28,20},{20,12},{12,4},{4,0},{1,9},{9... | collective-permute-start | bytes 786440 | tf_op jit(solution)/shard_map/ppermute | solution.py:399
  24.5 5.0 %collective-permute-start.7 = (bf16[1,2,256,128]{3,2,1,0:T(8,128)(2,1)S(1)}, bf16[1,2,256,128]{3,2,1,0:T(8,128)(2,1)S(1)}, u32[]{:S(2)}, u32[]{:S(2)}) collective-permute-start(bf16[1,2,256,128]{3,2,1,0:T(8,128)(2,1)S(1)} %slice.9), channel_id=1, source_target_pairs={{8,0},{16,8},{24,16},{28,24},{20,28},{12,20},{4,12},{0,4},{9,1},{1... | collective-permute-start | bytes 393224 | tf_op jit(solution)/shard_map/ppermute | solution.py:400
  25.7 11.7 %copy-start = (bf16[1024,2048]{1,0:T(8,128)(2,1)S(1)}, bf16[1024,2048]{1,0:T(8,128)(2,1)}, u32[]{:S(2)}) copy-start(bf16[1024,2048]{1,0:T(8,128)(2,1)} %refs_4_.1) | copy-start | bytes 12582916
  25.7 11.7 %copy-start.1 = (bf16[128,2048]{1,0:T(8,128)(2,1)S(1)}, bf16[128,2048]{1,0:T(8,128)(2,1)}, u32[]{:S(2)}) copy-start(bf16[128,2048]{1,0:T(8,128)(2,1)} %refs_5_.1) | copy-start | bytes 1572868
  25.7 11.7 %copy-start.2 = (f32[2048]{0:T(1024)S(1)}, f32[2048]{0:T(1024)}, u32[]{:S(2)}) copy-start(f32[2048]{0:T(1024)} %param.17) | copy-start | bytes 24580
  25.7 11.7 %copy-start.3 = (f32[2048]{0:T(1024)S(1)}, f32[2048]{0:T(1024)}, u32[]{:S(2)}) copy-start(f32[2048]{0:T(1024)} %param.18) | copy-start | bytes 24580
  25.8 5.0 %collective-permute-start.3 = (bf16[1,2,256,128]{3,2,1,0:T(8,128)(2,1)S(1)}, bf16[1,2,256,128]{3,2,1,0:T(8,128)(2,1)S(1)}, u32[]{:S(2)}, u32[]{:S(2)}) collective-permute-start(bf16[1,2,256,128]{3,2,1,0:T(8,128)(2,1)S(1)} %slice.8), channel_id=1, source_target_pairs={{0,8},{8,16},{16,24},{24,28},{28,20},{20,12},{12,4},{4,0},{1,9},{9... | collective-permute-start | bytes 393224 | tf_op jit(solution)/shard_map/ppermute | solution.py:399
  29.5 63.2 %copy-start.6 = (bf16[1,1024,2048]{2,1,0:T(8,128)(2,1)S(1)}, bf16[1,1024,2048]{2,1,0:T(8,128)(2,1)}, u32[]{:S(2)}) copy-start(bf16[1,1024,2048]{2,1,0:T(8,128)(2,1)} %param.23) | copy-start | bytes 12582916
  31.7 1.9 %collective-permute-start.8 = (bf16[256,128]{1,0:T(8,128)(2,1)S(1)}, bf16[256,128]{1,0:T(8,128)(2,1)S(1)}, u32[]{:S(2)}, u32[]{:S(2)}) collective-permute-start(bf16[256,128]{1,0:T(8,128)(2,1)S(1)} %get-tuple-element.16), channel_id=1, source_target_pairs={{0,1},{1,0},{2,3},{3,2},{4,5},{5,4},{6,7},{7,6},{8,9},{9,8},{10,11... | collective-permute-start | bytes 196616 | tf_op jit(solution)/shard_map/ppermute | solution.py:219
  31.8 4.5 %collective-permute-start.9 = (bf16[256,128]{1,0:T(8,128)(2,1)S(1)}, bf16[256,128]{1,0:T(8,128)(2,1)S(1)}, u32[]{:S(2)}, u32[]{:S(2)}) collective-permute-start(bf16[256,128]{1,0:T(8,128)(2,1)S(1)} %get-tuple-element.17), channel_id=1, source_target_pairs={{0,2},{1,3},{2,0},{3,1},{4,6},{5,7},{6,4},{7,5},{8,10},{9,11},{10,... | collective-permute-start | bytes 196616 | tf_op jit(solution)/shard_map/ppermute | solution.py:219
  33.4 4.1 %collective-permute-start.10 = (bf16[256,128]{1,0:T(8,128)(2,1)S(1)}, bf16[256,128]{1,0:T(8,128)(2,1)S(1)}, u32[]{:S(2)}, u32[]{:S(2)}) collective-permute-start(bf16[256,128]{1,0:T(8,128)(2,1)S(1)} %get-tuple-element.18), channel_id=1, source_target_pairs={{0,3},{1,2},{2,1},{3,0},{4,7},{5,6},{6,5},{7,4},{8,11},{9,10},{10,... | collective-permute-start | bytes 196616 | tf_op jit(solution)/shard_map/ppermute | solution.py:219
  37.4 55.3 %copy-start.4 = (bf16[1,2048,1024]{2,1,0:T(8,128)(2,1)S(1)}, bf16[1,2048,1024]{2,1,0:T(8,128)(2,1)}, u32[]{:S(2)}) copy-start(bf16[1,2048,1024]{2,1,0:T(8,128)(2,1)} %param.21) | copy-start | bytes 12582916
  37.4 55.3 %copy-start.5 = (bf16[1,2048,1024]{2,1,0:T(8,128)(2,1)S(1)}, bf16[1,2048,1024]{2,1,0:T(8,128)(2,1)}, u32[]{:S(2)}) copy-start(bf16[1,2048,1024]{2,1,0:T(8,128)(2,1)} %param.22) | copy-start | bytes 12582916

commit v10 on v9

--- a/solution.py
+++ b/solution.py
@@ -391,13 +391,21 @@
     steps = sp_size // 2
     acc = None
     queries = query_proj
-    from_left = from_right = raw_own
+    from_left = from_right = [(raw_own, 0)]
     held, pieces = [raw_own], [(0, 0)]
     for step in range(steps):
+        if step == 1:
+            cuts = [(slice(0, halves // 2), 0), (slice(halves // 2, halves), halves // 2)]
+            from_left = [(from_left[0][0][cut], first) for cut, first in cuts]
+            from_right = [(from_right[0][0][cut], first) for cut, first in cuts]
         if step == steps - 1:
-            from_left, from_right = from_left[: halves // 2], from_right[halves // 2 :]
-        next_left = lax.ppermute(from_left, "sp", ahead)
-        next_right = lax.ppermute(from_right, "sp", behind)
+            from_left, from_right = from_left[:1], from_right[-1:]
+        next_left, next_right = [], []
+        for part in range(len(from_left)):
+            left, first = from_left[part]
+            next_left.append((lax.ppermute(left, "sp", ahead), first))
+            right, first = from_right[part]
+            next_right.append((lax.ppermute(right, "sp", behind), first))
         after = (table,) if step == steps - 1 else ()
         out = attend(queries, tables, held, pieces, acc, sp_size, tp_size, after=after)
         if step == 0:
@@ -405,8 +413,9 @@
         else:
             (acc,) = out
         from_left, from_right = next_left, next_right
-        held = [from_left, from_right]
-        pieces = [(-step - 1, 0), (step + 1, halves // 2 if step == steps - 1 else 0)]
+        held = [part for part, _ in from_left + from_right]
+        pieces = [(-step - 1, first) for _, first in from_left]
+        pieces += [(step + 1, first) for _, first in from_right]
     (acc,) = attend(queries, tables, held[1:], pieces[1:], acc, sp_size, tp_size)
     pieces = attend(queries, tables, held[:1], pieces[:1], acc, sp_size, tp_size, last=True)
     blocks = direct_exchange(pieces, tp_size)

time: 154 us -> 155 us (level)
  starting transfers between devices: 11.3 us -> 15.5 us
  waiting for transfers between devices: 12 us -> 10.1 us
    ppermute x8 -> x12, starting transfers between devices: 9.35 us -> 13.6 us  [the longest x6 10.7 us: layer(): next_right.append((lax.ppermute(right, 'sp', behind), first))]
    ppermute x8 -> x12, waiting for transfers between devices: 8.21 us -> 6.28 us  [the longest x6 3.53 us: layer(): next_left.append((lax.ppermute(left, 'sp', ahead), first))]
  transfers between devices with their start and end apart: 11 -> 15, of which waited for: 7 -> 6; matrix products, arithmetic and copies ran while one was open for 1% -> 0% of each run, Pallas kernels for 6% -> 6%
where the time goes in v10:
time: 155 us
  blocking collectives  105 us (68%)
  Pallas kernels  20.4 us (13%)
  starting transfers between devices  15.5 us (10%)
  waiting for transfers between devices  10.1 us (7%)
    all_to_all x2, blocking collectives, exchange(): lax.all_to_all(slots, ('sp', 'tp'), split_axis=0, concat_axis=0, tiled=True)  105 us
    ppermute x6, starting transfers between devices, layer(): next_right.append((lax.ppermute(right, 'sp', behind), first))  10.7 us
    pallas_call x6, Pallas kernels, attend(): pl.pallas_call(functools.partial(attend_kernel, sp_size, pieces, last, ra...  9.69 us
    pallas_call x1, Pallas kernels, layer(): pl.pallas_call(expert_kernel, out_shape=slots_shape, in_specs=[VMEM] * 4,...  6.79 us
    ppermute x3, waiting for transfers between devices, direct_exchange(): lax.ppermute(pieces[rel], 'tp', [(i, i ^ rel) for i in range(tp_size)])  3.82 us
    ppermute x6, waiting for transfers between devices, layer(): next_left.append((lax.ppermute(left, 'sp', ahead), first))  3.53 us
  transfers between devices with their start and end apart: 15, of which 6 were waited for; matrix products, arithmetic and copies ran while one was open for 0% of the time, Pallas kernels for 6%

profile of v10, /device:TPU:0, one launch (start us, length us, event | category | flops | bytes accessed | tf_op | source)
XLA Modules:
  0.0 154.5 jit_solution(5103816607439031353)
XLA Ops:
  0.0 1.0 pad_maximum_fusion.refs_3_
  1.0 3.0 %collective-permute-start.4 = (bf16[2,2,256,128]{3,2,1,0:T(8,128)(2,1)S(1)}, bf16[2,2,256,128]{3,2,1,0:T(8,128)(2,1)S(1)}, u32[]{:S(2)}, u32[]{:S(2)}) collective-permute-start(bf16[2,2,256,128]{3,2,1,0:T(8,128)(2,1)S(1)} %pad_maximum_fusion.refs_3_), channel_id=1, source_target_pairs={{8,0},{16,8},{24,16},{28,24},{20,28},{12,20},{4,12},{0,4},{9,1},{1... | collective-permute-start | bytes 786440 | tf_op jit(solution)/shard_map/ppermute | solution.py:408
  4.5 0.9 copy-done.7
  5.5 1.5 shard_map.118
  7.7 2.7 %collective-permute-done.4.refs_4_ = bf16[2,2,256,128]{3,2,1,0:T(8,128)(2,1)S(1)} collective-permute-done((bf16[2,2,256,128]{3,2,1,0:T(8,128)(2,1)S(1)}, bf16[2,2,256,128]{3,2,1,0:T(8,128)(2,1)S(1)}, u32[]{:S(2)}, u32[]{:S(2)}) %collective-permute-start.4) | collective-permute-done | bytes 262176 | tf_op jit(solution)/shard_map/ppermute | solution.py:408
  10.5 1.7 %collective-permute-start.10 = (bf16[1,2,256,128]{3,2,1,0:T(8,128)(2,1)S(1)}, bf16[1,2,256,128]{3,2,1,0:T(8,128)(2,1)S(1)}, u32[]{:S(2)}, u32[]{:S(2)}) collective-permute-start(bf16[1,2,256,128]{3,2,1,0:T(8,128)(2,1)S(1)} %get-tuple-element.21), channel_id=1, source_target_pairs={{8,0},{16,8},{24,16},{28,24},{20,28},{12,20},{4,12},{0,4},{9,1},{1... | collective-permute-start | bytes 393224 | tf_op jit(solution)/shard_map/ppermute | solution.py:408
  12.2 1.6 %collective-permute-start.5 = (bf16[1,2,256,128]{3,2,1,0:T(8,128)(2,1)S(1)}, bf16[1,2,256,128]{3,2,1,0:T(8,128)(2,1)S(1)}, u32[]{:S(2)}, u32[]{:S(2)}) collective-permute-start(bf16[1,2,256,128]{3,2,1,0:T(8,128)(2,1)S(1)} %get-tuple-element.22), channel_id=1, source_target_pairs={{8,0},{16,8},{24,16},{28,24},{20,28},{12,20},{4,12},{0,4},{9,1},{1... | collective-permute-start | bytes 393224 | tf_op jit(solution)/shard_map/ppermute | solution.py:408
  14.6 2.1 %shard_map.119.refs_7_ = f32[80,2048]{1,0:T(8,128)S(1)} custom-call(bf16[128,2048]{1,0:T(8,128)(2,1)S(1)} %get-tuple-element.13.refs_0_, f32[128,128]{1,0:T(8,128)S(1)} %get-tuple-element.26.refs_1_, f32[128,128]{1,0:T(8,128)S(1)} %get-tuple-element.25.refs_2_, ...), custom_call_target="tpu_custom_call", output_to_operand_aliasing={{}: (5, {})} | custom-call | flops 2147483648 | bytes 1048576 | tf_op jit(solution)/shard_map/pallas_call | solution.py:200
  16.8 1.7 %collective-permute-start.11 = (bf16[1,2,256,128]{3,2,1,0:T(8,128)(2,1)S(1)}, bf16[1,2,256,128]{3,2,1,0:T(8,128)(2,1)S(1)}, u32[]{:S(2)}, u32[]{:S(2)}) collective-permute-start(bf16[1,2,256,128]{3,2,1,0:T(8,128)(2,1)S(1)} %collective-permute-done.10.refs_5_), channel_id=1, source_target_pairs={{8,0},{16,8},{24,16},{28,24},{20,28},{12,20},{4,12},{0,4},{9,1},{1... | collective-permute-start | bytes 393224 | tf_op jit(solution)/shard_map/ppermute | solution.py:408
  18.5 1.6 %collective-permute-start.6 = (bf16[1,2,256,128]{3,2,1,0:T(8,128)(2,1)S(1)}, bf16[1,2,256,128]{3,2,1,0:T(8,128)(2,1)S(1)}, u32[]{:S(2)}, u32[]{:S(2)}) collective-permute-start(bf16[1,2,256,128]{3,2,1,0:T(8,128)(2,1)S(1)} %collective-permute-done.5.refs_6_), channel_id=1, source_target_pairs={{8,0},{16,8},{24,16},{28,24},{20,28},{12,20},{4,12},{0,4},{9,1},{1... | collective-permute-start | bytes 393224 | tf_op jit(solution)/shard_map/ppermute | solution.py:408
  20.9 1.0 collective-permute-start.2
  21.9 2.1 %shard_map.120.refs_7_ = f32[80,2048]{1,0:T(8,128)S(1)} custom-call(bf16[128,2048]{1,0:T(8,128)(2,1)S(1)} %get-tuple-element.13.refs_0_, f32[128,128]{1,0:T(8,128)S(1)} %get-tuple-element.26.refs_1_, f32[128,128]{1,0:T(8,128)S(1)} %get-tuple-element.25.refs_2_, ...), custom_call_target="tpu_custom_call", output_to_operand_aliasing={{}: (7, {})} | custom-call | flops 2147483648 | bytes 1048576 | tf_op jit(solution)/shard_map/pallas_call | solution.py:200
  24.1 1.1 collective-permute-start.7
  25.2 1.7 %collective-permute-done.2.refs_3_ = bf16[1,2,256,128]{3,2,1,0:T(8,128)(2,1)S(1)} collective-permute-done((bf16[1,2,256,128]{3,2,1,0:T(8,128)(2,1)S(1)}, bf16[1,2,256,128]{3,2,1,0:T(8,128)(2,1)S(1)}, u32[]{:S(2)}, u32[]{:S(2)}) %collective-permute-start.2) | collective-permute-done | bytes 131104 | tf_op jit(solution)/shard_map/ppermute | solution.py:406
  27.4 2.1 %shard_map.122.refs_4_ = f32[80,2048]{1,0:T(8,128)S(1)} custom-call(bf16[128,2048]{1,0:T(8,128)(2,1)S(1)} %get-tuple-element.13.refs_0_, f32[128,128]{1,0:T(8,128)S(1)} %get-tuple-element.26.refs_1_, f32[128,128]{1,0:T(8,128)S(1)} %get-tuple-element.25.refs_2_, ...), custom_call_target="tpu_custom_call", output_to_operand_aliasing={{}: (7, {})} | custom-call | flops 2147483648 | bytes 1048576 | tf_op jit(solution)/shard_map/pallas_call | solution.py:200
  30.4 1.4 collective-permute-done.3.refs_3_
  32.9 1.6 %collective-permute-start.13 = (bf16[256,128]{1,0:T(8,128)(2,1)S(1)}, bf16[256,128]{1,0:T(8,128)(2,1)S(1)}, u32[]{:S(2)}, u32[]{:S(2)}) collective-permute-start(bf16[256,128]{1,0:T(8,128)(2,1)S(1)} %get-tuple-element.17), channel_id=1, source_target_pairs={{0,2},{1,3},{2,0},{3,1},{4,6},{5,7},{6,4},{7,5},{8,10},{9,11},{10,... | collective-permute-start | bytes 196616 | tf_op jit(solution)/shard_map/ppermute | solution.py:219
  34.7 2.6 %collective-permute-done.13.refs_2_ = bf16[256,128]{1,0:T(8,128)(2,1)S(1)} collective-permute-done((bf16[256,128]{1,0:T(8,128)(2,1)S(1)}, bf16[256,128]{1,0:T(8,128)(2,1)S(1)}, u32[]{:S(2)}, u32[]{:S(2)}) %collective-permute-start.13) | collective-permute-done | bytes 65568 | tf_op jit(solution)/shard_map/ppermute | solution.py:219
  37.3 1.2 collective-permute-done.14.refs_3_
  38.6 1.9 %shard_map.125 = (bf16[128,2048]{1,0:T(8,128)(2,1)S(1)}, bf16[512,2048]{1,0:T(8,128)(2,1)S(1)}) custom-call(bf16[256,128]{1,0:T(8,128)(2,1)S(1)} %get-tuple-element.15.refs_0_, bf16[256,128]{1,0:T(8,128)(2,1)S(1)} %collective-permute-done.12.refs_1_, bf16[256,128]{1,0:T(8,128)(2,1)S(1)} %collective-permute-done.13.refs_2_, ...), custom_call_target="tpu_custom_call" | custom-call | flops 805306368 | bytes 8388608 | tf_op jit(solution)/shard_map/pallas_call | solution.py:425
  40.4 53.3 %all_to_all.10 = bf16[32,16,2048]{2,1,0:T(8,128)(2,1)S(1)} all-to-all(bf16[32,16,2048]{2,1,0:T(8,128)(2,1)S(1)} %bitcast.12), channel_id=1, replica_groups=mesh['sp'=8,'tp'=4] {'sp','tp'}, dimensions={0} | all-to-all | bytes 4194304 | tf_op jit(solution)/shard_map/all_to_all | solution.py:444
  93.8 6.8 %shard_map.126 = bf16[512,2048]{1,0:T(8,128)(2,1)S(1)} custom-call(bf16[512,2048]{1,0:T(8,128)(2,1)S(1)} %bitcast.13, bf16[2048,1024]{1,0:T(8,128)(2,1)S(1)} %bitcast.17, bf16[2048,1024]{1,0:T(8,128)(2,1)S(1)} %bitcast.18, bf16[1024,2048]{1,0:T(8,128)(2,1)S(1)} %bitcast.19), custom_call_target="tpu_custom_call" | custom-call | flops 6442450944 | bytes 16777216 | tf_op jit(solution)/shard_map/pallas_call | solution.py:448
  100.6 52.2 %all_to_all.11 = bf16[32,16,2048]{2,1,0:T(8,128)(2,1)S(1)} all-to-all(bf16[32,16,2048]{2,1,0:T(8,128)(2,1)S(1)} %bitcast.14), channel_id=1, replica_groups=mesh['sp'=8,'tp'=4] {'sp','tp'}, dimensions={0} | all-to-all | bytes 4194304 | tf_op jit(solution)/shard_map/all_to_all | solution.py:444
  152.7 1.6 %shard_map.127 = bf16[128,2048]{1,0:T(8,128)(2,1)} custom-call(bf16[128,2048]{1,0:T(8,128)(2,1)S(1)} %get-tuple-element.19.base_ref, bf16[512,2048]{1,0:T(8,128)(2,1)S(1)} %bitcast.11, f32[8,128]{1,0:T(8,128)S(1)} %shard_map.121.refs_8_.table_ref), custom_call_target="tpu_custom_call" | custom-call | flops 536870912 | bytes 3145728 | tf_op jit(solution)/shard_map/pallas_call | solution.py:461
  (46 shorter events, 5.6 us)
Async XLA Ops:
  0.0 7.0 %copy-start.8 = (s32[128,2]{0,1:T(2,128)S(1)}, s32[128,2]{0,1:T(2,128)}, u32[]{:S(2)}) copy-start(s32[128,2]{0,1:T(2,128)} %param.19) | copy-start | bytes 3076
  0.0 7.1 %copy-start.9 = (f32[128,2]{0,1:T(2,128)S(1)}, f32[128,2]{0,1:T(2,128)}, u32[]{:S(2)}) copy-start(f32[128,2]{0,1:T(2,128)} %param.20) | copy-start | bytes 3076
  1.0 9.4 %collective-permute-start.4 = (bf16[2,2,256,128]{3,2,1,0:T(8,128)(2,1)S(1)}, bf16[2,2,256,128]{3,2,1,0:T(8,128)(2,1)S(1)}, u32[]{:S(2)}, u32[]{:S(2)}) collective-permute-start(bf16[2,2,256,128]{3,2,1,0:T(8,128)(2,1)S(1)} %pad_maximum_fusion.refs_3_), channel_id=1, source_target_pairs={{8,0},{16,8},{24,16},{28,24},{20,28},{12,20},{4,12},{0,4},{9,1},{1... | collective-permute-start | bytes 786440 | tf_op jit(solution)/shard_map/ppermute | solution.py:408
  4.0 9.7 %collective-permute-start = (bf16[2,2,256,128]{3,2,1,0:T(8,128)(2,1)S(1)}, bf16[2,2,256,128]{3,2,1,0:T(8,128)(2,1)S(1)}, u32[]{:S(2)}, u32[]{:S(2)}) collective-permute-start(bf16[2,2,256,128]{3,2,1,0:T(8,128)(2,1)S(1)} %pad_maximum_fusion.refs_3_), channel_id=1, source_target_pairs={{0,8},{8,16},{16,24},{24,28},{28,20},{20,12},{12,4},{4,0},{1,9},{9... | collective-permute-start | bytes 786440 | tf_op jit(solution)/shard_map/ppermute | solution.py:406
  10.5 6.3 %collective-permute-start.10 = (bf16[1,2,256,128]{3,2,1,0:T(8,128)(2,1)S(1)}, bf16[1,2,256,128]{3,2,1,0:T(8,128)(2,1)S(1)}, u32[]{:S(2)}, u32[]{:S(2)}) collective-permute-start(bf16[1,2,256,128]{3,2,1,0:T(8,128)(2,1)S(1)} %get-tuple-element.21), channel_id=1, source_target_pairs={{8,0},{16,8},{24,16},{28,24},{20,28},{12,20},{4,12},{0,4},{9,1},{1... | collective-permute-start | bytes 393224 | tf_op jit(solution)/shard_map/ppermute | solution.py:408
  12.2 6.3 %collective-permute-start.5 = (bf16[1,2,256,128]{3,2,1,0:T(8,128)(2,1)S(1)}, bf16[1,2,256,128]{3,2,1,0:T(8,128)(2,1)S(1)}, u32[]{:S(2)}, u32[]{:S(2)}) collective-permute-start(bf16[1,2,256,128]{3,2,1,0:T(8,128)(2,1)S(1)} %get-tuple-element.22), channel_id=1, source_target_pairs={{8,0},{16,8},{24,16},{28,24},{20,28},{12,20},{4,12},{0,4},{9,1},{1... | collective-permute-start | bytes 393224 | tf_op jit(solution)/shard_map/ppermute | solution.py:408
  13.8 6.3 %collective-permute-start.8 = (bf16[1,2,256,128]{3,2,1,0:T(8,128)(2,1)S(1)}, bf16[1,2,256,128]{3,2,1,0:T(8,128)(2,1)S(1)}, u32[]{:S(2)}, u32[]{:S(2)}) collective-permute-start(bf16[1,2,256,128]{3,2,1,0:T(8,128)(2,1)S(1)} %get-tuple-element.23), channel_id=1, source_target_pairs={{0,8},{8,16},{16,24},{24,28},{28,20},{20,12},{12,4},{4,0},{1,9},{9... | collective-permute-start | bytes 393224 | tf_op jit(solution)/shard_map/ppermute | solution.py:406
  14.3 6.7 %collective-permute-start.1 = (bf16[1,2,256,128]{3,2,1,0:T(8,128)(2,1)S(1)}, bf16[1,2,256,128]{3,2,1,0:T(8,128)(2,1)S(1)}, u32[]{:S(2)}, u32[]{:S(2)}) collective-permute-start(bf16[1,2,256,128]{3,2,1,0:T(8,128)(2,1)S(1)} %get-tuple-element.24), channel_id=1, source_target_pairs={{0,8},{8,16},{16,24},{24,28},{28,20},{20,12},{12,4},{4,0},{1,9},{9... | collective-permute-start | bytes 393224 | tf_op jit(solution)/shard_map/ppermute | solution.py:406
  16.8 10.6 %collective-permute-start.11 = (bf16[1,2,256,128]{3,2,1,0:T(8,128)(2,1)S(1)}, bf16[1,2,256,128]{3,2,1,0:T(8,128)(2,1)S(1)}, u32[]{:S(2)}, u32[]{:S(2)}) collective-permute-start(bf16[1,2,256,128]{3,2,1,0:T(8,128)(2,1)S(1)} %collective-permute-done.10.refs_5_), channel_id=1, source_target_pairs={{8,0},{16,8},{24,16},{28,24},{20,28},{12,20},{4,12},{0,4},{9,1},{1... | collective-permute-start | bytes 393224 | tf_op jit(solution)/shard_map/ppermute | solution.py:408
  18.5 5.6 %collective-permute-start.6 = (bf16[1,2,256,128]{3,2,1,0:T(8,128)(2,1)S(1)}, bf16[1,2,256,128]{3,2,1,0:T(8,128)(2,1)S(1)}, u32[]{:S(2)}, u32[]{:S(2)}) collective-permute-start(bf16[1,2,256,128]{3,2,1,0:T(8,128)(2,1)S(1)} %collective-permute-done.5.refs_6_), channel_id=1, source_target_pairs={{8,0},{16,8},{24,16},{28,24},{20,28},{12,20},{4,12},{0,4},{9,1},{1... | collective-permute-start | bytes 393224 | tf_op jit(solution)/shard_map/ppermute | solution.py:408
  20.1 7.3 %collective-permute-start.9 = (bf16[1,2,256,128]{3,2,1,0:T(8,128)(2,1)S(1)}, bf16[1,2,256,128]{3,2,1,0:T(8,128)(2,1)S(1)}, u32[]{:S(2)}, u32[]{:S(2)}) collective-permute-start(bf16[1,2,256,128]{3,2,1,0:T(8,128)(2,1)S(1)} %collective-permute-done.8.refs_4_), channel_id=1, source_target_pairs={{0,8},{8,16},{16,24},{24,28},{28,20},{20,12},{12,4},{4,0},{1,9},{9... | collective-permute-start | bytes 393224 | tf_op jit(solution)/shard_map/ppermute | solution.py:406
  20.9 6.0 %collective-permute-start.2 = (bf16[1,2,256,128]{3,2,1,0:T(8,128)(2,1)S(1)}, bf16[1,2,256,128]{3,2,1,0:T(8,128)(2,1)S(1)}, u32[]{:S(2)}, u32[]{:S(2)}) collective-permute-start(bf16[1,2,256,128]{3,2,1,0:T(8,128)(2,1)S(1)} %collective-permute-done.1.refs_3_), channel_id=1, source_target_pairs={{0,8},{8,16},{16,24},{24,28},{28,20},{20,12},{12,4},{4,0},{1,9},{9... | collective-permute-start | bytes 393224 | tf_op jit(solution)/shard_map/ppermute | solution.py:406
  24.0 14.5 %copy-start = (bf16[1024,2048]{1,0:T(8,128)(2,1)S(1)}, bf16[1024,2048]{1,0:T(8,128)(2,1)}, u32[]{:S(2)}) copy-start(bf16[1024,2048]{1,0:T(8,128)(2,1)} %refs_4_.1) | copy-start | bytes 12582916
  24.0 14.5 %copy-start.1 = (bf16[128,2048]{1,0:T(8,128)(2,1)S(1)}, bf16[128,2048]{1,0:T(8,128)(2,1)}, u32[]{:S(2)}) copy-start(bf16[128,2048]{1,0:T(8,128)(2,1)} %refs_5_.1) | copy-start | bytes 1572868
  24.0 14.5 %copy-start.2 = (f32[2048]{0:T(1024)S(1)}, f32[2048]{0:T(1024)}, u32[]{:S(2)}) copy-start(f32[2048]{0:T(1024)} %param.17) | copy-start | bytes 24580
  24.1 14.5 %copy-start.3 = (f32[2048]{0:T(1024)S(1)}, f32[2048]{0:T(1024)}, u32[]{:S(2)}) copy-start(f32[2048]{0:T(1024)} %param.18) | copy-start | bytes 24580
  24.1 5.4 %collective-permute-start.7 = (bf16[1,2,256,128]{3,2,1,0:T(8,128)(2,1)S(1)}, bf16[1,2,256,128]{3,2,1,0:T(8,128)(2,1)S(1)}, u32[]{:S(2)}, u32[]{:S(2)}) collective-permute-start(bf16[1,2,256,128]{3,2,1,0:T(8,128)(2,1)S(1)} %collective-permute-done.6.refs_6_), channel_id=1, source_target_pairs={{8,0},{16,8},{24,16},{28,24},{20,28},{12,20},{4,12},{0,4},{9,1},{1... | collective-permute-start | bytes 393224 | tf_op jit(solution)/shard_map/ppermute | solution.py:408
  26.9 5.0 %collective-permute-start.3 = (bf16[1,2,256,128]{3,2,1,0:T(8,128)(2,1)S(1)}, bf16[1,2,256,128]{3,2,1,0:T(8,128)(2,1)S(1)}, u32[]{:S(2)}, u32[]{:S(2)}) collective-permute-start(bf16[1,2,256,128]{3,2,1,0:T(8,128)(2,1)S(1)} %collective-permute-done.2.refs_3_), channel_id=1, source_target_pairs={{0,8},{8,16},{16,24},{24,28},{28,20},{20,12},{12,4},{4,0},{1,9},{9... | collective-permute-start | bytes 393224 | tf_op jit(solution)/shard_map/ppermute | solution.py:406
  29.5 64.3 %copy-start.6 = (bf16[1,1024,2048]{2,1,0:T(8,128)(2,1)S(1)}, bf16[1,1024,2048]{2,1,0:T(8,128)(2,1)}, u32[]{:S(2)}) copy-start(bf16[1,1024,2048]{2,1,0:T(8,128)(2,1)} %param.23) | copy-start | bytes 12582916
  32.8 1.9 %collective-permute-start.12 = (bf16[256,128]{1,0:T(8,128)(2,1)S(1)}, bf16[256,128]{1,0:T(8,128)(2,1)S(1)}, u32[]{:S(2)}, u32[]{:S(2)}) collective-permute-start(bf16[256,128]{1,0:T(8,128)(2,1)S(1)} %get-tuple-element.16), channel_id=1, source_target_pairs={{0,1},{1,0},{2,3},{3,2},{4,5},{5,4},{6,7},{7,6},{8,9},{9,8},{10,11... | collective-permute-start | bytes 196616 | tf_op jit(solution)/shard_map/ppermute | solution.py:219
  32.9 4.5 %collective-permute-start.13 = (bf16[256,128]{1,0:T(8,128)(2,1)S(1)}, bf16[256,128]{1,0:T(8,128)(2,1)S(1)}, u32[]{:S(2)}, u32[]{:S(2)}) collective-permute-start(bf16[256,128]{1,0:T(8,128)(2,1)S(1)} %get-tuple-element.17), channel_id=1, source_target_pairs={{0,2},{1,3},{2,0},{3,1},{4,6},{5,7},{6,4},{7,5},{8,10},{9,11},{10,... | collective-permute-start | bytes 196616 | tf_op jit(solution)/shard_map/ppermute | solution.py:219
  34.5 4.1 %collective-permute-start.14 = (bf16[256,128]{1,0:T(8,128)(2,1)S(1)}, bf16[256,128]{1,0:T(8,128)(2,1)S(1)}, u32[]{:S(2)}, u32[]{:S(2)}) collective-permute-start(bf16[256,128]{1,0:T(8,128)(2,1)S(1)} %get-tuple-element.18), channel_id=1, source_target_pairs={{0,3},{1,2},{2,1},{3,0},{4,7},{5,6},{6,5},{7,4},{8,11},{9,10},{10,... | collective-permute-start | bytes 196616 | tf_op jit(solution)/shard_map/ppermute | solution.py:219
  38.5 55.2 %copy-start.4 = (bf16[1,2048,1024]{2,1,0:T(8,128)(2,1)S(1)}, bf16[1,2048,1024]{2,1,0:T(8,128)(2,1)}, u32[]{:S(2)}) copy-start(bf16[1,2048,1024]{2,1,0:T(8,128)(2,1)} %param.21) | copy-start | bytes 12582916
  38.6 55.2 %copy-start.5 = (bf16[1,2048,1024]{2,1,0:T(8,128)(2,1)S(1)}, bf16[1,2048,1024]{2,1,0:T(8,128)(2,1)}, u32[]{:S(2)}) copy-start(bf16[1,2048,1024]{2,1,0:T(8,128)(2,1)} %param.22) | copy-start | bytes 12582916
  (1 other events, 1.0 us)

commit v11 on v6

--- a/solution.py
+++ b/solution.py
@@ -241,6 +241,7 @@
             )
         mixed_ref[:, at : at + step] = mixed
         power = power + jnp.sum(mixed * mixed, axis=1, keepdims=True)
+    step = width
     scale = lax.rsqrt(power / width + epsilon)
     power = jnp.zeros((row_count, 1), jnp.float32)
     for at in range(0, width, step):

time: 154 us -> 154 us (level)
  no operation moved by 1% of the time
where the time goes in v11:
time: 154 us
  blocking collectives  105 us (68%)
  Pallas kernels  19.9 us (13%)
  waiting for transfers between devices  12.9 us (8%)
  starting transfers between devices  11.3 us (7%)
  local copies, waits for them, and re-layouts  2.57 us (2%)
    all_to_all x2, blocking collectives, exchange(): lax.all_to_all(slots, ('sp', 'tp'), split_axis=0, concat_axis=0, tiled=True)  105 us
    pallas_call x5, Pallas kernels, attend(): pl.pallas_call(functools.partial(attend_kernel, sp_size, pieces, last, ra...  9.2 us
    ppermute x4, waiting for transfers between devices, local(): next_right = lax.ppermute(from_right, 'sp', behind)  7.83 us
    ppermute x4, starting transfers between devices, local(): next_right = lax.ppermute(from_right, 'sp', behind)  7.23 us
    pallas_call x1, Pallas kernels, local(): pl.pallas_call(expert_kernel, out_shape=slots_shape, in_specs=[VMEM] * 4,...  6.8 us
    ppermute x3, waiting for transfers between devices, direct_exchange(): lax.ppermute(pieces[rel], 'tp', [(i, i ^ rel) for i in range(tp_size)])  3.79 us
  transfers between devices with their start and end apart: 11, of which 7 were waited for; matrix products, arithmetic and copies ran while one was open for 1% of the time, Pallas kernels for 5%

profile of v11, /device:TPU:0, one launch (start us, length us, event | category | flops | bytes accessed | tf_op | source)
XLA Modules:
  0.0 153.5 jit_solution(17890431213859834237)
XLA Ops:
  0.0 1.0 pad_maximum_fusion.refs_3_
  1.0 3.0 %collective-permute-start.4 = (bf16[2,2,256,128]{3,2,1,0:T(8,128)(2,1)S(1)}, bf16[2,2,256,128]{3,2,1,0:T(8,128)(2,1)S(1)}, u32[]{:S(2)}, u32[]{:S(2)}) collective-permute-start(bf16[2,2,256,128]{3,2,1,0:T(8,128)(2,1)S(1)} %pad_maximum_fusion.refs_3_), channel_id=1, source_target_pairs={{8,0},{16,8},{24,16},{28,24},{20,28},{12,20},{4,12},{0,4},{9,1},{1... | collective-permute-start | bytes 786440 | tf_op jit(solution)/shard_map/ppermute | solution.py:402
  4.2 0.8 copy.16.expert_ref
  6.2 4.2 %collective-permute-done.4.refs_4_ = bf16[2,2,256,128]{3,2,1,0:T(8,128)(2,1)S(1)} collective-permute-done((bf16[2,2,256,128]{3,2,1,0:T(8,128)(2,1)S(1)}, bf16[2,2,256,128]{3,2,1,0:T(8,128)(2,1)S(1)}, u32[]{:S(2)}, u32[]{:S(2)}) %collective-permute-start.4) | collective-permute-done | bytes 262176 | tf_op jit(solution)/shard_map/ppermute | solution.py:402
  10.4 1.7 %collective-permute-start.5 = (bf16[2,2,256,128]{3,2,1,0:T(8,128)(2,1)S(1)}, bf16[2,2,256,128]{3,2,1,0:T(8,128)(2,1)S(1)}, u32[]{:S(2)}, u32[]{:S(2)}) collective-permute-start(bf16[2,2,256,128]{3,2,1,0:T(8,128)(2,1)S(1)} %collective-permute-done.4.refs_4_), channel_id=1, source_target_pairs={{8,0},{16,8},{24,16},{28,24},{20,28},{12,20},{4,12},{0,4},{9,1},{1... | collective-permute-start | bytes 786440 | tf_op jit(solution)/shard_map/ppermute | solution.py:402
  12.8 0.9 copy-done.7
  13.7 1.5 shard_map.118
  15.2 2.6 %collective-permute-done.5.refs_4_ = bf16[2,2,256,128]{3,2,1,0:T(8,128)(2,1)S(1)} collective-permute-done((bf16[2,2,256,128]{3,2,1,0:T(8,128)(2,1)S(1)}, bf16[2,2,256,128]{3,2,1,0:T(8,128)(2,1)S(1)}, u32[]{:S(2)}, u32[]{:S(2)}) %collective-permute-start.5) | collective-permute-done | bytes 262176 | tf_op jit(solution)/shard_map/ppermute | solution.py:402
  17.9 1.4 collective-permute-start.6
  19.9 2.1 %shard_map.119.refs_5_ = f32[80,2048]{1,0:T(8,128)S(1)} custom-call(bf16[128,2048]{1,0:T(8,128)(2,1)S(1)} %get-tuple-element.13.refs_0_, f32[128,128]{1,0:T(8,128)S(1)} %get-tuple-element.22.refs_1_, f32[128,128]{1,0:T(8,128)S(1)} %get-tuple-element.21.refs_2_, ...), custom_call_target="tpu_custom_call", output_to_operand_aliasing={{}: (5, {})} | custom-call | flops 2147483648 | bytes 1048576 | tf_op jit(solution)/shard_map/pallas_call | solution.py:200
  22.0 2.1 %shard_map.120.refs_5_ = f32[80,2048]{1,0:T(8,128)S(1)} custom-call(bf16[128,2048]{1,0:T(8,128)(2,1)S(1)} %get-tuple-element.13.refs_0_, f32[128,128]{1,0:T(8,128)S(1)} %get-tuple-element.22.refs_1_, f32[128,128]{1,0:T(8,128)S(1)} %get-tuple-element.21.refs_2_, ...), custom_call_target="tpu_custom_call", output_to_operand_aliasing={{}: (5, {})} | custom-call | flops 2147483648 | bytes 1048576 | tf_op jit(solution)/shard_map/pallas_call | solution.py:200
  24.5 1.2 collective-permute-start.7
  25.8 0.9 collective-permute-start.3
  26.7 2.1 %shard_map.122.refs_5_ = f32[80,2048]{1,0:T(8,128)S(1)} custom-call(bf16[128,2048]{1,0:T(8,128)(2,1)S(1)} %get-tuple-element.13.refs_0_, f32[128,128]{1,0:T(8,128)S(1)} %get-tuple-element.22.refs_1_, f32[128,128]{1,0:T(8,128)S(1)} %get-tuple-element.21.refs_2_, ...), custom_call_target="tpu_custom_call", output_to_operand_aliasing={{}: (5, {})} | custom-call | flops 2147483648 | bytes 1048576 | tf_op jit(solution)/shard_map/pallas_call | solution.py:200
  29.5 1.2 collective-permute-done.3.refs_3_
  30.8 1.3 shard_map.123
  32.2 1.6 %collective-permute-start.9 = (bf16[256,128]{1,0:T(8,128)(2,1)S(1)}, bf16[256,128]{1,0:T(8,128)(2,1)S(1)}, u32[]{:S(2)}, u32[]{:S(2)}) collective-permute-start(bf16[256,128]{1,0:T(8,128)(2,1)S(1)} %get-tuple-element.17), channel_id=1, source_target_pairs={{0,2},{1,3},{2,0},{3,1},{4,6},{5,7},{6,4},{7,5},{8,10},{9,11},{10,... | collective-permute-start | bytes 196616 | tf_op jit(solution)/shard_map/ppermute | solution.py:219
  34.0 2.6 %collective-permute-done.9.refs_2_ = bf16[256,128]{1,0:T(8,128)(2,1)S(1)} collective-permute-done((bf16[256,128]{1,0:T(8,128)(2,1)S(1)}, bf16[256,128]{1,0:T(8,128)(2,1)S(1)}, u32[]{:S(2)}, u32[]{:S(2)}) %collective-permute-start.9) | collective-permute-done | bytes 65568 | tf_op jit(solution)/shard_map/ppermute | solution.py:219
  36.7 1.1 collective-permute-done.10.refs_3_
  37.8 1.9 %shard_map.124 = (bf16[128,2048]{1,0:T(8,128)(2,1)S(1)}, bf16[512,2048]{1,0:T(8,128)(2,1)S(1)}) custom-call(bf16[256,128]{1,0:T(8,128)(2,1)S(1)} %get-tuple-element.15.refs_0_, bf16[256,128]{1,0:T(8,128)(2,1)S(1)} %collective-permute-done.8.refs_1_, bf16[256,128]{1,0:T(8,128)(2,1)S(1)} %collective-permute-done.9.refs_2_, ...), custom_call_target="tpu_custom_call" | custom-call | flops 805306368 | bytes 8388608 | tf_op jit(solution)/shard_map/pallas_call | solution.py:417
  39.7 53.1 %all_to_all.10 = bf16[32,16,2048]{2,1,0:T(8,128)(2,1)S(1)} all-to-all(bf16[32,16,2048]{2,1,0:T(8,128)(2,1)S(1)} %bitcast.12), channel_id=1, replica_groups=mesh['sp'=8,'tp'=4] {'sp','tp'}, dimensions={0} | all-to-all | bytes 4194304 | tf_op jit(solution)/shard_map/all_to_all | solution.py:436
  92.8 6.8 %shard_map.125 = bf16[512,2048]{1,0:T(8,128)(2,1)S(1)} custom-call(bf16[512,2048]{1,0:T(8,128)(2,1)S(1)} %bitcast.13, bf16[2048,1024]{1,0:T(8,128)(2,1)S(1)} %bitcast.17, bf16[2048,1024]{1,0:T(8,128)(2,1)S(1)} %bitcast.18, bf16[1024,2048]{1,0:T(8,128)(2,1)S(1)} %bitcast.19), custom_call_target="tpu_custom_call" | custom-call | flops 6442450944 | bytes 16777216 | tf_op jit(solution)/shard_map/pallas_call | solution.py:440
  99.6 52.1 %all_to_all.11 = bf16[32,16,2048]{2,1,0:T(8,128)(2,1)S(1)} all-to-all(bf16[32,16,2048]{2,1,0:T(8,128)(2,1)S(1)} %bitcast.14), channel_id=1, replica_groups=mesh['sp'=8,'tp'=4] {'sp','tp'}, dimensions={0} | all-to-all | bytes 4194304 | tf_op jit(solution)/shard_map/all_to_all | solution.py:436
  151.8 1.6 %shard_map.126 = bf16[128,2048]{1,0:T(8,128)(2,1)} custom-call(bf16[128,2048]{1,0:T(8,128)(2,1)S(1)} %get-tuple-element.19.base_ref, bf16[512,2048]{1,0:T(8,128)(2,1)S(1)} %bitcast.11, f32[8,128]{1,0:T(8,128)S(1)} %shard_map.121.refs_6_.refs_8_.table_ref), custom_call_target="tpu_custom_call" | custom-call | flops 536870912 | bytes 3145728 | tf_op jit(solution)/shard_map/pallas_call | solution.py:453
  (33 shorter events, 4.2 us)
Async XLA Ops:
  1.0 9.4 %collective-permute-start.4 = (bf16[2,2,256,128]{3,2,1,0:T(8,128)(2,1)S(1)}, bf16[2,2,256,128]{3,2,1,0:T(8,128)(2,1)S(1)}, u32[]{:S(2)}, u32[]{:S(2)}) collective-permute-start(bf16[2,2,256,128]{3,2,1,0:T(8,128)(2,1)S(1)} %pad_maximum_fusion.refs_3_), channel_id=1, source_target_pairs={{8,0},{16,8},{24,16},{28,24},{20,28},{12,20},{4,12},{0,4},{9,1},{1... | collective-permute-start | bytes 786440 | tf_op jit(solution)/shard_map/ppermute | solution.py:402
  4.0 8.0 %collective-permute-start = (bf16[2,2,256,128]{3,2,1,0:T(8,128)(2,1)S(1)}, bf16[2,2,256,128]{3,2,1,0:T(8,128)(2,1)S(1)}, u32[]{:S(2)}, u32[]{:S(2)}) collective-permute-start(bf16[2,2,256,128]{3,2,1,0:T(8,128)(2,1)S(1)} %pad_maximum_fusion.refs_3_), channel_id=1, source_target_pairs={{0,8},{8,16},{16,24},{24,28},{28,20},{20,12},{12,4},{4,0},{1,9},{9... | collective-permute-start | bytes 786440 | tf_op jit(solution)/shard_map/ppermute | solution.py:401
  10.4 7.5 %collective-permute-start.5 = (bf16[2,2,256,128]{3,2,1,0:T(8,128)(2,1)S(1)}, bf16[2,2,256,128]{3,2,1,0:T(8,128)(2,1)S(1)}, u32[]{:S(2)}, u32[]{:S(2)}) collective-permute-start(bf16[2,2,256,128]{3,2,1,0:T(8,128)(2,1)S(1)} %collective-permute-done.4.refs_4_), channel_id=1, source_target_pairs={{8,0},{16,8},{24,16},{28,24},{20,28},{12,20},{4,12},{0,4},{9,1},{1... | collective-permute-start | bytes 786440 | tf_op jit(solution)/shard_map/ppermute | solution.py:402
  12.1 7.2 %collective-permute-start.1 = (bf16[2,2,256,128]{3,2,1,0:T(8,128)(2,1)S(1)}, bf16[2,2,256,128]{3,2,1,0:T(8,128)(2,1)S(1)}, u32[]{:S(2)}, u32[]{:S(2)}) collective-permute-start(bf16[2,2,256,128]{3,2,1,0:T(8,128)(2,1)S(1)} %collective-permute-done.refs_3_), channel_id=1, source_target_pairs={{0,8},{8,16},{16,24},{24,28},{28,20},{20,12},{12,4},{4,0},{1,9},{9... | collective-permute-start | bytes 786440 | tf_op jit(solution)/shard_map/ppermute | solution.py:401
  12.8 1.0 copy-start.7
  17.9 6.6 %collective-permute-start.6 = (bf16[2,2,256,128]{3,2,1,0:T(8,128)(2,1)S(1)}, bf16[2,2,256,128]{3,2,1,0:T(8,128)(2,1)S(1)}, u32[]{:S(2)}, u32[]{:S(2)}) collective-permute-start(bf16[2,2,256,128]{3,2,1,0:T(8,128)(2,1)S(1)} %collective-permute-done.5.refs_4_), channel_id=1, source_target_pairs={{8,0},{16,8},{24,16},{28,24},{20,28},{12,20},{4,12},{0,4},{9,1},{1... | collective-permute-start | bytes 786440 | tf_op jit(solution)/shard_map/ppermute | solution.py:402
  19.3 6.4 %collective-permute-start.2 = (bf16[2,2,256,128]{3,2,1,0:T(8,128)(2,1)S(1)}, bf16[2,2,256,128]{3,2,1,0:T(8,128)(2,1)S(1)}, u32[]{:S(2)}, u32[]{:S(2)}) collective-permute-start(bf16[2,2,256,128]{3,2,1,0:T(8,128)(2,1)S(1)} %collective-permute-done.1.refs_3_), channel_id=1, source_target_pairs={{0,8},{8,16},{16,24},{24,28},{28,20},{20,12},{12,4},{4,0},{1,9},{9... | collective-permute-start | bytes 786440 | tf_op jit(solution)/shard_map/ppermute | solution.py:401
  24.5 5.0 %collective-permute-start.7 = (bf16[1,2,256,128]{3,2,1,0:T(8,128)(2,1)S(1)}, bf16[1,2,256,128]{3,2,1,0:T(8,128)(2,1)S(1)}, u32[]{:S(2)}, u32[]{:S(2)}) collective-permute-start(bf16[1,2,256,128]{3,2,1,0:T(8,128)(2,1)S(1)} %slice.9), channel_id=1, source_target_pairs={{8,0},{16,8},{24,16},{28,24},{20,28},{12,20},{4,12},{0,4},{9,1},{1... | collective-permute-start | bytes 393224 | tf_op jit(solution)/shard_map/ppermute | solution.py:402
  25.7 12.1 %copy-start = (bf16[1024,2048]{1,0:T(8,128)(2,1)S(1)}, bf16[1024,2048]{1,0:T(8,128)(2,1)}, u32[]{:S(2)}) copy-start(bf16[1024,2048]{1,0:T(8,128)(2,1)} %refs_4_.1) | copy-start | bytes 12582916
  25.7 12.1 %copy-start.1 = (bf16[128,2048]{1,0:T(8,128)(2,1)S(1)}, bf16[128,2048]{1,0:T(8,128)(2,1)}, u32[]{:S(2)}) copy-start(bf16[128,2048]{1,0:T(8,128)(2,1)} %refs_5_.1) | copy-start | bytes 1572868
  25.7 12.1 %copy-start.2 = (f32[2048]{0:T(1024)S(1)}, f32[2048]{0:T(1024)}, u32[]{:S(2)}) copy-start(f32[2048]{0:T(1024)} %param.17) | copy-start | bytes 24580
  25.7 12.1 %copy-start.3 = (f32[2048]{0:T(1024)S(1)}, f32[2048]{0:T(1024)}, u32[]{:S(2)}) copy-start(f32[2048]{0:T(1024)} %param.18) | copy-start | bytes 24580
  25.8 5.0 %collective-permute-start.3 = (bf16[1,2,256,128]{3,2,1,0:T(8,128)(2,1)S(1)}, bf16[1,2,256,128]{3,2,1,0:T(8,128)(2,1)S(1)}, u32[]{:S(2)}, u32[]{:S(2)}) collective-permute-start(bf16[1,2,256,128]{3,2,1,0:T(8,128)(2,1)S(1)} %slice.8), channel_id=1, source_target_pairs={{0,8},{8,16},{16,24},{24,28},{28,20},{20,12},{12,4},{4,0},{1,9},{9... | collective-permute-start | bytes 393224 | tf_op jit(solution)/shard_map/ppermute | solution.py:401
  30.8 62.0 %copy-start.6 = (bf16[1,1024,2048]{2,1,0:T(8,128)(2,1)S(1)}, bf16[1,1024,2048]{2,1,0:T(8,128)(2,1)}, u32[]{:S(2)}) copy-start(bf16[1,1024,2048]{2,1,0:T(8,128)(2,1)} %param.23) | copy-start | bytes 12582916
  32.1 1.9 %collective-permute-start.8 = (bf16[256,128]{1,0:T(8,128)(2,1)S(1)}, bf16[256,128]{1,0:T(8,128)(2,1)S(1)}, u32[]{:S(2)}, u32[]{:S(2)}) collective-permute-start(bf16[256,128]{1,0:T(8,128)(2,1)S(1)} %get-tuple-element.16), channel_id=1, source_target_pairs={{0,1},{1,0},{2,3},{3,2},{4,5},{5,4},{6,7},{7,6},{8,9},{9,8},{10,11... | collective-permute-start | bytes 196616 | tf_op jit(solution)/shard_map/ppermute | solution.py:219
  32.2 4.5 %collective-permute-start.9 = (bf16[256,128]{1,0:T(8,128)(2,1)S(1)}, bf16[256,128]{1,0:T(8,128)(2,1)S(1)}, u32[]{:S(2)}, u32[]{:S(2)}) collective-permute-start(bf16[256,128]{1,0:T(8,128)(2,1)S(1)} %get-tuple-element.17), channel_id=1, source_target_pairs={{0,2},{1,3},{2,0},{3,1},{4,6},{5,7},{6,4},{7,5},{8,10},{9,11},{10,... | collective-permute-start | bytes 196616 | tf_op jit(solution)/shard_map/ppermute | solution.py:219
  33.7 4.1 %collective-permute-start.10 = (bf16[256,128]{1,0:T(8,128)(2,1)S(1)}, bf16[256,128]{1,0:T(8,128)(2,1)S(1)}, u32[]{:S(2)}, u32[]{:S(2)}) collective-permute-start(bf16[256,128]{1,0:T(8,128)(2,1)S(1)} %get-tuple-element.18), channel_id=1, source_target_pairs={{0,3},{1,2},{2,1},{3,0},{4,7},{5,6},{6,5},{7,4},{8,11},{9,10},{10,... | collective-permute-start | bytes 196616 | tf_op jit(solution)/shard_map/ppermute | solution.py:219
  37.8 55.0 %copy-start.4 = (bf16[1,2048,1024]{2,1,0:T(8,128)(2,1)S(1)}, bf16[1,2048,1024]{2,1,0:T(8,128)(2,1)}, u32[]{:S(2)}) copy-start(bf16[1,2048,1024]{2,1,0:T(8,128)(2,1)} %param.21) | copy-start | bytes 12582916
  37.8 55.0 %copy-start.5 = (bf16[1,2048,1024]{2,1,0:T(8,128)(2,1)S(1)}, bf16[1,2048,1024]{2,1,0:T(8,128)(2,1)}, u32[]{:S(2)}) copy-start(bf16[1,2048,1024]{2,1,0:T(8,128)(2,1)} %param.22) | copy-start | bytes 12582916
